TPU v7x, 512 devices: a whole 4x4x16 slice. The times are simulated.
512 devices in a mesh: tp: 64 (over z, y), dp: 8 (over x, core).
Axes of the slice: x: 4, y: 4, z: 16, core: 2. Of those that a mesh axis runs over, the one named last changes fastest.
Arguments:
- tokens: bfloat16 [192, 4096], P('tp', 'dp'), may hold values from -6 to 6
- lengths: int32 [48], P('dp'), may hold values from 1 to 4, 84 in all
- norm_gain: float32 [2, 4096], P(None, 'dp'), may hold values from 0.1 to 1.9
- gate_weight: bfloat16 [2, 4096, 8192], P(None, 'dp', 'tp'), may hold values from -0.09375 to 0.09375
- value_weight: bfloat16 [2, 4096, 8192], P(None, 'dp', 'tp'), may hold values from -0.09375 to 0.09375
- vector_weight: bfloat16 [2, 4096, 2, 2048], P(None, 'dp', None, 'tp'), may hold values from -0.09375 to 0.09375
- step_weight: bfloat16 [2, 4096, 128], P(None, 'dp'), may hold values from -0.09375 to 0.09375
- step_bias: float32 [2, 128], P(None, 'tp'), may hold values from -3 to 0
- decay_rate: float32 [2, 128], P(None, 'tp'), may hold values from 0.003 to 1
- value_taps: bfloat16 [2, 4, 8192], P(None, None, 'tp'), may hold values from -3 to 3
- vector_taps: bfloat16 [2, 4, 2, 2048], P(None, None, None, 'tp'), may hold values from -3 to 3
- out_weight: bfloat16 [2, 8192, 4096], P(None, 'tp', 'dp'), may hold values from -0.0625 to 0.0625
- recurrent_state: float32 [2, 48, 128, 64, 128], P(None, 'dp', 'tp'), may hold values from -4 to 4
- value_history: bfloat16 [2, 48, 3, 8192], P(None, 'dp', None, 'tp'), may hold values from -6 to 6
- vector_history: bfloat16 [2, 48, 3, 2, 2048], P(None, 'dp', None, None, 'tp'), may hold values from -6 to 6
Outputs:
- next_tokens: bfloat16 [192, 4096], P('tp', 'dp')
- next_state: float32 [2, 48, 128, 64, 128], P(None, 'dp', 'tp')
- next_value_history: bfloat16 [2, 48, 3, 8192], P(None, 'dp', None, 'tp')
- next_vector_history: bfloat16 [2, 48, 3, 2, 2048], P(None, 'dp', None, None, 'tp')
Inputs may be any that keep to these rules, and one draw needn't show every extreme that they name: `lengths`: the number of live new tokens of each sequence; some sequences have more than twice the mean.
All inputs are finite; a program needn't handle non-finite values. No bound on the sum of `lengths` on one device may be relied on, other than what follows from the above.
Results may differ from a plain program's by a relative error of at most 0.029.
Values may be sent and summed in bfloat16 or wider, within the bound.
No kernel may reach another device: no remote copies, remote signals or barrier semaphores. Data moves between devices by JAX's collectives and lax.ppermute only.
A program may use at most 64 MiB of HBM per device.

v0:
```python
import jax
import jax.numpy as jnp
from jax import lax
from jax.sharding import PartitionSpec as P

D = 4096
HEADS = 128
HEAD_DIM = 64
STATE = 128
GROUPS = 16
CONV = 4
NEW = 4
LAYERS = 2


norm_floor = 0.1


def copy_for_each(value, axis):
    peers = lax.axis_size(axis)
    return lax.all_to_all(
        jnp.broadcast_to(value[None], (peers, *value.shape)), axis, 0, 0, tiled=True
    )


def laid_out(pieces, dim):
    dims = list(pieces.shape[1:])
    dims[dim] *= pieces.shape[0]
    return jnp.moveaxis(pieces, 0, dim).reshape(dims)


def gather_directly(value, axis, dim):
    pieces = copy_for_each(value, axis)
    return laid_out(pieces, dim)


def split_up(value, dim, peers):
    dims = value.shape
    pieces = value.reshape(*dims[:dim], peers, dims[dim] // peers, *dims[dim + 1 :])
    return jnp.moveaxis(pieces, dim, 0)


def sum_at_owner(value, axis, dim):
    peers = lax.axis_size(axis)
    pieces = lax.all_to_all(split_up(value, dim, peers), axis, 0, 0, tiled=True)
    return jnp.sum(pieces, axis=0)


def sent_together(arrays, axis, dim, along):
    columns = [a.reshape(*a.shape[:along], -1) for a in arrays]
    both = jnp.concatenate(columns, axis=along)
    filled, at, finished = (sum_at_owner(both, axis, dim), 0, [])
    for a, column in zip(arrays, columns):
        slab = filled[..., at : at + column.shape[along]]
        finished.append(slab.reshape(*slab.shape[:along], *a.shape[along:]))
        at += column.shape[along]
    return tuple(finished)


def short_conv(history, fresh_rows, conv_taps):
    padded = jnp.concatenate([history, fresh_rows], axis=1)
    block_len = fresh_rows.shape[1]
    summed = jnp.zeros(fresh_rows.shape, jnp.float32)
    for offset in range(conv_taps.shape[0]):
        summed = summed + padded[:, offset : offset + block_len].astype(jnp.float32) * conv_taps[
            offset
        ].astype(jnp.float32)
    return (jax.nn.silu(summed), padded)


def state_block(values, write_vec, read_vec, step_sizes, rate_vec, carried_state):
    block_len = values.shape[1]
    cumulative = jnp.cumsum(step_sizes * rate_vec, axis=1)
    causal = jnp.tril(jnp.ones((block_len, block_len), dtype=bool))[None, :, :, None, None]
    log_gap = cumulative[:, :, None] - cumulative[:, None, :]
    decays = jnp.where(causal, jnp.exp(-jnp.where(causal, log_gap, 0.0)), 0.0)
    scores = jnp.einsum("stgn,sugn->stug", read_vec, write_vec)
    weights = scores[..., None] * decays * step_sizes[:, None]
    within = jnp.einsum("stugr,sugrp->stgrp", weights, values)
    carried = (
        jnp.einsum("stgn,sgrpn->stgrp", read_vec, carried_state) * jnp.exp(-cumulative)[..., None]
    )
    ending = jnp.exp(cumulative - cumulative[:, -1:]) * step_sizes
    weighted = values * ending[..., None]
    fresh_state = jnp.einsum("sugrp,sugn->sgrpn", weighted, write_vec)
    next_state = carried_state * jnp.exp(-cumulative[:, -1])[..., None, None] + fresh_state
    return (within + carried, next_state)


def collect(token_rows):
    return gather_directly(token_rows, "tp", 0)


def body(
    tokens,
    lengths,
    norm_gain,
    gate_weight,
    value_weight,
    vector_weight,
    step_weight,
    step_bias,
    decay_rate,
    value_taps,
    vector_taps,
    out_weight,
    recurrent_state,
    value_history,
    vector_history,
):
    local_seqs = lengths.shape[0]
    local_heads = step_bias.shape[1]
    local_tokens = local_seqs * NEW
    heads_group = HEADS // GROUPS
    group_count = max(1, local_heads // heads_group)
    per_group = local_heads // group_count
    live_mask = (jnp.arange(NEW, dtype=jnp.int32)[None, :] < lengths[:, None]).astype(jnp.float32)
    kept_rows = lengths[:, None] + jnp.arange(CONV - 1, dtype=jnp.int32)[None, :]
    picker = (
        kept_rows[:, :, None] == jnp.arange(CONV - 1 + NEW, dtype=jnp.int32)[None, None, :]
    ).astype(jnp.bfloat16)
    head_start = lax.axis_index("tp") * local_heads
    first_group = head_start // heads_group
    token_rows = tokens
    whole = collect(tokens)
    state_list, value_list, vector_list = ([], [], [])
    for ordinal in range(LAYERS):
        widened = whole.astype(jnp.float32)
        squares = jnp.sum(widened * widened, axis=1)
        normed = (widened * norm_gain[ordinal]).astype(jnp.bfloat16)
        own_step = lax.dynamic_slice_in_dim(step_weight[ordinal], head_start, local_heads, 1)
        gate_part = jnp.dot(normed, gate_weight[ordinal], preferred_element_type=jnp.float32)
        value_part = jnp.dot(normed, value_weight[ordinal], preferred_element_type=jnp.float32)
        vector_part = jnp.einsum(
            "td,dkc->tkc", normed, vector_weight[ordinal], preferred_element_type=jnp.float32
        )
        step_part = jnp.dot(normed, own_step, preferred_element_type=jnp.float32)
        gate_sum, value_sum, vector_sum, step_sum, own_squares = sent_together(
            (gate_part, value_part, vector_part, step_part, squares), "dp", 0, 1
        )
        scaling = lax.rsqrt(own_squares / D + norm_floor)[:, None]
        gate = (gate_sum * scaling).astype(jnp.bfloat16)
        value_in = (value_sum * scaling).astype(jnp.bfloat16)
        vector_in = (vector_sum * scaling[:, :, None]).astype(jnp.bfloat16)
        step_in = (step_sum * scaling).astype(jnp.bfloat16)
        step_sizes = (
            jax.nn.softplus(
                step_in.astype(jnp.float32).reshape(local_seqs, NEW, local_heads)
                + step_bias[ordinal]
            )
            * live_mask[:, :, None]
        )
        value_conv, padded_value = short_conv(
            value_history[ordinal], value_in.reshape(local_seqs, NEW, -1), value_taps[ordinal]
        )
        vector_conv, padded_vector = short_conv(
            vector_history[ordinal], vector_in.reshape(local_seqs, NEW, 2, -1), vector_taps[ordinal]
        )
        vector_whole = gather_directly(vector_conv, "tp", 3)
        arranged = vector_whole.reshape(local_seqs, NEW, 2, STATE, GROUPS)
        own_vectors = lax.dynamic_slice_in_dim(arranged, first_group, group_count, 4)
        write_vec = jnp.swapaxes(own_vectors[:, :, 0], 2, 3)
        read_vec = jnp.swapaxes(own_vectors[:, :, 1], 2, 3)
        output, next_state = state_block(
            value_conv.reshape(local_seqs, NEW, group_count, per_group, HEAD_DIM),
            write_vec,
            read_vec,
            step_sizes.reshape(local_seqs, NEW, group_count, per_group),
            decay_rate[ordinal].reshape(group_count, per_group),
            recurrent_state[ordinal].reshape(local_seqs, group_count, per_group, HEAD_DIM, STATE),
        )
        state_list.append(next_state.reshape(recurrent_state.shape[1:]))
        value_list.append(
            jnp.einsum(
                "sjk,skc->sjc", picker, padded_value, preferred_element_type=jnp.float32
            ).astype(jnp.bfloat16)
        )
        vector_list.append(
            jnp.einsum(
                "sjk,skmc->sjmc", picker, padded_vector, preferred_element_type=jnp.float32
            ).astype(jnp.bfloat16)
        )
        gated = (
            output.reshape(local_seqs, NEW, -1)
            * jax.nn.silu(gate.astype(jnp.float32).reshape(local_seqs, NEW, -1))
            * live_mask[:, :, None]
        )
        mixed = gated.reshape(local_tokens, -1).astype(jnp.bfloat16)
        mixed_all = gather_directly(mixed, "dp", 0)
        layer_out = out_weight[ordinal]
        update = sum_at_owner(
            jnp.dot(mixed_all, layer_out, preferred_element_type=jnp.float32), "tp", 0
        )
        token_rows = (token_rows.astype(jnp.float32) + update).astype(jnp.bfloat16)
        if ordinal + 1 < LAYERS:
            whole = collect(token_rows)
    return (token_rows, jnp.stack(state_list), jnp.stack(value_list), jnp.stack(vector_list))


def solution(mesh):
    return jax.shard_map(
        body,
        mesh=mesh,
        in_specs=(
            P("tp", "dp"),
            P("dp"),
            P(None, "dp"),
            P(None, "dp", "tp"),
            P(None, "dp", "tp"),
            P(None, "dp", None, "tp"),
            P(None, "dp", None),
            P(None, "tp"),
            P(None, "tp"),
            P(None, None, "tp"),
            P(None, None, None, "tp"),
            P(None, "tp", "dp"),
            P(None, "dp", "tp", None, None),
            P(None, "dp", None, "tp"),
            P(None, "dp", None, None, "tp"),
        ),
        out_specs=(
            P("tp", "dp"),
            P(None, "dp", "tp", None, None),
            P(None, "dp", None, "tp"),
            P(None, "dp", None, None, "tp"),
        ),
        check_vma=False,
    )
```

profile of v0, /device:TPU:1, one launch (start us, length us, event | category | flops | bytes accessed | tf_op | source)
XLA Modules:
  0.0 258.2 jit_solution(2208537713792775392)
XLA Ops:
  0.6 1.5 broadcast_in_dim.42
  2.1 19.4 %all-to-all-start = ((bf16[64,3,512]{2,1,0:T(4,128)(2,1)}), bf16[64,3,512]{2,1,0:T(4,128)(2,1)S(1)}, u32[]{:S(2)}, u32[]{:S(2)}) async-start(bf16[64,3,512]{2,1,0:T(4,128)(2,1)} %broadcast_in_dim.42), calls=%async_computation | async-start | bytes 524288 | tf_op jit(solution)/shard_map/all_to_all | solution.py:21
  24.7 1.4 bitcast_convert_fusion.7
  29.4 11.6 %all-to-all-done = bf16[64,3,512]{2,1,0:T(4,128)(2,1)S(1)} async-done(((bf16[64,3,512]{2,1,0:T(4,128)(2,1)}), bf16[64,3,512]{2,1,0:T(4,128)(2,1)S(1)}, u32[]{:S(2)}, u32[]{:S(2)}) %all-to-all-start) | async-done | bytes 196640 | tf_op jit(solution)/shard_map/all_to_all | solution.py:21
  43.4 8.2 %all-to-all-start.1 = ((f32[8,24,323]{2,1,0:T(8,128)}), f32[8,24,323]{2,1,0:T(8,128)S(1)}, u32[]{:S(2)}, u32[]{:S(2)}) async-start(f32[8,24,323]{2,1,0:T(8,128)} %concatenate.25), calls=%async_computation.1 | async-start | bytes 589824 | tf_op jit(solution)/shard_map/all_to_all | solution.py:45
  51.6 6.8 %all-to-all-done.1 = f32[8,24,323]{2,1,0:T(8,128)S(1)} async-done(((f32[8,24,323]{2,1,0:T(8,128)}), f32[8,24,323]{2,1,0:T(8,128)S(1)}, u32[]{:S(2)}, u32[]{:S(2)}) %all-to-all-start.1) | async-done | bytes 248096 | tf_op jit(solution)/shard_map/all_to_all | solution.py:45
  59.6 1.3 reshape.661
  60.9 4.7 %all-to-all-start.2 = ((bf16[64,2,768]{2,1,0:T(2,128)(2,1)}), bf16[64,2,768]{2,1,0:T(2,128)(2,1)S(1)}, u32[]{:S(2)}, u32[]{:S(2)}) async-start(bf16[64,2,768]{2,1,0:T(2,128)(2,1)} %reshape.661), calls=%async_computation.2 | async-start | bytes 393216 | tf_op jit(solution)/shard_map/all_to_all | solution.py:21
  67.0 15.6 %all-to-all-done.2 = bf16[64,2,768]{2,1,0:T(2,128)(2,1)S(1)} async-done(((bf16[64,2,768]{2,1,0:T(2,128)(2,1)}), bf16[64,2,768]{2,1,0:T(2,128)(2,1)S(1)}, u32[]{:S(2)}, u32[]{:S(2)}) %all-to-all-start.2) | async-done | bytes 196640 | tf_op jit(solution)/shard_map/all_to_all | solution.py:21
  83.9 1.4 constant_dynamic-slice_fusion.1
  85.3 1.5 copy.420
  88.1 11.4 %all_to_all.50 = bf16[8,24,128]{2,1,0:T(8,128)(2,1)S(1)} all-to-all(bf16[8,24,128]{2,1,0:T(8,128)(2,1)S(1)} %broadcast_in_dim.46), channel_id=1, replica_groups=mesh['tp'=64,'dp'=8] {'dp'}, dimensions={0} | all-to-all | bytes 98304 | tf_op jit(solution)/shard_map/all_to_all | solution.py:21
  100.1 33.9 %all_to_all.51 = f32[64,3,512]{2,1,0:T(4,128)S(1)} all-to-all(f32[64,3,512]{2,1,0:T(4,128)S(1)} %copy.372), channel_id=1, replica_groups=mesh['tp'=64,'dp'=8] {'tp'}, dimensions={0} | all-to-all | bytes 786432 | tf_op jit(solution)/shard_map/all_to_all | solution.py:45
  134.2 26.5 %all_to_all.52 = bf16[64,3,512]{2,1,0:T(4,128)(2,1)S(1)} all-to-all(bf16[64,3,512]{2,1,0:T(4,128)(2,1)S(1)} %broadcast_in_dim.47), channel_id=1, replica_groups=mesh['tp'=64,'dp'=8] {'tp'}, dimensions={0} | all-to-all | bytes 393216 | tf_op jit(solution)/shard_map/all_to_all | solution.py:21
  162.3 14.6 %all_to_all.53 = f32[8,24,323]{2,1,0:T(8,128)S(1)} all-to-all(f32[8,24,323]{2,1,0:T(8,128)S(1)} %concatenate.29), channel_id=1, replica_groups=mesh['tp'=64,'dp'=8] {'dp'}, dimensions={0} | all-to-all | bytes 496128 | tf_op jit(solution)/shard_map/all_to_all | solution.py:45
  178.2 1.3 reshape.663
  179.4 4.6 %all-to-all-start.7 = ((bf16[64,2,768]{2,1,0:T(2,128)(2,1)}), bf16[64,2,768]{2,1,0:T(2,128)(2,1)S(1)}, u32[]{:S(2)}, u32[]{:S(2)}) async-start(bf16[64,2,768]{2,1,0:T(2,128)(2,1)} %reshape.663), calls=%async_computation.7 | async-start | bytes 393216 | tf_op jit(solution)/shard_map/all_to_all | solution.py:21
  185.5 16.8 %all-to-all-done.7 = bf16[64,2,768]{2,1,0:T(2,128)(2,1)S(1)} async-done(((bf16[64,2,768]{2,1,0:T(2,128)(2,1)}), bf16[64,2,768]{2,1,0:T(2,128)(2,1)S(1)}, u32[]{:S(2)}, u32[]{:S(2)}) %all-to-all-start.7) | async-done | bytes 196640 | tf_op jit(solution)/shard_map/all_to_all | solution.py:21
  203.8 2.4 reshape_reshape.7
  206.2 1.4 constant_dynamic-slice_fusion
  207.6 1.5 copy.426
  210.4 10.3 %all_to_all.54 = bf16[8,24,128]{2,1,0:T(8,128)(2,1)S(1)} all-to-all(bf16[8,24,128]{2,1,0:T(8,128)(2,1)S(1)} %broadcast_in_dim.49), channel_id=1, replica_groups=mesh['tp'=64,'dp'=8] {'dp'}, dimensions={0} | all-to-all | bytes 98304 | tf_op jit(solution)/shard_map/all_to_all | solution.py:21
  221.9 4.6 %all-to-all-start.9 = ((f32[64,3,512]{2,1,0:T(4,128)}), f32[64,3,512]{2,1,0:T(4,128)S(1)}, u32[]{:S(2)}, u32[]{:S(2)}) async-start(f32[64,3,512]{2,1,0:T(4,128)} %copy.395), calls=%async_computation.9 | async-start | bytes 1048576 | tf_op jit(solution)/shard_map/all_to_all | solution.py:45
  230.8 26.7 %all-to-all-done.9 = f32[64,3,512]{2,1,0:T(4,128)S(1)} async-done(((f32[64,3,512]{2,1,0:T(4,128)}), f32[64,3,512]{2,1,0:T(4,128)S(1)}, u32[]{:S(2)}, u32[]{:S(2)}) %all-to-all-start.9) | async-done | bytes 393248 | tf_op jit(solution)/shard_map/all_to_all | solution.py:45
  (165 shorter events, 27.6 us)
Async XLA Ops:
  0.6 41.1 %copy-start.1 = (bf16[2,512,128]{2,1,0:T(8,128)(2,1)S(1)}, bf16[2,512,128]{2,1,0:T(8,128)(2,1)}, u32[]{:S(2)}) copy-start(bf16[2,512,128]{2,1,0:T(8,128)(2,1)} %param.19) | copy-start | bytes 786436
  2.1 39.8 %copy-start.3 = (bf16[2,512,128]{2,1,0:T(8,128)(2,1)S(1)}, bf16[2,512,128]{2,1,0:T(8,128)(2,1)}, u32[]{:S(2)}) copy-start(bf16[2,512,128]{2,1,0:T(8,128)(2,1)} %param.18) | copy-start | bytes 786436
  2.1 38.9 %all-to-all-start = ((bf16[64,3,512]{2,1,0:T(4,128)(2,1)}), bf16[64,3,512]{2,1,0:T(4,128)(2,1)S(1)}, u32[]{:S(2)}, u32[]{:S(2)}) async-start(bf16[64,3,512]{2,1,0:T(4,128)(2,1)} %broadcast_in_dim.42), calls=%async_computation | async-start | bytes 524288 | tf_op jit(solution)/shard_map/all_to_all | solution.py:21
  41.5 10.1 %copy-start.12 = (f32[2,2]{1,0:T(2,128)S(1)}, f32[2,2]{1,0:T(2,128)}, u32[]{:S(2)}) copy-start(f32[2,2]{1,0:T(2,128)} %param.23) | copy-start | bytes 52
  41.5 10.1 %copy-start.13 = (f32[2,2]{1,0:T(2,128)S(1)}, f32[2,2]{1,0:T(2,128)}, u32[]{:S(2)}) copy-start(f32[2,2]{1,0:T(2,128)} %param.22) | copy-start | bytes 52
  43.4 15.0 %all-to-all-start.1 = ((f32[8,24,323]{2,1,0:T(8,128)}), f32[8,24,323]{2,1,0:T(8,128)S(1)}, u32[]{:S(2)}, u32[]{:S(2)}) async-start(f32[8,24,323]{2,1,0:T(8,128)} %concatenate.25), calls=%async_computation.1 | async-start | bytes 589824 | tf_op jit(solution)/shard_map/all_to_all | solution.py:45
  60.9 21.7 %all-to-all-start.2 = ((bf16[64,2,768]{2,1,0:T(2,128)(2,1)}), bf16[64,2,768]{2,1,0:T(2,128)(2,1)S(1)}, u32[]{:S(2)}, u32[]{:S(2)}) async-start(bf16[64,2,768]{2,1,0:T(2,128)(2,1)} %reshape.661), calls=%async_computation.2 | async-start | bytes 393216 | tf_op jit(solution)/shard_map/all_to_all | solution.py:21
  85.3 2.1 copy-start.14
  85.3 2.3 copy-start
  85.3 14.2 %copy-start.5 = (bf16[2,128,512]{2,1,0:T(8,128)(2,1)S(1)}, bf16[2,128,512]{2,1,0:T(8,128)(2,1)}, u32[]{:S(2)}) copy-start(bf16[2,128,512]{2,1,0:T(8,128)(2,1)} %param.26) | copy-start | bytes 786436
  99.5 34.5 %copy-start.7 = (bf16[3,512]{1,0:T(4,128)(2,1)S(1)}, bf16[3,512]{1,0:T(4,128)(2,1)}, u32[]{:S(2)}) copy-start(bf16[3,512]{1,0:T(4,128)(2,1)} %param.15) | copy-start | bytes 9220
  100.1 61.1 %copy-start.2 = (bf16[2,512,128]{2,1,0:T(8,128)(2,1)S(1)}, bf16[2,512,128]{2,1,0:T(8,128)(2,1)}, u32[]{:S(2)}) copy-start(bf16[2,512,128]{2,1,0:T(8,128)(2,1)} %param.19) | copy-start | bytes 786436
  134.0 27.4 %copy-start.4 = (bf16[2,512,128]{2,1,0:T(8,128)(2,1)S(1)}, bf16[2,512,128]{2,1,0:T(8,128)(2,1)}, u32[]{:S(2)}) copy-start(bf16[2,512,128]{2,1,0:T(8,128)(2,1)} %param.18) | copy-start | bytes 786436
  176.9 7.9 %copy-start.9 = (f32[128]{0:T(128)S(1)}, f32[128]{0:T(128)}, u32[]{:S(2)}) copy-start(f32[128]{0:T(128)} %get-tuple-element.65) | copy-start | bytes 1540
  176.9 7.9 %copy-start.10 = (f32[128]{0:T(128)S(1)}, f32[128]{0:T(128)}, u32[]{:S(2)}) copy-start(f32[128]{0:T(128)} %get-tuple-element.70) | copy-start | bytes 1540
  176.9 7.9 %copy-start.11 = (f32[128]{0:T(128)S(1)}, f32[128]{0:T(128)}, u32[]{:S(2)}) copy-start(f32[128]{0:T(128)} %get-tuple-element.71) | copy-start | bytes 1540
  179.4 22.9 %all-to-all-start.7 = ((bf16[64,2,768]{2,1,0:T(2,128)(2,1)}), bf16[64,2,768]{2,1,0:T(2,128)(2,1)S(1)}, u32[]{:S(2)}, u32[]{:S(2)}) async-start(bf16[64,2,768]{2,1,0:T(2,128)(2,1)} %reshape.663), calls=%async_computation.7 | async-start | bytes 393216 | tf_op jit(solution)/shard_map/all_to_all | solution.py:21
  207.6 2.0 copy-start.15
  207.6 13.0 %copy-start.6 = (bf16[2,128,512]{2,1,0:T(8,128)(2,1)S(1)}, bf16[2,128,512]{2,1,0:T(8,128)(2,1)}, u32[]{:S(2)}) copy-start(bf16[2,128,512]{2,1,0:T(8,128)(2,1)} %param.26) | copy-start | bytes 786436
  210.1 16.4 %copy-start.8 = (s32[6]{0:T(128)S(1)}, s32[6]{0:T(128)}, u32[]{:S(2)}) copy-start(s32[6]{0:T(128)} %param.16) | copy-start | bytes 76
  221.9 35.5 %all-to-all-start.9 = ((f32[64,3,512]{2,1,0:T(4,128)}), f32[64,3,512]{2,1,0:T(4,128)S(1)}, u32[]{:S(2)}, u32[]{:S(2)}) async-start(f32[64,3,512]{2,1,0:T(4,128)} %copy.395), calls=%async_computation.9 | async-start | bytes 1048576 | tf_op jit(solution)/shard_map/all_to_all | solution.py:45
where the time goes:
time: 260 us; the launch traced here: 258 us
  blocking collectives  96.7 us (37%)
  waiting for transfers between devices  77.5 us (30%)
  starting transfers between devices  41.6 us (16%)
  local copies, waits for them, and re-layouts  28.4 us (11%)
  other arithmetic  8.09 us (3%)
  matrix products  4.77 us (2%)
    all_to_all x2, blocking collectives, sum_at_owner(): pieces = lax.all_to_all(split_up(value, dim, peers), axis, 0, 0, tiled=True)  48.5 us
    all_to_all x3, blocking collectives, copy_for_each(): lax.all_to_all(jnp.broadcast_to(value[None], (peers, *value.shape)), axis...  48.2 us
    all_to_all x3, waiting for transfers between devices, copy_for_each(): lax.all_to_all(jnp.broadcast_to(value[None], (peers, *value.shape)), axis...  44 us
    all_to_all x2, waiting for transfers between devices, sum_at_owner(): pieces = lax.all_to_all(split_up(value, dim, peers), axis, 0, 0, tiled=True)  33.5 us
    all_to_all x3, starting transfers between devices, copy_for_each(): lax.all_to_all(jnp.broadcast_to(value[None], (peers, *value.shape)), axis...  28.7 us
    all_to_all x2, starting transfers between devices, sum_at_owner(): pieces = lax.all_to_all(split_up(value, dim, peers), axis, 0, 0, tiled=True)  12.8 us
    unnamed x44, local copies, waits for them, and re-layouts  8.33 us
  transfers between devices with their start and end apart: 5, of which 5 were waited for; matrix products, arithmetic and copies ran while one was open for 6% of the time, Pallas kernels for 0%

commit v1 on v0

v1 whole, which is shorter than its diff:
```python
import jax
import jax.numpy as jnp
from jax import lax
from jax.sharding import Mesh, PartitionSpec as P

D = 4096
HEADS = 128
HEAD_DIM = 64
STATE = 128
GROUPS = 16
CONV = 4
NEW = 4
LAYERS = 2
norm_floor = 0.1

ZN, YN, DN = 16, 4, 8
SEQ = 6
bf16 = jnp.bfloat16
f32 = jnp.float32
COLS = 640


def exchange(pieces, axis):
    return lax.all_to_all(pieces, axis, 0, 0, tiled=True)


def copies(value, peers):
    return jnp.broadcast_to(value[None], (peers, *value.shape))


def short_conv(history, fresh_rows, conv_taps):
    padded = jnp.concatenate([history, fresh_rows], axis=1)
    summed = jnp.zeros(fresh_rows.shape, f32)
    for offset in range(CONV):
        summed = summed + padded[:, offset : offset + NEW].astype(f32) * conv_taps[offset].astype(
            f32
        )
    return (jax.nn.silu(summed), padded)


def project(rows, gain, gate_w, value_w, vector_w, step_w, square_lane):
    widened = rows.astype(f32)
    squares = jnp.sum(widened * widened, axis=1, keepdims=True)
    normed = (widened * gain[None]).astype(bf16)
    gate = jnp.einsum("td,ydc->tyc", normed, gate_w, preferred_element_type=f32)
    value = jnp.einsum("td,ydc->tyc", normed, value_w, preferred_element_type=f32)
    vector = jnp.einsum("td,cd->tc", normed, vector_w, preferred_element_type=f32)
    step = jnp.dot(normed, step_w, preferred_element_type=f32)
    lane = jnp.arange(HEADS, dtype=jnp.int32)[None]
    extra = jnp.where(lane == square_lane, squares, step)
    width = gate_w.shape[0]
    shared = jnp.concatenate([vector, extra], axis=1).astype(bf16)
    parts = [gate.astype(bf16), value.astype(bf16)]
    parts.append(jnp.broadcast_to(shared[:, None], (rows.shape[0], width, shared.shape[1])))
    return jnp.concatenate(parts, axis=2)


def middle(total, head_start, square_lane, live_mask, picker, bias, rate, history, taps, vhist, vtaps, state):
    squares = lax.dynamic_slice_in_dim(total, 512 + square_lane, 1, 1)
    scaling = lax.rsqrt(squares / D + norm_floor)
    scaled = (total * scaling).astype(bf16)
    gate = scaled[:, :128]
    value_in = scaled[:, 128:256]
    vector_in = scaled[:, 256:512]
    step_in = lax.dynamic_slice_in_dim(scaled, 512 + head_start, 2, 1)
    step = (
        jax.nn.softplus(step_in.astype(f32).reshape(SEQ, NEW, 2) + bias) * live_mask[:, :, None]
    )
    value_conv, padded_value = short_conv(history, value_in.reshape(SEQ, NEW, 128), taps)
    vector_conv, padded_vector = short_conv(vhist, vector_in.reshape(SEQ, NEW, 256), vtaps)
    write = vector_conv[:, :, :128]
    read = vector_conv[:, :, 128:]
    values = value_conv.reshape(SEQ, NEW, 2, HEAD_DIM)
    cumulative = jnp.cumsum(step * rate, axis=1)
    causal = jnp.tril(jnp.ones((NEW, NEW), dtype=bool))[None, :, :, None]
    log_gap = cumulative[:, :, None] - cumulative[:, None, :]
    decays = jnp.where(causal, jnp.exp(-jnp.where(causal, log_gap, 0.0)), 0.0)
    scores = jnp.einsum("stn,sun->stu", read, write)
    weights = scores[..., None] * decays * step[:, None]
    within = jnp.einsum("stur,surp->strp", weights, values)
    carried = jnp.einsum("stn,srpn->strp", read, state) * jnp.exp(-cumulative)[..., None]
    ending = jnp.exp(cumulative - cumulative[:, -1:]) * step
    weighted = values * ending[..., None]
    fresh = jnp.einsum("surp,sun->srpn", weighted, write)
    next_state = state * jnp.exp(-cumulative[:, -1])[..., None, None] + fresh
    output = (within + carried).reshape(SEQ, NEW, 128)
    gated = (
        output * jax.nn.silu(gate.astype(f32).reshape(SEQ, NEW, 128)) * live_mask[:, :, None]
    )
    mixed = gated.astype(bf16)
    next_value = jnp.einsum(
        "sjk,skc->sjc", picker, padded_value, preferred_element_type=f32
    ).astype(bf16)
    next_vector = jnp.einsum(
        "sjk,skc->sjc", picker, padded_vector, preferred_element_type=f32
    ).astype(bf16)
    return mixed, next_state, next_value, next_vector


def send_mixed(mixed):
    rows = mixed.reshape(2, YN, 3, 128).transpose(1, 0, 2, 3)
    rows = jnp.pad(rows, ((0, 0), (0, 0), (0, 1), (0, 0))).reshape(YN, 1, 8, 128)
    rows = jnp.broadcast_to(rows, (YN, DN, 8, 128)).reshape(YN * DN, 8, 128)
    return exchange(rows, ("y", "dp")).reshape(YN, DN * 8, 128)


def body(
    tokens,
    lengths,
    norm_gain,
    gate_weight,
    value_weight,
    vector_weight,
    step_weight,
    step_bias,
    decay_rate,
    value_taps,
    vector_taps,
    out_weight,
    recurrent_state,
    value_history,
    vector_history,
):
    z = lax.axis_index("z")
    y = lax.axis_index("y")
    head_start = 8 * z + 2 * y
    square_lane = (8 * z + 64) % HEADS
    live_mask = (jnp.arange(NEW, dtype=jnp.int32)[None, :] < lengths[:, None]).astype(f32)
    kept_rows = lengths[:, None] + jnp.arange(CONV - 1, dtype=jnp.int32)[None, :]
    picker = (
        kept_rows[:, :, None] == jnp.arange(CONV - 1 + NEW, dtype=jnp.int32)[None, None, :]
    ).astype(bf16)

    vector_cols = vector_weight.transpose(0, 2, 3, 1).reshape(2, 2, 2, GROUPS, 512)
    vector_cols = vector_cols.transpose(3, 0, 1, 2, 4).reshape(GROUPS, 8, 512)
    small = jnp.concatenate([vector_history.reshape(72, 32), vector_taps.reshape(16, 32)], axis=0)
    small = small.reshape(88, 2, GROUPS).transpose(2, 1, 0).reshape(GROUPS, 1, 176)
    small = jnp.pad(small, ((0, 0), (0, 0), (0, 512 - 176)))
    first = jnp.concatenate(
        [copies(tokens, ZN), vector_cols[:, :4], small, vector_cols[:, 4:]], axis=1
    )
    first = exchange(first, "z")
    own_out = exchange(copies(out_weight[0], YN), "y")
    plane = exchange(copies(first[:, :8], YN), "y")

    def lanes(w):
        return w.reshape(4, 128, 128).transpose(1, 0, 2).reshape(128, 512)

    later = jnp.concatenate(
        [
            lanes(gate_weight[1]),
            lanes(value_weight[1]),
            out_weight[1],
            first[:, 8:].reshape(64, 512),
        ],
        axis=0,
    )
    later = exchange(copies(later, YN), "y")

    whole = plane[:, :, :3].transpose(1, 0, 2, 3).reshape(192, 512)
    vector_w = [
        plane[:, :, 3:7].reshape(YN, ZN, 2, 2, 512).transpose(2, 1, 0, 3, 4).reshape(256, 512),
        later[:, 384:].reshape(YN, ZN, 2, 2, 512).transpose(2, 1, 0, 3, 4).reshape(256, 512),
    ]
    small = plane[:, :, 7, :176].reshape(YN, ZN, 2, 88).transpose(3, 1, 0, 2).reshape(88, 128)
    vhist = small[:72].reshape(2, SEQ, 3, 256)
    vtaps = small[72:].reshape(2, CONV, 256)

    def mid(total, layer):
        return middle(
            total,
            head_start,
            square_lane,
            live_mask,
            picker,
            step_bias[layer],
            decay_rate[layer],
            value_history[layer],
            value_taps[layer],
            vhist[layer],
            vtaps[layer],
            recurrent_state[layer],
        )

    part = project(
        whole,
        norm_gain[0],
        gate_weight[:1],
        value_weight[:1],
        vector_w[0],
        step_weight[0],
        square_lane,
    )
    part = exchange(part.reshape(DN, 24, COLS), "dp")
    total = jnp.sum(part.astype(f32), axis=0)
    mixed, state0, value0, vector0 = mid(total, 0)
    mixed = send_mixed(mixed)
    update = jnp.einsum("ytc,ycf->tf", mixed, own_out, preferred_element_type=f32)
    update = exchange(update.astype(bf16).reshape(ZN, 4, 512), "z")
    update = jnp.sum(update.astype(f32), axis=0)[:3]
    token_rows = (tokens.astype(f32) + update).astype(bf16)

    quarter = exchange(copies(jnp.pad(token_rows, ((0, 1), (0, 0))), ZN), "z").reshape(64, 512)

    def unlanes(w):
        return w.reshape(YN, 128, 4, 128).transpose(0, 2, 1, 3).reshape(YN, 512, 128)

    part = project(
        quarter,
        norm_gain[1],
        unlanes(later[:, :128]),
        unlanes(later[:, 128:256]),
        vector_w[1],
        step_weight[1],
        square_lane,
    )
    part = part.reshape(DN, 8, YN, COLS).transpose(2, 0, 1, 3).reshape(YN * DN, 8, COLS)
    part = exchange(part, ("y", "dp")).reshape(YN, DN, 8, COLS)
    total = jnp.sum(part.astype(f32), axis=1).reshape(YN, 2, 4, COLS)[:, :, :3]
    total = total.transpose(1, 0, 2, 3).reshape(24, COLS)
    mixed, state1, value1, vector1 = mid(total, 1)
    mixed = send_mixed(mixed)
    update = jnp.einsum("ytc,ycf->tf", mixed, later[:, 256:384], preferred_element_type=f32)
    update = update.astype(bf16).reshape(ZN, 4, 512)
    returned = jnp.stack([vector0, vector1]).reshape(72, ZN, YN, 2)
    returned = lax.dynamic_index_in_dim(returned, y, 2, keepdims=False)
    returned = returned.reshape(36, 2, ZN, 2).transpose(2, 3, 0, 1).reshape(ZN, 1, 144)
    returned = jnp.pad(returned, ((0, 0), (0, 0), (0, 512 - 144)))
    update = exchange(jnp.concatenate([update[:, :3], returned], axis=1), "z")
    token_rows = (
        token_rows.astype(f32) + jnp.sum(update[:, :3].astype(f32), axis=0)
    ).astype(bf16)
    returned = update[:, 3, :144].reshape(GROUPS, 2, 72).transpose(2, 1, 0)
    next_vector = returned.reshape(2, SEQ, 3, 2, 32)
    return (
        token_rows,
        jnp.stack([state0, state1]),
        jnp.stack([value0, value1]),
        next_vector,
    )


def solution(mesh):
    grid = Mesh(mesh.devices.reshape(ZN, YN, DN), ("z", "y", "dp"))
    tp = ("z", "y")
    return jax.shard_map(
        body,
        mesh=grid,
        in_specs=(
            P(tp, "dp"),
            P("dp"),
            P(None, "dp"),
            P(None, "dp", tp),
            P(None, "dp", tp),
            P(None, "dp", None, tp),
            P(None, "dp", None),
            P(None, tp),
            P(None, tp),
            P(None, None, tp),
            P(None, None, None, tp),
            P(None, tp, "dp"),
            P(None, "dp", tp, None, None),
            P(None, "dp", None, tp),
            P(None, "dp", None, None, tp),
        ),
        out_specs=(
            P(tp, "dp"),
            P(None, "dp", tp, None, None),
            P(None, "dp", None, tp),
            P(None, "dp", None, None, tp),
        ),
        check_vma=False,
    )
```

time: 260 us -> 213 us (0.82)
  blocking collectives: 96.7 us -> 12.5 us
  starting transfers between devices: 41.6 us -> 63.6 us
  waiting for transfers between devices: 77.5 us -> 93.3 us
    all_to_all x5 -> x1, blocking collectives: 96.7 us -> 12.5 us  [exchange(): return lax.all_to_all(pieces, axis, 0, 0, tiled=True)]
    all_to_all x5 -> x10, starting transfers between devices: 41.6 us -> 63.6 us  [exchange(): return lax.all_to_all(pieces, axis, 0, 0, tiled=True)]
    all_to_all x5 -> x10, waiting for transfers between devices: 77.5 us -> 93.3 us  [exchange(): return lax.all_to_all(pieces, axis, 0, 0, tiled=True)]
    unnamed x44 -> x31, local copies, waits for them, and re-layouts: 8.33 us -> 0.85 us
    reshape x10 -> x29, local copies, waits for them, and re-layouts: 0.87 us -> 7.87 us  [the longest x1 3.61 us: body(): returned = jnp.stack([vector0, vector1]).reshape(72, ZN, YN, 2)]
    slice x13 -> x25, local copies, waits for them, and re-layouts: 7.46 us -> 2.79 us  [the longest x3 1.93 us: mid(): vhist[layer]]
    concatenate x0 -> x6, other arithmetic: none -> 3.06 us  [the longest x2 1.47 us: project(): return jnp.concatenate(parts, axis=2)]
    another operation x6 -> x7, local copies, waits for them, and re-layouts: 3.53 us -> 0.55 us  [the longest x2 0.25 us: body(): plane[:, :, 7, :176].reshape(YN, ZN, 2, 88).transpose(3, 1, 0, 2)]
  transfers between devices with their start and end apart: 5 -> 10, of which waited for: 5 -> 10; matrix products, arithmetic and copies ran while one was open for 6% -> 7% of each run, Pallas kernels for 0% -> 0%
where the time goes in v1:
time: 213 us; the launch traced here: 212 us
  waiting for transfers between devices  93.3 us (44%)
  starting transfers between devices  63.6 us (30%)
  local copies, waits for them, and re-layouts  27.5 us (13%)
  blocking collectives  12.5 us (6%)
  other arithmetic  7.24 us (3%)
  matrix products  6.3 us (3%)
    all_to_all x10, waiting for transfers between devices, exchange(): return lax.all_to_all(pieces, axis, 0, 0, tiled=True)  93.3 us
    all_to_all x10, starting transfers between devices, exchange(): return lax.all_to_all(pieces, axis, 0, 0, tiled=True)  63.6 us
    all_to_all x1, blocking collectives, exchange(): return lax.all_to_all(pieces, axis, 0, 0, tiled=True)  12.5 us
    broadcast_in_dim x5, local copies, waits for them, and re-layouts, copies(): return jnp.broadcast_to(value[None], (peers, *value.shape))  4.48 us
  transfers between devices with their start and end apart: 10, of which 10 were waited for; matrix products, arithmetic and copies ran while one was open for 7% of the time, Pallas kernels for 0%

profile of v1, /device:TPU:1, one launch (start us, length us, event | category | flops | bytes accessed | tf_op | source)
XLA Modules:
  0.0 212.1 jit_solution(1212963030755509982)
XLA Ops:
  5.4 15.7 %all-to-all-start = ((bf16[16,12,512]{2,1,0:T(8,128)(2,1)}), bf16[16,12,512]{2,1,0:T(8,128)(2,1)S(1)}, u32[]{:S(2)}, u32[]{:S(2)}) async-start(bf16[16,12,512]{2,1,0:T(8,128)(2,1)} %fusion.22), calls=%async_computation | async-start | bytes 524288 | tf_op jit(solution)/shard_map/all_to_all | solution.py:24
  21.4 13.6 %all-to-all-done = bf16[16,12,512]{2,1,0:T(8,128)(2,1)S(1)} async-done(((bf16[16,12,512]{2,1,0:T(8,128)(2,1)}), bf16[16,12,512]{2,1,0:T(8,128)(2,1)S(1)}, u32[]{:S(2)}, u32[]{:S(2)}) %all-to-all-start) | async-done | bytes 196640 | tf_op jit(solution)/shard_map/all_to_all | solution.py:24
  35.9 4.2 %all-to-all-start.1 = ((bf16[4,16,8,512]{3,1,2,0:T(8,128)(2,1)}), bf16[4,16,8,512]{3,1,2,0:T(8,128)(2,1)S(1)}, u32[]{:S(2)}, u32[]{:S(2)}) async-start(bf16[4,16,8,512]{3,1,2,0:T(8,128)(2,1)} %broadcast_in_dim.89), calls=%async_computation.1 | async-start | bytes 1048576 | tf_op jit(solution)/shard_map/all_to_all | solution.py:24
  40.2 6.8 %all-to-all-done.1 = bf16[4,16,8,512]{3,1,2,0:T(8,128)(2,1)S(1)} async-done(((bf16[4,16,8,512]{3,1,2,0:T(8,128)(2,1)}), bf16[4,16,8,512]{3,1,2,0:T(8,128)(2,1)S(1)}, u32[]{:S(2)}, u32[]{:S(2)}) %all-to-all-start.1) | async-done | bytes 524320 | tf_op jit(solution)/shard_map/all_to_all | solution.py:24
  49.9 11.3 %all-to-all-start.2 = ((bf16[8,24,640]{2,1,0:T(8,128)(2,1)}), bf16[8,24,640]{2,1,0:T(8,128)(2,1)S(1)}, u32[]{:S(2)}, u32[]{:S(2)}) async-start(bf16[8,24,640]{2,1,0:T(8,128)(2,1)} %pad_maximum_fusion.3), calls=%async_computation.2 | async-start | bytes 491520 | tf_op jit(solution)/shard_map/all_to_all | solution.py:24
  64.5 3.1 %all-to-all-done.2 = bf16[8,24,640]{2,1,0:T(8,128)(2,1)S(1)} async-done(((bf16[8,24,640]{2,1,0:T(8,128)(2,1)}), bf16[8,24,640]{2,1,0:T(8,128)(2,1)S(1)}, u32[]{:S(2)}, u32[]{:S(2)}) %all-to-all-start.2) | async-done | bytes 245792 | tf_op jit(solution)/shard_map/all_to_all | solution.py:24
  68.4 3.5 %all-to-all-start.4 = ((bf16[4,128,512]{2,1,0:T(8,128)(2,1)}), bf16[4,128,512]{2,1,0:T(8,128)(2,1)S(1)}, u32[]{:S(2)}, u32[]{:S(2)}) async-start(bf16[4,128,512]{2,1,0:T(8,128)(2,1)} %broadcast_in_dim.98), calls=%async_computation.4 | async-start | bytes 1048576 | tf_op jit(solution)/shard_map/all_to_all | solution.py:24
  74.5 5.6 %all-to-all-done.4 = bf16[4,128,512]{2,1,0:T(8,128)(2,1)S(1)} async-done(((bf16[4,128,512]{2,1,0:T(8,128)(2,1)}), bf16[4,128,512]{2,1,0:T(8,128)(2,1)S(1)}, u32[]{:S(2)}, u32[]{:S(2)}) %all-to-all-start.4) | async-done | bytes 524320 | tf_op jit(solution)/shard_map/all_to_all | solution.py:24
  80.1 12.5 %all_to_all.55 = bf16[32,8,128]{2,1,0:T(8,128)(2,1)S(1)} all-to-all(bf16[32,8,128]{2,1,0:T(8,128)(2,1)S(1)} %bitcast.228), channel_id=1, replica_groups=mesh['z'=16,'y'=4,'dp'=8] {'y','dp'}, dimensions={0} | all-to-all | bytes 131072 | tf_op jit(solution)/shard_map/all_to_all | solution.py:24
  93.5 6.8 %all-to-all-start.5 = ((bf16[16,4,512]{2,1,0:T(4,128)(2,1)}), bf16[16,4,512]{2,1,0:T(4,128)(2,1)S(1)}, u32[]{:S(2)}, u32[]{:S(2)}) async-start(bf16[16,4,512]{2,1,0:T(4,128)(2,1)} %reshape.539), calls=%async_computation.5 | async-start | bytes 131072 | tf_op jit(solution)/shard_map/all_to_all | solution.py:24
  100.5 11.4 %all-to-all-done.5 = bf16[16,4,512]{2,1,0:T(4,128)(2,1)S(1)} async-done(((bf16[16,4,512]{2,1,0:T(4,128)(2,1)}), bf16[16,4,512]{2,1,0:T(4,128)(2,1)S(1)}, u32[]{:S(2)}, u32[]{:S(2)}) %all-to-all-start.5) | async-done | bytes 65568 | tf_op jit(solution)/shard_map/all_to_all | solution.py:24
  112.6 4.0 %all-to-all-start.6 = ((bf16[16,4,512]{2,1,0:T(4,128)(2,1)}), bf16[16,4,512]{2,1,0:T(4,128)(2,1)S(1)}, u32[]{:S(2)}, u32[]{:S(2)}) async-start(bf16[16,4,512]{2,1,0:T(4,128)(2,1)} %broadcast_in_dim.99), calls=%async_computation.6 | async-start | bytes 131072 | tf_op jit(solution)/shard_map/all_to_all | solution.py:24
  116.7 11.4 %all-to-all-done.6 = bf16[16,4,512]{2,1,0:T(4,128)(2,1)S(1)} async-done(((bf16[16,4,512]{2,1,0:T(4,128)(2,1)}), bf16[16,4,512]{2,1,0:T(4,128)(2,1)S(1)}, u32[]{:S(2)}, u32[]{:S(2)}) %all-to-all-start.6) | async-done | bytes 65568 | tf_op jit(solution)/shard_map/all_to_all | solution.py:24
  128.1 1.4 broadcast_in_dim.100
  129.5 3.6 %all-to-all-start.7 = ((bf16[4,448,512]{2,1,0:T(8,128)(2,1)}), bf16[4,448,512]{2,1,0:T(8,128)(2,1)S(1)}, u32[]{:S(2)}, u32[]{:S(2)}) async-start(bf16[4,448,512]{2,1,0:T(8,128)(2,1)} %broadcast_in_dim.100), calls=%async_computation.7 | async-start | bytes 3670016 | tf_op jit(solution)/shard_map/all_to_all | solution.py:24
  137.5 16.2 %all-to-all-done.7 = bf16[4,448,512]{2,1,0:T(8,128)(2,1)S(1)} async-done(((bf16[4,448,512]{2,1,0:T(8,128)(2,1)}), bf16[4,448,512]{2,1,0:T(8,128)(2,1)S(1)}, u32[]{:S(2)}, u32[]{:S(2)}) %all-to-all-start.7) | async-done | bytes 1835040 | tf_op jit(solution)/shard_map/all_to_all | solution.py:24
  156.0 7.3 %all-to-all-start.8 = ((bf16[32,8,640]{2,1,0:T(8,128)(2,1)}), bf16[32,8,640]{2,1,0:T(8,128)(2,1)S(1)}, u32[]{:S(2)}, u32[]{:S(2)}) async-start(bf16[32,8,640]{2,1,0:T(8,128)(2,1)} %bitcast.49), calls=%async_computation.8 | async-start | bytes 655360 | tf_op jit(solution)/shard_map/all_to_all | solution.py:24
  164.8 8.1 %all-to-all-done.8 = bf16[32,8,640]{2,1,0:T(8,128)(2,1)S(1)} async-done(((bf16[32,8,640]{2,1,0:T(8,128)(2,1)}), bf16[32,8,640]{2,1,0:T(8,128)(2,1)S(1)}, u32[]{:S(2)}, u32[]{:S(2)}) %all-to-all-start.8) | async-done | bytes 327712 | tf_op jit(solution)/shard_map/all_to_all | solution.py:24
  174.6 3.6 %reshape.564 = bf16[72,16,4,2]{3,2,1,0:T(4,128)(2,1)} reshape(bf16[2,6,3,256]{3,2,1,0:T(4,128)(2,1)S(1)} %pad_maximum_fusion.9) | data formatting | bytes 36864 | tf_op jit(solution)/shard_map/reshape | solution.py:225
  178.2 1.9 constant_dynamic-slice_fusion
  183.2 3.7 %all-to-all-start.9 = ((bf16[32,8,128]{2,1,0:T(8,128)(2,1)}), bf16[32,8,128]{2,1,0:T(8,128)(2,1)S(1)}, u32[]{:S(2)}, u32[]{:S(2)}) async-start(bf16[32,8,128]{2,1,0:T(8,128)(2,1)} %bitcast.66), calls=%async_computation.9 | async-start | bytes 131072 | tf_op jit(solution)/shard_map/all_to_all | solution.py:24
  187.6 6.7 %all-to-all-done.9 = bf16[32,8,128]{2,1,0:T(8,128)(2,1)S(1)} async-done(((bf16[32,8,128]{2,1,0:T(8,128)(2,1)}), bf16[32,8,128]{2,1,0:T(8,128)(2,1)S(1)}, u32[]{:S(2)}, u32[]{:S(2)}) %all-to-all-start.9) | async-done | bytes 65568 | tf_op jit(solution)/shard_map/all_to_all | solution.py:24
  195.3 3.5 %all-to-all-start.10 = ((bf16[16,4,512]{2,1,0:T(4,128)(2,1)}), bf16[16,4,512]{2,1,0:T(4,128)(2,1)S(1)}, u32[]{:S(2)}, u32[]{:S(2)}) async-start(bf16[16,4,512]{2,1,0:T(4,128)(2,1)} %fusion.35), calls=%async_computation.10 | async-start | bytes 131072 | tf_op jit(solution)/shard_map/all_to_all | solution.py:24
  200.1 10.4 %all-to-all-done.10 = bf16[16,4,512]{2,1,0:T(4,128)(2,1)S(1)} async-done(((bf16[16,4,512]{2,1,0:T(4,128)(2,1)}), bf16[16,4,512]{2,1,0:T(4,128)(2,1)S(1)}, u32[]{:S(2)}, u32[]{:S(2)}) %all-to-all-start.10) | async-done | bytes 65568 | tf_op jit(solution)/shard_map/all_to_all | solution.py:24
  (221 shorter events, 34.2 us)
Async XLA Ops:
  0.6 20.5 %copy-start.9 = (s32[6]{0:T(128)S(1)}, s32[6]{0:T(128)}, u32[]{:S(2)}) copy-start(s32[6]{0:T(128)} %param.16) | copy-start | bytes 76
  0.6 20.6 %copy-start.7 = (bf16[2,4,128]{2,1,0:T(4,128)(2,1)S(1)}, bf16[2,4,128]{2,1,0:T(4,128)(2,1)}, u32[]{:S(2)}) copy-start(bf16[2,4,128]{2,1,0:T(4,128)(2,1)} %param.24) | copy-start | bytes 6148
  0.7 20.6 %copy-start.10 = (f32[2,2]{1,0:T(2,128)S(1)}, f32[2,2]{1,0:T(2,128)}, u32[]{:S(2)}) copy-start(f32[2,2]{1,0:T(2,128)} %param.23) | copy-start | bytes 52
  0.7 20.6 %copy-start.11 = (f32[2,2]{1,0:T(2,128)S(1)}, f32[2,2]{1,0:T(2,128)}, u32[]{:S(2)}) copy-start(f32[2,2]{1,0:T(2,128)} %param.22) | copy-start | bytes 52
  0.7 20.6 %copy-start.8 = (f32[2,512]{1,0:T(2,128)S(1)}, f32[2,512]{1,0:T(2,128)}, u32[]{:S(2)}) copy-start(f32[2,512]{1,0:T(2,128)} %param.17) | copy-start | bytes 12292
  0.7 20.7 %copy-start.5 = (bf16[2,6,3,128]{3,0,2,1:T(2,128)(2,1)S(1)}, bf16[2,6,3,128]{3,0,2,1:T(2,128)(2,1)}, u32[]{:S(2)}) copy-start(bf16[2,6,3,128]{3,0,2,1:T(2,128)(2,1)} %param.28) | copy-start | bytes 27652
  3.8 36.4 %copy-start.4 = (bf16[2,128,512]{2,1,0:T(8,128)(2,1)S(1)}, bf16[2,128,512]{2,1,0:T(8,128)(2,1)}, u32[]{:S(2)}) copy-start(bf16[2,128,512]{2,1,0:T(8,128)(2,1)} %param.26) | copy-start | bytes 786436
  5.4 29.5 %all-to-all-start = ((bf16[16,12,512]{2,1,0:T(8,128)(2,1)}), bf16[16,12,512]{2,1,0:T(8,128)(2,1)S(1)}, u32[]{:S(2)}, u32[]{:S(2)}) async-start(bf16[16,12,512]{2,1,0:T(8,128)(2,1)} %fusion.22), calls=%async_computation | async-start | bytes 524288 | tf_op jit(solution)/shard_map/all_to_all | solution.py:24
  35.9 11.1 %all-to-all-start.1 = ((bf16[4,16,8,512]{3,1,2,0:T(8,128)(2,1)}), bf16[4,16,8,512]{3,1,2,0:T(8,128)(2,1)S(1)}, u32[]{:S(2)}, u32[]{:S(2)}) async-start(bf16[4,16,8,512]{3,1,2,0:T(8,128)(2,1)} %broadcast_in_dim.89), calls=%async_computation.1 | async-start | bytes 1048576 | tf_op jit(solution)/shard_map/all_to_all | solution.py:24
  40.1 8.2 %copy-start.3 = (bf16[2,512,128]{2,1,0:T(8,128)(2,1)S(1)}, bf16[2,512,128]{2,1,0:T(8,128)(2,1)}, u32[]{:S(2)}) copy-start(bf16[2,512,128]{2,1,0:T(8,128)(2,1)} %param.19) | copy-start | bytes 786436
  47.3 1.7 copy-start.12
  49.9 17.6 %all-to-all-start.2 = ((bf16[8,24,640]{2,1,0:T(8,128)(2,1)}), bf16[8,24,640]{2,1,0:T(8,128)(2,1)S(1)}, u32[]{:S(2)}, u32[]{:S(2)}) async-start(bf16[8,24,640]{2,1,0:T(8,128)(2,1)} %pad_maximum_fusion.3), calls=%async_computation.2 | async-start | bytes 491520 | tf_op jit(solution)/shard_map/all_to_all | solution.py:24
  64.5 9.2 %copy-start = (f32[2,6,2,64,128]{4,3,2,1,0:T(8,128)S(1)}, f32[2,6,2,64,128]{4,3,2,1,0:T(8,128)}, u32[]{:S(2)}) copy-start(f32[2,6,2,64,128]{4,3,2,1,0:T(8,128)} %param.27) | copy-start | bytes 2359300
  68.4 11.7 %all-to-all-start.4 = ((bf16[4,128,512]{2,1,0:T(8,128)(2,1)}), bf16[4,128,512]{2,1,0:T(8,128)(2,1)S(1)}, u32[]{:S(2)}, u32[]{:S(2)}) async-start(bf16[4,128,512]{2,1,0:T(8,128)(2,1)} %broadcast_in_dim.98), calls=%async_computation.4 | async-start | bytes 1048576 | tf_op jit(solution)/shard_map/all_to_all | solution.py:24
  72.3 28.0 %slice-start.1 = ((bf16[2,512,128]{2,1,0:T(8,128)(2,1)}), bf16[1,512,128]{2,1,0:T(8,128)(2,1)S(1)}, s32[]{:S(2)}) async-start(bf16[2,512,128]{2,1,0:T(8,128)(2,1)} %param.19), calls=%async_computation.12 | async-start | bytes 262144 | tf_op jit(solution)/shard_map/slice | solution.py:152
  72.3 28.1 %slice-start = ((bf16[2,512,128]{2,1,0:T(8,128)(2,1)}), bf16[1,512,128]{2,1,0:T(8,128)(2,1)S(1)}, s32[]{:S(2)}) async-start(bf16[2,512,128]{2,1,0:T(8,128)(2,1)} %param.18), calls=%async_computation.11 | async-start | bytes 262144 | tf_op jit(solution)/shard_map/slice | solution.py:151
  73.1 38.9 %copy-start.6 = (bf16[3,512]{1,0:T(4,128)(2,1)S(1)}, bf16[3,512]{1,0:T(4,128)(2,1)}, u32[]{:S(2)}) copy-start(bf16[3,512]{1,0:T(4,128)(2,1)} %param.15) | copy-start | bytes 9220
  93.5 18.4 %all-to-all-start.5 = ((bf16[16,4,512]{2,1,0:T(4,128)(2,1)}), bf16[16,4,512]{2,1,0:T(4,128)(2,1)S(1)}, u32[]{:S(2)}, u32[]{:S(2)}) async-start(bf16[16,4,512]{2,1,0:T(4,128)(2,1)} %reshape.539), calls=%async_computation.5 | async-start | bytes 131072 | tf_op jit(solution)/shard_map/all_to_all | solution.py:24
  112.6 15.5 %all-to-all-start.6 = ((bf16[16,4,512]{2,1,0:T(4,128)(2,1)}), bf16[16,4,512]{2,1,0:T(4,128)(2,1)S(1)}, u32[]{:S(2)}, u32[]{:S(2)}) async-start(bf16[16,4,512]{2,1,0:T(4,128)(2,1)} %broadcast_in_dim.99), calls=%async_computation.6 | async-start | bytes 131072 | tf_op jit(solution)/shard_map/all_to_all | solution.py:24
  129.5 24.2 %all-to-all-start.7 = ((bf16[4,448,512]{2,1,0:T(8,128)(2,1)}), bf16[4,448,512]{2,1,0:T(8,128)(2,1)S(1)}, u32[]{:S(2)}, u32[]{:S(2)}) async-start(bf16[4,448,512]{2,1,0:T(8,128)(2,1)} %broadcast_in_dim.100), calls=%async_computation.7 | async-start | bytes 3670016 | tf_op jit(solution)/shard_map/all_to_all | solution.py:24
  156.0 17.0 %all-to-all-start.8 = ((bf16[32,8,640]{2,1,0:T(8,128)(2,1)}), bf16[32,8,640]{2,1,0:T(8,128)(2,1)S(1)}, u32[]{:S(2)}, u32[]{:S(2)}) async-start(bf16[32,8,640]{2,1,0:T(8,128)(2,1)} %bitcast.49), calls=%async_computation.8 | async-start | bytes 655360 | tf_op jit(solution)/shard_map/all_to_all | solution.py:24
  181.0 18.1 %copy-start.1 = (f32[1,6,2,64,128]{4,3,2,1,0:T(8,128)S(1)}, f32[1,6,2,64,128]{4,3,2,1,0:T(8,128)}, u32[]{:S(2)}) copy-start(f32[1,6,2,64,128]{4,3,2,1,0:T(8,128)} %fusion.1) | copy-start | bytes 1179652
  183.2 11.2 %all-to-all-start.9 = ((bf16[32,8,128]{2,1,0:T(8,128)(2,1)}), bf16[32,8,128]{2,1,0:T(8,128)(2,1)S(1)}, u32[]{:S(2)}, u32[]{:S(2)}) async-start(bf16[32,8,128]{2,1,0:T(8,128)(2,1)} %bitcast.66), calls=%async_computation.9 | async-start | bytes 131072 | tf_op jit(solution)/shard_map/all_to_all | solution.py:24
  195.3 15.2 %all-to-all-start.10 = ((bf16[16,4,512]{2,1,0:T(4,128)(2,1)}), bf16[16,4,512]{2,1,0:T(4,128)(2,1)S(1)}, u32[]{:S(2)}, u32[]{:S(2)}) async-start(bf16[16,4,512]{2,1,0:T(4,128)(2,1)} %fusion.35), calls=%async_computation.10 | async-start | bytes 131072 | tf_op jit(solution)/shard_map/all_to_all | solution.py:24
  (1 other events, 1.6 us)

commit v2 on v1

--- a/solution.py
+++ b/solution.py
@@ -1,6 +1,10 @@
+import functools
+
 import jax
 import jax.numpy as jnp
 from jax import lax
+from jax.experimental import pallas as pl
+from jax.experimental.pallas import tpu as pltpu
 from jax.sharding import Mesh, PartitionSpec as P
 
 D = 4096
@@ -38,21 +42,126 @@
     return (jax.nn.silu(summed), padded)
 
 
-def project(rows, gain, gate_w, value_w, vector_w, step_w, square_lane):
+def one_hot(rows, cols, target):
+    row = lax.broadcasted_iota(jnp.int32, (rows, cols), 0)
+    col = lax.broadcasted_iota(jnp.int32, (rows, cols), 1)
+    return jnp.where(row == target(col), 1.0, 0.0).astype(bf16)
+
+
+def mm(a, b):
+    return lax.dot_general(a, b, (((1,), (0,)), ((), ())), preferred_element_type=f32)
+
+
+def mm_t(a, b):
+    return lax.dot_general(a, b, (((1,), (1,)), ((), ())), preferred_element_type=f32)
+
+
+def normed_rows(rows, gain):
     widened = rows.astype(f32)
     squares = jnp.sum(widened * widened, axis=1, keepdims=True)
-    normed = (widened * gain[None]).astype(bf16)
-    gate = jnp.einsum("td,ydc->tyc", normed, gate_w, preferred_element_type=f32)
-    value = jnp.einsum("td,ydc->tyc", normed, value_w, preferred_element_type=f32)
-    vector = jnp.einsum("td,cd->tc", normed, vector_w, preferred_element_type=f32)
-    step = jnp.dot(normed, step_w, preferred_element_type=f32)
-    lane = jnp.arange(HEADS, dtype=jnp.int32)[None]
-    extra = jnp.where(lane == square_lane, squares, step)
-    width = gate_w.shape[0]
-    shared = jnp.concatenate([vector, extra], axis=1).astype(bf16)
-    parts = [gate.astype(bf16), value.astype(bf16)]
-    parts.append(jnp.broadcast_to(shared[:, None], (rows.shape[0], width, shared.shape[1])))
-    return jnp.concatenate(parts, axis=2)
+    return (widened * gain).astype(bf16), squares
+
+
+def step_lanes(at_ref, normed, squares, step_w):
+    step = mm(normed, step_w)
+    lane = lax.broadcasted_iota(jnp.int32, step.shape, 1)
+    return jnp.where(lane == at_ref[2], squares, step)
+
+
+def first_projection(at_ref, plane_ref, gain_ref, gate_ref, value_ref, step_ref, out_ref):
+    plane = plane_ref[...]
+
+    def token_source(col):
+        i = col % 8
+        return jnp.where(i < 3, 12 * ((col // 8) % ZN) + 3 * (col // 128) + i, -1)
+
+    def vector_source(col):
+        j = col % 8 - 3
+        n = 8 * ((col // 8) % ZN) + 2 * (col // 128) + j % 2
+        return jnp.where((j >= 0) & (j < 4), 128 * (j // 2) + n, -1)
+
+    rows = mm(one_hot(192, 512, token_source), plane).astype(bf16)
+    vector_w = mm(one_hot(256, 512, vector_source), plane).astype(bf16)
+    normed, squares = normed_rows(rows, gain_ref[0:1])
+    parts = [
+        mm(normed, gate_ref[0]),
+        mm(normed, value_ref[0]),
+        mm_t(normed, vector_w),
+        step_lanes(at_ref, normed, squares, step_ref[0]),
+    ]
+    at = 0
+    for part in parts:
+        width = part.shape[1]
+        out_ref[:, :, at : at + width] = part.astype(bf16).reshape(DN, 24, width)
+        at += width
+
+
+def second_projection(at_ref, rows_ref, gain_ref, step_ref, w0, w1, w2, w3, out_ref):
+    y = at_ref[1]
+    normed, squares = normed_rows(rows_ref[...], gain_ref[1:2])
+    pieces = [w0, w1, w2, w3]
+
+    def source(col):
+        j = col % 4
+        n = 8 * ((col // 4) % ZN) + 2 * ((y - col // 64) % YN) + j % 2
+        return 128 * (j // 2) + n
+
+    stacked = jnp.concatenate([w[384:448] for w in pieces], axis=0)
+    vector_w = mm(one_hot(256, 256, source), stacked).astype(bf16)
+    vector = mm_t(normed, vector_w).astype(bf16)
+    extra = step_lanes(at_ref, normed, squares, step_ref[0]).astype(bf16)
+    for k, w in enumerate(pieces):
+        to = (y - k) % YN
+        for n in range(2):
+            total = jnp.zeros((64, 128), f32)
+            for b in range(4):
+                total += mm(
+                    normed[:, 128 * b : 128 * b + 128],
+                    w[128 * n : 128 * n + 128, 128 * b : 128 * b + 128],
+                )
+            out_ref[to, :, 128 * n : 128 * n + 128] = total.astype(bf16)
+        out_ref[to, :, 256:512] = vector
+        out_ref[to, :, 512:640] = extra
+
+
+def out_projection(at_ref, mixed_ref, w0, w1, w2, w3, *rest, first_row):
+    y = at_ref[1]
+    total = jnp.zeros((64, 512), f32)
+    for k, w in enumerate([w0, w1, w2, w3]):
+        total += mm(mixed_ref[(y - k) % YN], w[first_row : first_row + 128])
+    if len(rest) == 1:
+        rest[0][...] = total.astype(bf16)
+        return
+    returned_ref, out_ref = rest
+    slot = one_hot(64, ZN, lambda col: 4 * col + 3)
+    halves = []
+    for nl in range(2):
+        row = lax.broadcasted_iota(jnp.int32, (ZN, 128), 0)
+        col = lax.broadcasted_iota(jnp.int32, (ZN, 128), 1)
+        chosen = jnp.where(col == 8 * row + 2 * y + nl, 1.0, 0.0).astype(bf16)
+        halves.append(mm_t(chosen, returned_ref[...]).astype(bf16))
+    tail = jnp.concatenate(halves, axis=1)
+    out_ref[:, 256:512] = total[:, 256:512].astype(bf16)
+    out_ref[:, 0:256] = (total[:, 0:256] + mm(slot, tail)).astype(bf16)
+
+
+def call(kernel, shape, *args):
+    space = [pl.BlockSpec(memory_space=pltpu.SMEM)]
+    space += [pl.BlockSpec(memory_space=pltpu.VMEM)] * (len(args) - 1)
+    return pl.pallas_call(
+        kernel,
+        out_shape=jax.ShapeDtypeStruct(shape, bf16),
+        in_specs=space,
+        out_specs=pl.BlockSpec(memory_space=pltpu.VMEM),
+        compiler_params=pltpu.CompilerParams(vmem_limit_bytes=8 << 20),
+    )(*args)
+
+
+def around_y(value):
+    pieces = [value]
+    for k in range(1, YN):
+        pieces.append(lax.ppermute(value, "y", [(i, (i + k) % YN) for i in range(YN)]))
+    return pieces
 
 
 def middle(total, head_start, square_lane, live_mask, picker, bias, rate, history, taps, vhist, vtaps, state):
@@ -139,29 +248,11 @@
     first = jnp.concatenate(
         [copies(tokens, ZN), vector_cols[:, :4], small, vector_cols[:, 4:]], axis=1
     )
+    at = jnp.stack([z, y, square_lane]).astype(jnp.int32)
     first = exchange(first, "z")
-    own_out = exchange(copies(out_weight[0], YN), "y")
+    own_out = around_y(out_weight[0])
     plane = exchange(copies(first[:, :8], YN), "y")
 
-    def lanes(w):
-        return w.reshape(4, 128, 128).transpose(1, 0, 2).reshape(128, 512)
-
-    later = jnp.concatenate(
-        [
-            lanes(gate_weight[1]),
-            lanes(value_weight[1]),
-            out_weight[1],
-            first[:, 8:].reshape(64, 512),
-        ],
-        axis=0,
-    )
-    later = exchange(copies(later, YN), "y")
-
-    whole = plane[:, :, :3].transpose(1, 0, 2, 3).reshape(192, 512)
-    vector_w = [
-        plane[:, :, 3:7].reshape(YN, ZN, 2, 2, 512).transpose(2, 1, 0, 3, 4).reshape(256, 512),
-        later[:, 384:].reshape(YN, ZN, 2, 2, 512).transpose(2, 1, 0, 3, 4).reshape(256, 512),
-    ]
     small = plane[:, :, 7, :176].reshape(YN, ZN, 2, 88).transpose(3, 1, 0, 2).reshape(88, 128)
     vhist = small[:72].reshape(2, SEQ, 3, 256)
     vtaps = small[72:].reshape(2, CONV, 256)
@@ -182,55 +273,62 @@
             recurrent_state[layer],
         )
 
-    part = project(
-        whole,
-        norm_gain[0],
+    part = call(
+        first_projection,
+        (DN, 24, COLS),
+        at,
+        plane.reshape(512, 512),
+        norm_gain,
         gate_weight[:1],
         value_weight[:1],
-        vector_w[0],
-        step_weight[0],
-        square_lane,
-    )
-    part = exchange(part.reshape(DN, 24, COLS), "dp")
+        step_weight[:1],
+    )
+    part = exchange(part, "dp")
     total = jnp.sum(part.astype(f32), axis=0)
     mixed, state0, value0, vector0 = mid(total, 0)
     mixed = send_mixed(mixed)
-    update = jnp.einsum("ytc,ycf->tf", mixed, own_out, preferred_element_type=f32)
-    update = exchange(update.astype(bf16).reshape(ZN, 4, 512), "z")
+    update = call(
+        functools.partial(out_projection, first_row=0), (64, 512), at, mixed, *own_out
+    )
+
+    def lanes(w):
+        return w.reshape(4, 128, 128).transpose(1, 0, 2).reshape(128, 512)
+
+    later = jnp.concatenate(
+        [
+            lanes(gate_weight[1]),
+            lanes(value_weight[1]),
+            out_weight[1],
+            first[:, 8:].reshape(64, 512),
+        ],
+        axis=0,
+    )
+    update, later = lax.optimization_barrier((update, later))
+    update = exchange(update.reshape(ZN, 4, 512), "z")
+    later = around_y(later)
     update = jnp.sum(update.astype(f32), axis=0)[:3]
     token_rows = (tokens.astype(f32) + update).astype(bf16)
 
     quarter = exchange(copies(jnp.pad(token_rows, ((0, 1), (0, 0))), ZN), "z").reshape(64, 512)
-
-    def unlanes(w):
-        return w.reshape(YN, 128, 4, 128).transpose(0, 2, 1, 3).reshape(YN, 512, 128)
-
-    part = project(
-        quarter,
-        norm_gain[1],
-        unlanes(later[:, :128]),
-        unlanes(later[:, 128:256]),
-        vector_w[1],
-        step_weight[1],
-        square_lane,
-    )
-    part = part.reshape(DN, 8, YN, COLS).transpose(2, 0, 1, 3).reshape(YN * DN, 8, COLS)
-    part = exchange(part, ("y", "dp")).reshape(YN, DN, 8, COLS)
+    part = call(
+        second_projection, (YN, 64, COLS), at, quarter, norm_gain, step_weight[1:], *later
+    )
+    part = exchange(part.reshape(YN * DN, 8, COLS), ("y", "dp")).reshape(YN, DN, 8, COLS)
     total = jnp.sum(part.astype(f32), axis=1).reshape(YN, 2, 4, COLS)[:, :, :3]
     total = total.transpose(1, 0, 2, 3).reshape(24, COLS)
     mixed, state1, value1, vector1 = mid(total, 1)
+    mixed, vector1 = lax.optimization_barrier((mixed, vector1))
     mixed = send_mixed(mixed)
-    update = jnp.einsum("ytc,ycf->tf", mixed, later[:, 256:384], preferred_element_type=f32)
-    update = update.astype(bf16).reshape(ZN, 4, 512)
-    returned = jnp.stack([vector0, vector1]).reshape(72, ZN, YN, 2)
-    returned = lax.dynamic_index_in_dim(returned, y, 2, keepdims=False)
-    returned = returned.reshape(36, 2, ZN, 2).transpose(2, 3, 0, 1).reshape(ZN, 1, 144)
-    returned = jnp.pad(returned, ((0, 0), (0, 0), (0, 512 - 144)))
-    update = exchange(jnp.concatenate([update[:, :3], returned], axis=1), "z")
+    returned = jnp.stack([vector0, vector1]).reshape(72, 128)
+    returned = jnp.pad(returned, ((0, 56), (0, 0)))
+    update = call(
+        functools.partial(out_projection, first_row=256), (64, 512), at, mixed, *later, returned
+    )
+    update = exchange(update.reshape(ZN, 4, 512), "z")
     token_rows = (
         token_rows.astype(f32) + jnp.sum(update[:, :3].astype(f32), axis=0)
     ).astype(bf16)
-    returned = update[:, 3, :144].reshape(GROUPS, 2, 72).transpose(2, 1, 0)
+    returned = update[:, 3, :256].reshape(GROUPS, 2, 128)[:, :, :72].transpose(2, 1, 0)
     next_vector = returned.reshape(2, SEQ, 3, 2, 32)
     return (
         token_rows,

time: 213 us -> 196 us (0.920)
  waiting for transfers between devices: 93.3 us -> 55.9 us
  starting transfers between devices: 63.6 us -> 89.3 us
  blocking collectives: 12.5 us -> 0 us
  Pallas kernels: 0 us -> 5.46 us
  local copies, waits for them, and re-layouts: 27.5 us -> 31.9 us
  matrix products: 6.3 us -> 3.21 us
    all_to_all x10 -> x9, waiting for transfers between devices: 93.3 us -> 55.9 us  [exchange(): return lax.all_to_all(pieces, axis, 0, 0, tiled=True)]
    ppermute x0 -> x6, starting transfers between devices: none -> 20.4 us  [around_y(): lax.ppermute(value, 'y', [(i, (i + k) % YN) for i in range(YN)])]
    all_to_all x1 -> x0, blocking collectives: 12.5 us -> none  [exchange(): return lax.all_to_all(pieces, axis, 0, 0, tiled=True)]
    unnamed x31 -> x121, local copies, waits for them, and re-layouts: 0.85 us -> 11.3 us
    pallas_call x0 -> x4, Pallas kernels: none -> 5.46 us  [call(): pl.pallas_call(kernel, out_shape=jax.ShapeDtypeStruct(shape, bf16), in_sp...]
    all_to_all x10 -> x9, starting transfers between devices: 63.6 us -> 68.9 us  [exchange(): return lax.all_to_all(pieces, axis, 0, 0, tiled=True)]
    reshape x12 -> x5, local copies, waits for them, and re-layouts: 6.15 us -> 1.38 us  [the longest x2 1.31 us: body(): update = exchange(update.reshape(ZN, 4, 512), 'z')]
    broadcast_in_dim x5 -> x3, local copies, waits for them, and re-layouts: 4.48 us -> 1.52 us  [copies(): return jnp.broadcast_to(value[None], (peers, *value.shape))]
  transfers between devices with their start and end apart: 10 -> 15, of which waited for: 10 -> 9; matrix products, arithmetic and copies ran while one was open for 7% -> 13% of each run, Pallas kernels for 0% -> 1%
where the time goes in v2:
time: 196 us; the launch traced here: 195 us
  starting transfers between devices  89.3 us (46%)
  waiting for transfers between devices  55.9 us (29%)
  local copies, waits for them, and re-layouts  31.9 us (16%)
  other arithmetic  7.23 us (4%)
  Pallas kernels  5.46 us (3%)
  matrix products  3.21 us (2%)
    all_to_all x9, starting transfers between devices, exchange(): return lax.all_to_all(pieces, axis, 0, 0, tiled=True)  68.9 us
    all_to_all x9, waiting for transfers between devices, exchange(): return lax.all_to_all(pieces, axis, 0, 0, tiled=True)  55.9 us
    ppermute x6, starting transfers between devices, around_y(): lax.ppermute(value, 'y', [(i, (i + k) % YN) for i in range(YN)])  20.4 us
    unnamed x121, local copies, waits for them, and re-layouts  11.3 us
    pallas_call x4, Pallas kernels, call(): pl.pallas_call(kernel, out_shape=jax.ShapeDtypeStruct(shape, bf16), in_sp...  5.46 us
    convert_element_type x16, local copies, waits for them, and re-layouts, short_conv(): conv_taps[offset].astype(f32)  4.57 us
  transfers between devices with their start and end apart: 15, of which 9 were waited for; matrix products, arithmetic and copies ran while one was open for 13% of the time, Pallas kernels for 1%

profile of v2, /device:TPU:1, one launch (start us, length us, event | category | flops | bytes accessed | tf_op | source)
XLA Modules:
  0.0 194.6 jit_solution(7845482666880740029)
XLA Ops:
  1.7 4.2 %collective-permute-start = (bf16[128,512]{1,0:T(8,128)(2,1)S(1)}, bf16[128,512]{1,0:T(8,128)(2,1)S(1)}, u32[]{:S(2)}, u32[]{:S(2)}) collective-permute-start(bf16[128,512]{1,0:T(8,128)(2,1)S(1)} %get-tuple-element.55.w0), channel_id=1, source_target_pairs={{0,8},{8,16},{16,24},{24,0},{1,9},{9,17},{17,25},{25,1},{2,10},{10... | collective-permute-start | bytes 393224 | tf_op jit(solution)/shard_map/ppermute | solution.py:163
  5.8 4.5 %collective-permute-start.1 = (bf16[128,512]{1,0:T(8,128)(2,1)S(1)}, bf16[128,512]{1,0:T(8,128)(2,1)S(1)}, u32[]{:S(2)}, u32[]{:S(2)}) collective-permute-start(bf16[128,512]{1,0:T(8,128)(2,1)S(1)} %get-tuple-element.55.w0), channel_id=1, source_target_pairs={{0,16},{8,24},{16,0},{24,8},{1,17},{9,25},{17,1},{25,9},{2,18},{10... | collective-permute-start | bytes 393224 | tf_op jit(solution)/shard_map/ppermute | solution.py:163
  10.4 3.0 %collective-permute-start.2 = (bf16[128,512]{1,0:T(8,128)(2,1)S(1)}, bf16[128,512]{1,0:T(8,128)(2,1)S(1)}, u32[]{:S(2)}, u32[]{:S(2)}) collective-permute-start(bf16[128,512]{1,0:T(8,128)(2,1)S(1)} %get-tuple-element.55.w0), channel_id=1, source_target_pairs={{0,24},{8,0},{16,8},{24,16},{1,25},{9,1},{17,9},{25,17},{2,26},{10... | collective-permute-start | bytes 393224 | tf_op jit(solution)/shard_map/ppermute | solution.py:163
  15.5 15.0 %all-to-all-start = ((bf16[16,12,512]{2,1,0:T(8,128)(2,1)}), bf16[16,12,512]{2,1,0:T(8,128)(2,1)S(1)}, u32[]{:S(2)}, u32[]{:S(2)}) async-start(bf16[16,12,512]{2,1,0:T(8,128)(2,1)} %fusion.14), calls=%async_computation | async-start | bytes 524288 | tf_op jit(solution)/shard_map/all_to_all | solution.py:28
  34.0 9.3 %all-to-all-done = bf16[16,12,512]{2,1,0:T(8,128)(2,1)S(1)} async-done(((bf16[16,12,512]{2,1,0:T(8,128)(2,1)}), bf16[16,12,512]{2,1,0:T(8,128)(2,1)S(1)}, u32[]{:S(2)}, u32[]{:S(2)}) %all-to-all-start) | async-done | bytes 196640 | tf_op jit(solution)/shard_map/all_to_all | solution.py:28
  44.2 3.6 %all-to-all-start.1 = ((bf16[4,16,8,512]{3,1,2,0:T(8,128)(2,1)}), bf16[4,16,8,512]{3,1,2,0:T(8,128)(2,1)S(1)}, u32[]{:S(2)}, u32[]{:S(2)}) async-start(bf16[4,16,8,512]{3,1,2,0:T(8,128)(2,1)} %broadcast_in_dim.45), calls=%async_computation.1 | async-start | bytes 1048576 | tf_op jit(solution)/shard_map/all_to_all | solution.py:28
  49.1 5.7 %all-to-all-done.1 = bf16[4,16,8,512]{3,1,2,0:T(8,128)(2,1)S(1)} async-done(((bf16[4,16,8,512]{3,1,2,0:T(8,128)(2,1)}), bf16[4,16,8,512]{3,1,2,0:T(8,128)(2,1)S(1)}, u32[]{:S(2)}, u32[]{:S(2)}) %all-to-all-start.1) | async-done | bytes 524320 | tf_op jit(solution)/shard_map/all_to_all | solution.py:28
  57.6 12.3 %all-to-all-start.2 = ((bf16[8,24,640]{2,1,0:T(8,128)(2,1)}), bf16[8,24,640]{2,1,0:T(8,128)(2,1)S(1)}, u32[]{:S(2)}, u32[]{:S(2)}) async-start(bf16[8,24,640]{2,1,0:T(8,128)(2,1)} %shard_map.174), calls=%async_computation.2 | async-start | bytes 491520 | tf_op jit(solution)/shard_map/all_to_all | solution.py:28
  73.8 2.5 %all-to-all-done.2 = bf16[8,24,640]{2,1,0:T(8,128)(2,1)S(1)} async-done(((bf16[8,24,640]{2,1,0:T(8,128)(2,1)}), bf16[8,24,640]{2,1,0:T(8,128)(2,1)S(1)}, u32[]{:S(2)}, u32[]{:S(2)}) %all-to-all-start.2) | async-done | bytes 245792 | tf_op jit(solution)/shard_map/all_to_all | solution.py:28
  82.3 4.5 %all-to-all-start.3 = ((bf16[32,8,128]{2,1,0:T(8,128)(2,1)}), bf16[32,8,128]{2,1,0:T(8,128)(2,1)S(1)}, u32[]{:S(2)}, u32[]{:S(2)}) async-start(bf16[32,8,128]{2,1,0:T(8,128)(2,1)} %bitcast.27), calls=%async_computation.3 | async-start | bytes 131072 | tf_op jit(solution)/shard_map/all_to_all | solution.py:28
  86.9 7.4 %all-to-all-done.3 = bf16[32,8,128]{2,1,0:T(8,128)(2,1)S(1)} async-done(((bf16[32,8,128]{2,1,0:T(8,128)(2,1)}), bf16[32,8,128]{2,1,0:T(8,128)(2,1)S(1)}, u32[]{:S(2)}, u32[]{:S(2)}) %all-to-all-start.3) | async-done | bytes 65568 | tf_op jit(solution)/shard_map/all_to_all | solution.py:28
  95.7 6.3 %all-to-all-start.4 = ((bf16[16,4,512]{2,1,0:T(4,128)(2,1)}), bf16[16,4,512]{2,1,0:T(4,128)(2,1)S(1)}, u32[]{:S(2)}, u32[]{:S(2)}) async-start(bf16[16,4,512]{2,1,0:T(4,128)(2,1)} %reshape.407), calls=%async_computation.4 | async-start | bytes 131072 | tf_op jit(solution)/shard_map/all_to_all | solution.py:28
  102.0 2.2 %collective-permute-start.3 = (bf16[448,512]{1,0:T(8,128)(2,1)S(1)}, bf16[448,512]{1,0:T(8,128)(2,1)S(1)}, u32[]{:S(2)}, u32[]{:S(2)}) collective-permute-start(bf16[448,512]{1,0:T(8,128)(2,1)S(1)} %pad_maximum_fusion.1.w0), channel_id=1, source_target_pairs={{0,8},{8,16},{16,24},{24,0},{1,9},{9,17},{17,25},{25,1},{2,10},{10... | collective-permute-start | bytes 1376264 | tf_op jit(solution)/shard_map/ppermute | solution.py:163
  104.3 3.6 %collective-permute-start.4 = (bf16[448,512]{1,0:T(8,128)(2,1)S(1)}, bf16[448,512]{1,0:T(8,128)(2,1)S(1)}, u32[]{:S(2)}, u32[]{:S(2)}) collective-permute-start(bf16[448,512]{1,0:T(8,128)(2,1)S(1)} %pad_maximum_fusion.1.w0), channel_id=1, source_target_pairs={{0,16},{8,24},{16,0},{24,8},{1,17},{9,25},{17,1},{25,9},{2,18},{10... | collective-permute-start | bytes 1376264 | tf_op jit(solution)/shard_map/ppermute | solution.py:163
  107.9 2.9 %collective-permute-start.5 = (bf16[448,512]{1,0:T(8,128)(2,1)S(1)}, bf16[448,512]{1,0:T(8,128)(2,1)S(1)}, u32[]{:S(2)}, u32[]{:S(2)}) collective-permute-start(bf16[448,512]{1,0:T(8,128)(2,1)S(1)} %pad_maximum_fusion.1.w0), channel_id=1, source_target_pairs={{0,24},{8,0},{16,8},{24,16},{1,25},{9,1},{17,9},{25,17},{2,26},{10... | collective-permute-start | bytes 1376264 | tf_op jit(solution)/shard_map/ppermute | solution.py:163
  110.8 2.8 %all-to-all-done.4 = bf16[16,4,512]{2,1,0:T(4,128)(2,1)S(1)} async-done(((bf16[16,4,512]{2,1,0:T(4,128)(2,1)}), bf16[16,4,512]{2,1,0:T(4,128)(2,1)S(1)}, u32[]{:S(2)}, u32[]{:S(2)}) %all-to-all-start.4) | async-done | bytes 65568 | tf_op jit(solution)/shard_map/all_to_all | solution.py:28
  114.9 8.7 %all-to-all-start.5 = ((bf16[16,4,512]{2,1,0:T(4,128)(2,1)}), bf16[16,4,512]{2,1,0:T(4,128)(2,1)S(1)}, u32[]{:S(2)}, u32[]{:S(2)}) async-start(bf16[16,4,512]{2,1,0:T(4,128)(2,1)} %broadcast_in_dim.50), calls=%async_computation.5 | async-start | bytes 131072 | tf_op jit(solution)/shard_map/all_to_all | solution.py:28
  131.4 3.7 %all-to-all-done.5 = bf16[16,4,512]{2,1,0:T(4,128)(2,1)S(1)} async-done(((bf16[16,4,512]{2,1,0:T(4,128)(2,1)}), bf16[16,4,512]{2,1,0:T(4,128)(2,1)S(1)}, u32[]{:S(2)}, u32[]{:S(2)}) %all-to-all-start.5) | async-done | bytes 65568 | tf_op jit(solution)/shard_map/all_to_all | solution.py:28
  137.1 7.8 %all-to-all-start.6 = ((bf16[32,8,640]{2,1,0:T(8,128)(2,1)}), bf16[32,8,640]{2,1,0:T(8,128)(2,1)S(1)}, u32[]{:S(2)}, u32[]{:S(2)}) async-start(bf16[32,8,640]{2,1,0:T(8,128)(2,1)} %bitcast.36), calls=%async_computation.6 | async-start | bytes 655360 | tf_op jit(solution)/shard_map/all_to_all | solution.py:28
  146.9 7.6 %all-to-all-done.6 = bf16[32,8,640]{2,1,0:T(8,128)(2,1)S(1)} async-done(((bf16[32,8,640]{2,1,0:T(8,128)(2,1)}), bf16[32,8,640]{2,1,0:T(8,128)(2,1)S(1)}, u32[]{:S(2)}, u32[]{:S(2)}) %all-to-all-start.6) | async-done | bytes 327712 | tf_op jit(solution)/shard_map/all_to_all | solution.py:28
  161.8 3.9 %all-to-all-start.7 = ((bf16[32,8,128]{2,1,0:T(8,128)(2,1)}), bf16[32,8,128]{2,1,0:T(8,128)(2,1)S(1)}, u32[]{:S(2)}, u32[]{:S(2)}) async-start(bf16[32,8,128]{2,1,0:T(8,128)(2,1)} %bitcast.54), calls=%async_computation.7 | async-start | bytes 131072 | tf_op jit(solution)/shard_map/all_to_all | solution.py:28
  166.5 6.6 %all-to-all-done.7 = bf16[32,8,128]{2,1,0:T(8,128)(2,1)S(1)} async-done(((bf16[32,8,128]{2,1,0:T(8,128)(2,1)}), bf16[32,8,128]{2,1,0:T(8,128)(2,1)S(1)}, u32[]{:S(2)}, u32[]{:S(2)}) %all-to-all-start.7) | async-done | bytes 65568 | tf_op jit(solution)/shard_map/all_to_all | solution.py:28
  174.7 6.8 %all-to-all-start.8 = ((bf16[16,4,512]{2,1,0:T(4,128)(2,1)}), bf16[16,4,512]{2,1,0:T(4,128)(2,1)S(1)}, u32[]{:S(2)}, u32[]{:S(2)}) async-start(bf16[16,4,512]{2,1,0:T(4,128)(2,1)} %reshape.424), calls=%async_computation.8 | async-start | bytes 131072 | tf_op jit(solution)/shard_map/all_to_all | solution.py:28
  182.8 10.3 %all-to-all-done.8 = bf16[16,4,512]{2,1,0:T(4,128)(2,1)S(1)} async-done(((bf16[16,4,512]{2,1,0:T(4,128)(2,1)}), bf16[16,4,512]{2,1,0:T(4,128)(2,1)S(1)}, u32[]{:S(2)}, u32[]{:S(2)}) %all-to-all-start.8) | async-done | bytes 65568 | tf_op jit(solution)/shard_map/all_to_all | solution.py:28
  (285 shorter events, 47.8 us)
Async XLA Ops:
  0.6 12.7 %copy-start.43 = (bf16[2,4,2,32]{3,2,1,0:T(2,128)(2,1)S(1)}, bf16[2,4,2,32]{3,2,1,0:T(2,128)(2,1)}, u32[]{:S(2)}) copy-start(bf16[2,4,2,32]{3,2,1,0:T(2,128)(2,1)} %param.25) | copy-start | bytes 3076
  0.6 12.9 %copy-start.32 = (bf16[2,6,3,2,32]{4,3,2,1,0:T(2,128)(2,1)S(1)}, bf16[2,6,3,2,32]{4,3,2,1,0:T(2,128)(2,1)}, u32[]{:S(2)}) copy-start(bf16[2,6,3,2,32]{4,3,2,1,0:T(2,128)(2,1)} %param.29) | copy-start | bytes 13828
  1.7 12.2 %copy-start.6 = (bf16[2,512,2,32]{1,3,2,0:T(8,128)(2,1)S(1)}, bf16[2,512,2,32]{1,3,2,0:T(8,128)(2,1)}, u32[]{:S(2)}) copy-start(bf16[2,512,2,32]{1,3,2,0:T(8,128)(2,1)} %param.20) | copy-start | bytes 393220
  1.7 85.2 %collective-permute-start = (bf16[128,512]{1,0:T(8,128)(2,1)S(1)}, bf16[128,512]{1,0:T(8,128)(2,1)S(1)}, u32[]{:S(2)}, u32[]{:S(2)}) collective-permute-start(bf16[128,512]{1,0:T(8,128)(2,1)S(1)} %get-tuple-element.55.w0), channel_id=1, source_target_pairs={{0,8},{8,16},{16,24},{24,0},{1,9},{9,17},{17,25},{25,1},{2,10},{10... | collective-permute-start | bytes 393224 | tf_op jit(solution)/shard_map/ppermute | solution.py:163
  5.8 81.1 %collective-permute-start.1 = (bf16[128,512]{1,0:T(8,128)(2,1)S(1)}, bf16[128,512]{1,0:T(8,128)(2,1)S(1)}, u32[]{:S(2)}, u32[]{:S(2)}) collective-permute-start(bf16[128,512]{1,0:T(8,128)(2,1)S(1)} %get-tuple-element.55.w0), channel_id=1, source_target_pairs={{0,16},{8,24},{16,0},{24,8},{1,17},{9,25},{17,1},{25,9},{2,18},{10... | collective-permute-start | bytes 393224 | tf_op jit(solution)/shard_map/ppermute | solution.py:163
  10.4 76.6 %collective-permute-start.2 = (bf16[128,512]{1,0:T(8,128)(2,1)S(1)}, bf16[128,512]{1,0:T(8,128)(2,1)S(1)}, u32[]{:S(2)}, u32[]{:S(2)}) collective-permute-start(bf16[128,512]{1,0:T(8,128)(2,1)S(1)} %get-tuple-element.55.w0), channel_id=1, source_target_pairs={{0,24},{8,0},{16,8},{24,16},{1,25},{9,1},{17,9},{25,17},{2,26},{10... | collective-permute-start | bytes 393224 | tf_op jit(solution)/shard_map/ppermute | solution.py:163
  15.5 15.1 %copy-start.3 = (bf16[2,512,128]{2,1,0:T(8,128)(2,1)S(1)}, bf16[2,512,128]{2,1,0:T(8,128)(2,1)}, u32[]{:S(2)}) copy-start(bf16[2,512,128]{2,1,0:T(8,128)(2,1)} %param.19) | copy-start | bytes 786436
  15.5 27.8 %all-to-all-start = ((bf16[16,12,512]{2,1,0:T(8,128)(2,1)}), bf16[16,12,512]{2,1,0:T(8,128)(2,1)S(1)}, u32[]{:S(2)}, u32[]{:S(2)}) async-start(bf16[16,12,512]{2,1,0:T(8,128)(2,1)} %fusion.14), calls=%async_computation | async-start | bytes 524288 | tf_op jit(solution)/shard_map/all_to_all | solution.py:28
  32.4 45.1 %copy-start.7 = (f32[6,4]{1,0:T(8,128)}, f32[6,4]{1,0:T(8,128)S(1)}, u32[]{:S(2)}) copy-start(f32[6,4]{1,0:T(8,128)S(1)} %fusion.85) | copy-start | bytes 292
  32.8 48.4 %copy-start.55 = (pred[4,4]{1,0:T(4,128)(4,1)}, pred[4,4]{1,0:T(4,128)(4,1)S(1)}, u32[]{:S(2)}) copy-start(pred[4,4]{1,0:T(4,128)(4,1)S(1)} %iota_compare_fusion.8) | copy-start | bytes 52
  44.2 10.5 %all-to-all-start.1 = ((bf16[4,16,8,512]{3,1,2,0:T(8,128)(2,1)}), bf16[4,16,8,512]{3,1,2,0:T(8,128)(2,1)S(1)}, u32[]{:S(2)}, u32[]{:S(2)}) async-start(bf16[4,16,8,512]{3,1,2,0:T(8,128)(2,1)} %broadcast_in_dim.45), calls=%async_computation.1 | async-start | bytes 1048576 | tf_op jit(solution)/shard_map/all_to_all | solution.py:28
  49.0 30.5 %copy-start.30 = (bf16[6,3,128]{2,1,0:T(4,128)(2,1)}, bf16[6,3,128]{2,1,0:T(4,128)(2,1)S(1)}, u32[]{:S(2)}) copy-start(bf16[6,3,128]{2,1,0:T(4,128)(2,1)S(1)} %get-tuple-element.95) | copy-start | bytes 13828
  57.6 18.7 %all-to-all-start.2 = ((bf16[8,24,640]{2,1,0:T(8,128)(2,1)}), bf16[8,24,640]{2,1,0:T(8,128)(2,1)S(1)}, u32[]{:S(2)}, u32[]{:S(2)}) async-start(bf16[8,24,640]{2,1,0:T(8,128)(2,1)} %shard_map.174), calls=%async_computation.2 | async-start | bytes 491520 | tf_op jit(solution)/shard_map/all_to_all | solution.py:28
  72.0 8.2 %copy-start.13 = (bf16[6,3,256]{2,1,0:T(4,128)(2,1)}, bf16[6,3,256]{2,1,0:T(4,128)(2,1)S(1)}, u32[]{:S(2)}) copy-start(bf16[6,3,256]{2,1,0:T(4,128)(2,1)S(1)} %squeeze.21) | copy-start | bytes 27652
  82.3 12.0 %all-to-all-start.3 = ((bf16[32,8,128]{2,1,0:T(8,128)(2,1)}), bf16[32,8,128]{2,1,0:T(8,128)(2,1)S(1)}, u32[]{:S(2)}, u32[]{:S(2)}) async-start(bf16[32,8,128]{2,1,0:T(8,128)(2,1)} %bitcast.27), calls=%async_computation.3 | async-start | bytes 131072 | tf_op jit(solution)/shard_map/all_to_all | solution.py:28
  95.7 17.9 %all-to-all-start.4 = ((bf16[16,4,512]{2,1,0:T(4,128)(2,1)}), bf16[16,4,512]{2,1,0:T(4,128)(2,1)S(1)}, u32[]{:S(2)}, u32[]{:S(2)}) async-start(bf16[16,4,512]{2,1,0:T(4,128)(2,1)} %reshape.407), calls=%async_computation.4 | async-start | bytes 131072 | tf_op jit(solution)/shard_map/all_to_all | solution.py:28
  102.0 33.1 %collective-permute-start.3 = (bf16[448,512]{1,0:T(8,128)(2,1)S(1)}, bf16[448,512]{1,0:T(8,128)(2,1)S(1)}, u32[]{:S(2)}, u32[]{:S(2)}) collective-permute-start(bf16[448,512]{1,0:T(8,128)(2,1)S(1)} %pad_maximum_fusion.1.w0), channel_id=1, source_target_pairs={{0,8},{8,16},{16,24},{24,0},{1,9},{9,17},{17,25},{25,1},{2,10},{10... | collective-permute-start | bytes 1376264 | tf_op jit(solution)/shard_map/ppermute | solution.py:163
  104.3 30.9 %collective-permute-start.4 = (bf16[448,512]{1,0:T(8,128)(2,1)S(1)}, bf16[448,512]{1,0:T(8,128)(2,1)S(1)}, u32[]{:S(2)}, u32[]{:S(2)}) collective-permute-start(bf16[448,512]{1,0:T(8,128)(2,1)S(1)} %pad_maximum_fusion.1.w0), channel_id=1, source_target_pairs={{0,16},{8,24},{16,0},{24,8},{1,17},{9,25},{17,1},{25,9},{2,18},{10... | collective-permute-start | bytes 1376264 | tf_op jit(solution)/shard_map/ppermute | solution.py:163
  107.9 27.3 %collective-permute-start.5 = (bf16[448,512]{1,0:T(8,128)(2,1)S(1)}, bf16[448,512]{1,0:T(8,128)(2,1)S(1)}, u32[]{:S(2)}, u32[]{:S(2)}) collective-permute-start(bf16[448,512]{1,0:T(8,128)(2,1)S(1)} %pad_maximum_fusion.1.w0), channel_id=1, source_target_pairs={{0,24},{8,0},{16,8},{24,16},{1,25},{9,1},{17,9},{25,17},{2,26},{10... | collective-permute-start | bytes 1376264 | tf_op jit(solution)/shard_map/ppermute | solution.py:163
  114.9 20.2 %all-to-all-start.5 = ((bf16[16,4,512]{2,1,0:T(4,128)(2,1)}), bf16[16,4,512]{2,1,0:T(4,128)(2,1)S(1)}, u32[]{:S(2)}, u32[]{:S(2)}) async-start(bf16[16,4,512]{2,1,0:T(4,128)(2,1)} %broadcast_in_dim.50), calls=%async_computation.5 | async-start | bytes 131072 | tf_op jit(solution)/shard_map/all_to_all | solution.py:28
  137.1 17.3 %all-to-all-start.6 = ((bf16[32,8,640]{2,1,0:T(8,128)(2,1)}), bf16[32,8,640]{2,1,0:T(8,128)(2,1)S(1)}, u32[]{:S(2)}, u32[]{:S(2)}) async-start(bf16[32,8,640]{2,1,0:T(8,128)(2,1)} %bitcast.36), calls=%async_computation.6 | async-start | bytes 655360 | tf_op jit(solution)/shard_map/all_to_all | solution.py:28
  161.8 11.3 %all-to-all-start.7 = ((bf16[32,8,128]{2,1,0:T(8,128)(2,1)}), bf16[32,8,128]{2,1,0:T(8,128)(2,1)S(1)}, u32[]{:S(2)}, u32[]{:S(2)}) async-start(bf16[32,8,128]{2,1,0:T(8,128)(2,1)} %bitcast.54), calls=%async_computation.7 | async-start | bytes 131072 | tf_op jit(solution)/shard_map/all_to_all | solution.py:28
  174.7 18.4 %all-to-all-start.8 = ((bf16[16,4,512]{2,1,0:T(4,128)(2,1)}), bf16[16,4,512]{2,1,0:T(4,128)(2,1)S(1)}, u32[]{:S(2)}, u32[]{:S(2)}) async-start(bf16[16,4,512]{2,1,0:T(4,128)(2,1)} %reshape.424), calls=%async_computation.8 | async-start | bytes 131072 | tf_op jit(solution)/shard_map/all_to_all | solution.py:28
  182.8 10.3 %copy-start.20 = (bf16[3,512]{1,0:T(4,128)(2,1)S(1)}, bf16[3,512]{1,0:T(4,128)(2,1)}, u32[]{:S(2)}) copy-start(bf16[3,512]{1,0:T(4,128)(2,1)} %copy-done.19) | copy-start | bytes 9220
  (49 other events, 72.0 us)

commit v3 on v2

v3 whole, which is shorter than its diff:
```python
import functools

import jax
import jax.numpy as jnp
from jax import lax
from jax.experimental import pallas as pl
from jax.experimental.pallas import tpu as pltpu
from jax.sharding import Mesh, PartitionSpec as P

D = 4096
HEADS = 128
HEAD_DIM = 64
STATE = 128
GROUPS = 16
CONV = 4
NEW = 4
LAYERS = 2
norm_floor = 0.1

ZN, YN, DN = 16, 4, 8
SEQ = 6
bf16 = jnp.bfloat16
f32 = jnp.float32
COLS = 640


def exchange(pieces, axis):
    return lax.all_to_all(pieces, axis, 0, 0, tiled=True)


def copies(value, peers):
    return jnp.broadcast_to(value[None], (peers, *value.shape))


def one_hot(rows, cols, target):
    row = lax.broadcasted_iota(jnp.int32, (rows, cols), 0)
    col = lax.broadcasted_iota(jnp.int32, (rows, cols), 1)
    return jnp.where(row == target(col), 1.0, 0.0).astype(bf16)


def mm(a, b):
    return lax.dot_general(a, b, (((1,), (0,)), ((), ())), preferred_element_type=f32)


def mm_t(a, b):
    return lax.dot_general(a, b, (((1,), (1,)), ((), ())), preferred_element_type=f32)


def normed_rows(rows, gain):
    widened = rows.astype(f32)
    squares = jnp.sum(widened * widened, axis=1, keepdims=True)
    return (widened * gain).astype(bf16), squares


def step_lanes(at_ref, normed, squares, step_w):
    step = mm(normed, step_w)
    lane = lax.broadcasted_iota(jnp.int32, step.shape, 1)
    return jnp.where(lane == at_ref[2], squares, step)


def first_projection(at_ref, plane_ref, gain_ref, gate_ref, value_ref, step_ref, out_ref):
    plane = plane_ref[...]

    def token_source(col):
        i = col % 8
        return jnp.where(i < 3, 12 * ((col // 8) % ZN) + 3 * (col // 128) + i, -1)

    def vector_source(col):
        j = col % 8 - 4
        n = 8 * ((col // 8) % ZN) + 2 * (col // 128) + j % 2
        return jnp.where((j >= 0) & (j < 4), 128 * (j // 2) + n, -1)

    rows = mm(one_hot(192, 512, token_source), plane).astype(bf16)
    vector_w = mm(one_hot(256, 512, vector_source), plane).astype(bf16)
    normed, squares = normed_rows(rows, gain_ref[0:1])
    parts = [
        mm(normed, gate_ref[0]),
        mm(normed, value_ref[0]),
        mm_t(normed, vector_w),
        step_lanes(at_ref, normed, squares, step_ref[0]),
    ]
    at = 0
    for part in parts:
        width = part.shape[1]
        out_ref[:, :, at : at + width] = part.astype(bf16).reshape(DN, 24, width)
        at += width


def second_projection(at_ref, rows_ref, gain_ref, step_ref, w0, w1, w2, w3, out_ref):
    y = at_ref[1]
    normed, squares = normed_rows(rows_ref[...], gain_ref[1:2])
    pieces = [w0, w1, w2, w3]

    def source(col):
        j = col % 4
        n = 8 * ((col // 4) % ZN) + 2 * ((y - col // 64) % YN) + j % 2
        return 128 * (j // 2) + n

    stacked = jnp.concatenate([w[384:448] for w in pieces], axis=0)
    vector_w = mm(one_hot(256, 256, source), stacked).astype(bf16)
    vector = mm_t(normed, vector_w).astype(bf16)
    extra = step_lanes(at_ref, normed, squares, step_ref[0]).astype(bf16)
    for k, w in enumerate(pieces):
        to = (y - k) % YN
        for n in range(2):
            total = jnp.zeros((64, 128), f32)
            for b in range(4):
                total += mm(
                    normed[:, 128 * b : 128 * b + 128],
                    w[128 * n : 128 * n + 128, 128 * b : 128 * b + 128],
                )
            out_ref[to, :, 128 * n : 128 * n + 128] = total.astype(bf16)
        out_ref[to, :, 256:512] = vector
        out_ref[to, :, 512:640] = extra


def out_projection(at_ref, mixed_ref, w0, w1, w2, w3, *rest, first_row):
    y = at_ref[1]
    total = jnp.zeros((64, 512), f32)
    for k, w in enumerate([w0, w1, w2, w3]):
        total += mm(mixed_ref[(y - k) % YN], w[first_row : first_row + 128])
    if len(rest) == 1:
        rest[0][...] = total.astype(bf16).reshape(ZN, 4, 512)
        return
    returned_ref, out_ref = rest
    returned = jnp.concatenate(
        [returned_ref[:, 0:128], returned_ref[:, 128:256], jnp.zeros((32, 128), bf16)], axis=0
    )
    slot = one_hot(64, ZN, lambda col: 4 * col + 3)
    halves = []
    for nl in range(2):
        row = lax.broadcasted_iota(jnp.int32, (ZN, 128), 0)
        col = lax.broadcasted_iota(jnp.int32, (ZN, 128), 1)
        chosen = jnp.where(col == 8 * row + 2 * y + nl, 1.0, 0.0).astype(bf16)
        halves.append(mm_t(chosen, returned).astype(bf16))
    tail = jnp.concatenate(halves, axis=1)
    left = (total[:, 0:256] + mm(slot, tail)).astype(bf16)
    whole = jnp.concatenate([left, total[:, 256:512].astype(bf16)], axis=1)
    out_ref[...] = whole.reshape(ZN, 4, 512)


def row_col(shape):
    return (
        lax.broadcasted_iota(jnp.int32, shape, 0),
        lax.broadcasted_iota(jnp.int32, shape, 1),
    )


def silu(x):
    return x * jax.nn.sigmoid(x)


def lengths_column(len_ref):
    row = lax.broadcasted_iota(jnp.int32, (8, 1), 0)
    lens = jnp.zeros((8, 1), jnp.int32)
    for s in range(SEQ):
        lens = jnp.where(row == s, len_ref[s], lens)
    return lens


def place_first(col):
    return 8 * (col % NEW) + col // NEW


def place_second(col):
    i = col % 4
    n = 12 * ((col // 4) % 2) + 3 * (col // 8) + i
    return jnp.where(i < 3, 8 * (n % NEW) + n // NEW, -1)


def conv(history_ref, fresh, taps_ref):
    rows = [history_ref[k].astype(f32) for k in range(CONV - 1)]
    rows += [fresh[8 * t : 8 * t + 8] for t in range(NEW)]
    taps = [taps_ref[k : k + 1].astype(f32) for k in range(CONV)]
    return [silu(sum(rows[t + k] * taps[k] for k in range(CONV))) for t in range(NEW)]


def middle(
    at_ref,
    len_ref,
    bias_ref,
    rate_ref,
    part_ref,
    history_ref,
    taps_ref,
    vhist_ref,
    vtaps_ref,
    state_ref,
    msg_ref,
    keep_ref,
    write_ref,
    decay_ref,
    fresh_ref,
    *,
    layer,
):
    if layer == 0:
        total = sum(part_ref[d].astype(f32) for d in range(DN))
        place = one_hot(32, 24, place_first)
    else:
        rows = [sum(part_ref[y, d].astype(f32) for d in range(DN)) for y in range(YN)]
        total = jnp.concatenate(rows, axis=0)
        place = one_hot(32, 32, place_second)
    tail = total[:, 512:640]
    _, lane = row_col(tail.shape)
    squares = jnp.sum(jnp.where(lane == at_ref[2], tail, 0.0), axis=1, keepdims=True)
    scaled = (total * lax.rsqrt(squares / D + norm_floor)).astype(bf16)
    rows = mm(place, scaled)
    fresh_ref[...] = rows[:, 128:512].astype(bf16)
    gate = rows[:, 0:128]

    head = 8 * at_ref[0] + 2 * at_ref[1]
    tail = rows[:, 512:640]
    _, lane = row_col(tail.shape)
    first = jnp.sum(jnp.where(lane == head, tail, 0.0), axis=1, keepdims=True)
    second = jnp.sum(jnp.where(lane == head + 1, tail, 0.0), axis=1, keepdims=True)
    left = lane < HEAD_DIM
    raw = jnp.where(left, first + bias_ref[layer, 0], second + bias_ref[layer, 1])
    rate = jnp.where(left[:8], rate_ref[layer, 0], rate_ref[layer, 1])
    soft = jnp.maximum(raw, 0.0) + jnp.log1p(jnp.exp(-jnp.abs(raw)))
    lens = lengths_column(len_ref)
    live = [jnp.where(lens > t, 1.0, 0.0) for t in range(NEW)]
    step = [soft[8 * t : 8 * t + 8] * live[t] for t in range(NEW)]
    cumulative = []
    for t in range(NEW):
        grown = step[t] * rate
        cumulative.append(grown if t == 0 else cumulative[-1] + grown)

    values = conv(history_ref, rows[:, 128:256], taps_ref)
    vectors = conv(vhist_ref, rows[:, 256:512], vtaps_ref)
    write = [v[:, 0:128] for v in vectors]
    read = [v[:, 128:256] for v in vectors]
    stepped = [values[t] * step[t] for t in range(NEW)]

    reads = jnp.concatenate(read, axis=0).astype(bf16)
    row, _ = row_col((32, 128))
    carried = jnp.zeros((32, 128), f32)
    for s in range(SEQ):
        carried = jnp.where(row % 8 == s, mm_t(reads, state_ref[s].astype(bf16)), carried)

    mixed = []
    for t in range(NEW):
        y = jnp.exp(-cumulative[t]) * carried[8 * t : 8 * t + 8]
        for u in range(t + 1):
            score = jnp.sum(read[t] * write[u], axis=1, keepdims=True)
            y = y + score * jnp.exp(cumulative[u] - cumulative[t]) * stepped[u]
        mixed.append(y * silu(gate[8 * t : 8 * t + 8]) * live[t])
    mixed = jnp.concatenate(mixed, axis=0).astype(bf16)
    row, col = row_col((32, 32))
    i = row % 4
    n = 12 * ((row // 4) % 2) + 3 * (row // 8) + i
    pick = (col == 8 * (n % NEW) + n // NEW) & (i < 3)
    ordered = mm(jnp.where(pick, 1.0, 0.0).astype(bf16), mixed).astype(bf16)
    for y in range(YN):
        for d in range(DN):
            msg_ref[y * DN + d] = ordered[8 * y : 8 * y + 8]

    last = cumulative[-1]
    for t in range(NEW):
        keep_ref[8 * t : 8 * t + 8] = jnp.exp(cumulative[t] - last) * stepped[t]
        write_ref[8 * t : 8 * t + 8] = write[t]
    decay_ref[...] = jnp.exp(-last)


def finish(
    len_ref,
    keep_ref,
    write_ref,
    decay_ref,
    fresh_ref,
    history_ref,
    vhist_ref,
    state_ref,
    next_ref,
    value_ref,
    vector_ref,
):
    kept = jnp.transpose(keep_ref[...])
    _, col = row_col(kept.shape)
    write = write_ref[...].astype(bf16)
    for s in range(SEQ):
        fresh = mm(jnp.where(col % 8 == s, kept, 0.0).astype(bf16), write)
        for h in range(2):
            at = slice(HEAD_DIM * h, HEAD_DIM * h + HEAD_DIM)
            decay = decay_ref[s : s + 1, HEAD_DIM * h : HEAD_DIM * h + 1]
            next_ref[s, at] = state_ref[s, at] * decay + fresh[at]
    lens = lengths_column(len_ref)
    for out_ref, old_ref, lo, hi in (
        (value_ref, history_ref, 0, 128),
        (vector_ref, vhist_ref, 128, 384),
    ):
        rows = [old_ref[k].astype(f32) for k in range(CONV - 1)]
        rows += [fresh_ref[8 * t : 8 * t + 8, lo:hi].astype(f32) for t in range(NEW)]
        for k in range(CONV - 1):
            chosen = rows[k + 1]
            for r in range(k + 2, k + NEW + 1):
                chosen = jnp.where(lens + k == r, rows[r], chosen)
            out_ref[k] = chosen.astype(bf16)


def call(kernel, shapes, scalars, *args):
    vmem = pl.BlockSpec(memory_space=pltpu.VMEM)
    space = [pl.BlockSpec(memory_space=pltpu.SMEM)] * scalars
    space += [vmem] * (len(args) - scalars)
    outs = [jax.ShapeDtypeStruct(shape, dtype) for shape, dtype in shapes]
    results = pl.pallas_call(
        kernel,
        out_shape=outs,
        in_specs=space,
        out_specs=[vmem] * len(outs),
        compiler_params=pltpu.CompilerParams(vmem_limit_bytes=12 << 20),
    )(*args)
    return results[0] if len(outs) == 1 else results


def around_y(value):
    pieces = [value]
    for k in range(1, YN):
        pieces.append(lax.ppermute(value, "y", [(i, (i + k) % YN) for i in range(YN)]))
    return pieces


def body(
    tokens,
    lengths,
    norm_gain,
    gate_weight,
    value_weight,
    vector_weight,
    step_weight,
    step_bias,
    decay_rate,
    value_taps,
    vector_taps,
    out_weight,
    recurrent_state,
    value_history,
    vector_history,
):
    z = lax.axis_index("z")
    y = lax.axis_index("y")
    square_lane = (8 * z + 64) % HEADS
    vector_cols = vector_weight.transpose(0, 2, 3, 1).reshape(2, 2, 2, GROUPS, 512)
    vector_cols = vector_cols.transpose(3, 0, 1, 2, 4).reshape(GROUPS, 8, 512)
    small = jnp.concatenate([vector_history.reshape(72, 32), vector_taps.reshape(16, 32)], axis=0)
    small = small.reshape(88, 2, GROUPS).transpose(2, 1, 0).reshape(GROUPS, 1, 176)
    small = jnp.pad(small, ((0, 0), (0, 0), (0, 512 - 176)))
    first = jnp.concatenate([copies(tokens, ZN), small], axis=1).reshape(ZN, 1, 4, 512)
    first = jnp.concatenate([first, vector_cols.reshape(ZN, 2, 4, 512)], axis=1)
    at = jnp.stack([z, y, square_lane]).astype(jnp.int32)
    first, own_out = lax.optimization_barrier((first, out_weight[0]))
    first = exchange(first, "z")
    own_out = around_y(own_out)
    plane = exchange(copies(first[:, :2], YN), "y").reshape(YN, ZN, 8, 512)

    small = plane[:, :, 3, :176].reshape(YN, ZN, 2, 88).transpose(3, 1, 0, 2).reshape(88, 128)
    vhist = small[:72].reshape(2, SEQ, 3, 256).transpose(0, 2, 1, 3)
    vhist = jnp.pad(vhist, ((0, 0), (0, 0), (0, 2), (0, 0)))
    vtaps = small[72:].reshape(2, CONV, 256)
    history = jnp.pad(value_history.transpose(0, 2, 1, 3), ((0, 0), (0, 0), (0, 2), (0, 0)))
    states = [recurrent_state[layer].reshape(SEQ, 128, 128) for layer in range(LAYERS)]

    def mid(part, layer):
        old = (history[layer], vhist[layer])
        msg, keep, write, decay, fresh = call(
            functools.partial(middle, layer=layer),
            [
                ((YN * DN, 8, 128), bf16),
                ((32, 128), f32),
                ((32, 128), f32),
                ((8, 128), f32),
                ((32, 384), bf16),
            ],
            4,
            at,
            lengths,
            step_bias,
            decay_rate,
            part,
            history[layer],
            value_taps[layer],
            vhist[layer],
            vtaps[layer],
            states[layer],
        )
        after = call(
            finish,
            [((SEQ, 128, 128), f32), ((3, 8, 128), bf16), ((3, 8, 256), bf16)],
            1,
            lengths,
            keep,
            write,
            decay,
            fresh,
            *old,
            states[layer],
        )
        return exchange(msg, ("y", "dp")).reshape(YN, DN * 8, 128), after

    part = call(
        first_projection,
        [((DN, 24, COLS), bf16)],
        1,
        at,
        plane.reshape(512, 512),
        norm_gain,
        gate_weight[:1],
        value_weight[:1],
        step_weight[:1],
    )
    part = exchange(part, "dp")
    mixed, (state0, value0, vector0) = mid(part, 0)
    update = call(
        functools.partial(out_projection, first_row=0),
        [((ZN, 4, 512), bf16)],
        1,
        at,
        mixed,
        *own_out,
    )

    def lanes(w):
        return w.reshape(4, 128, 128).transpose(1, 0, 2).reshape(128, 512)

    later = jnp.concatenate(
        [
            lanes(gate_weight[1]),
            lanes(value_weight[1]),
            out_weight[1],
            first[:, 2].reshape(64, 512),
        ],
        axis=0,
    )
    update, later = lax.optimization_barrier((update, later))
    update = exchange(update, "z")
    later = around_y(later)
    update = jnp.sum(update.astype(f32), axis=0)[:3]
    token_rows = (tokens.astype(f32) + update).astype(bf16)

    quarter = exchange(copies(jnp.pad(token_rows, ((0, 1), (0, 0))), ZN), "z").reshape(64, 512)
    part = call(
        second_projection,
        [((YN, 64, COLS), bf16)],
        1,
        at,
        quarter,
        norm_gain,
        step_weight[1:],
        *later,
    )
    part = exchange(part.reshape(YN * DN, 8, COLS), ("y", "dp")).reshape(YN, DN, 8, COLS)
    mixed, (state1, value1, vector1) = mid(part, 1)
    update = call(
        functools.partial(out_projection, first_row=256),
        [((ZN, 4, 512), bf16)],
        1,
        at,
        mixed,
        *later,
        jnp.concatenate([vector0, vector1], axis=0).reshape(48, 256),
    )
    update = exchange(update, "z")
    token_rows = (
        token_rows.astype(f32) + jnp.sum(update[:, :3].astype(f32), axis=0)
    ).astype(bf16)
    returned = update[:, 3, :256].reshape(GROUPS, 2, 128)[:, :, :96]
    returned = returned.reshape(GROUPS, 2, 2, 2, 3, 8)[..., :SEQ].transpose(3, 5, 4, 2, 1, 0)
    next_vector = returned.reshape(2, SEQ, 3, 2, 32)
    return (
        token_rows,
        jnp.stack([state0, state1]).reshape(recurrent_state.shape),
        jnp.stack([value0, value1])[:, :, :SEQ].transpose(0, 2, 1, 3),
        next_vector,
    )


def solution(mesh):
    grid = Mesh(mesh.devices.reshape(ZN, YN, DN), ("z", "y", "dp"))
    tp = ("z", "y")
    return jax.shard_map(
        body,
        mesh=grid,
        in_specs=(
            P(tp, "dp"),
            P("dp"),
            P(None, "dp"),
            P(None, "dp", tp),
            P(None, "dp", tp),
            P(None, "dp", None, tp),
            P(None, "dp", None),
            P(None, tp),
            P(None, tp),
            P(None, None, tp),
            P(None, None, None, tp),
            P(None, tp, "dp"),
            P(None, "dp", tp, None, None),
            P(None, "dp", None, tp),
            P(None, "dp", None, None, tp),
        ),
        out_specs=(
            P(tp, "dp"),
            P(None, "dp", tp, None, None),
            P(None, "dp", None, tp),
            P(None, "dp", None, None, tp),
        ),
        check_vma=False,
    )
```

time: 196 us -> 173 us (0.88)
  blocking collectives: 0 us -> 20 us
  local copies, waits for them, and re-layouts: 31.9 us -> 16.2 us
  waiting for transfers between devices: 55.9 us -> 42 us
  starting transfers between devices: 89.3 us -> 78.4 us
  Pallas kernels: 5.46 us -> 11.9 us
  other arithmetic: 7.23 us -> 2.7 us
  matrix products: 3.21 us -> 0 us
    all_to_all x0 -> x1, blocking collectives: none -> 20 us  [exchange(): return lax.all_to_all(pieces, axis, 0, 0, tiled=True)]
    all_to_all x9 -> x8, waiting for transfers between devices: 55.9 us -> 42 us  [exchange(): return lax.all_to_all(pieces, axis, 0, 0, tiled=True)]
    all_to_all x9 -> x8, starting transfers between devices: 68.9 us -> 59 us  [exchange(): return lax.all_to_all(pieces, axis, 0, 0, tiled=True)]
    unnamed x121 -> x30, local copies, waits for them, and re-layouts: 11.3 us -> 1.48 us
    pallas_call x4 -> x8, Pallas kernels: 5.46 us -> 11.9 us  [call(): pl.pallas_call(kernel, out_shape=outs, in_specs=space, out_specs=[vmem] *...]
    convert_element_type x17 -> x0, local copies, waits for them, and re-layouts: 4.65 us -> none  [the longest x16 4.57 us: short_conv(): conv_taps[offset].astype(f32)]
    dot_general x12 -> x0, matrix products: 3.21 us -> none  [the longest x2 0.98 us: middle(): jnp.einsum('sjk,skc->sjc', picker, padded_vector, preferred_element_type=...]
    squeeze x2 -> x1, local copies, waits for them, and re-layouts: 2.27 us -> 0.01 us  [mid(): vhist[layer]]
  transfers between devices with their start and end apart: 15 -> 14, of which waited for: 9 -> 7; matrix products, arithmetic and copies ran while one was open for 13% -> 7% of each run, Pallas kernels for 1% -> 3%
where the time goes in v3:
time: 173 us; the launch traced here: 172 us
  starting transfers between devices  78.4 us (45%)
  waiting for transfers between devices  42 us (24%)
  blocking collectives  20 us (12%)
  local copies, waits for them, and re-layouts  16.2 us (9%)
  Pallas kernels  11.9 us (7%)
  other arithmetic  2.7 us (2%)
    all_to_all x8, starting transfers between devices, exchange(): return lax.all_to_all(pieces, axis, 0, 0, tiled=True)  59 us
    all_to_all x8, waiting for transfers between devices, exchange(): return lax.all_to_all(pieces, axis, 0, 0, tiled=True)  42 us
    all_to_all x1, blocking collectives, exchange(): return lax.all_to_all(pieces, axis, 0, 0, tiled=True)  20 us
    ppermute x6, starting transfers between devices, around_y(): lax.ppermute(value, 'y', [(i, (i + k) % YN) for i in range(YN)])  19.5 us
    pallas_call x8, Pallas kernels, call(): pl.pallas_call(kernel, out_shape=outs, in_specs=space, out_specs=[vmem] *...  11.9 us
  transfers between devices with their start and end apart: 14, of which 7 were waited for; matrix products, arithmetic and copies ran while one was open for 7% of the time, Pallas kernels for 3%

profile of v3, /device:TPU:1, one launch (start us, length us, event | category | flops | bytes accessed | tf_op | source)
XLA Modules:
  0.0 172.4 jit_solution(18307147450052337896)
XLA Ops:
  6.4 15.7 %all-to-all-start = ((bf16[16,3,4,512]{3,2,1,0:T(4,128)(2,1)}), bf16[16,3,4,512]{3,2,1,0:T(4,128)(2,1)S(1)}, u32[]{:S(2)}, u32[]{:S(2)}) async-start(bf16[16,3,4,512]{3,2,1,0:T(4,128)(2,1)} %pad_maximum_fusion.2), calls=%async_computation | async-start | bytes 393216 | tf_op jit(solution)/shard_map/all_to_all | solution.py:28
  22.1 3.2 %collective-permute-start = (bf16[128,512]{1,0:T(8,128)(2,1)S(1)}, bf16[128,512]{1,0:T(8,128)(2,1)S(1)}, u32[]{:S(2)}, u32[]{:S(2)}) collective-permute-start(bf16[128,512]{1,0:T(8,128)(2,1)S(1)} %get-tuple-element.26.w0), channel_id=1, source_target_pairs={{0,8},{8,16},{16,24},{24,0},{1,9},{9,17},{17,25},{25,1},{2,10},{10... | collective-permute-start | bytes 393224 | tf_op jit(solution)/shard_map/ppermute | solution.py:319
  25.3 4.5 %collective-permute-start.1 = (bf16[128,512]{1,0:T(8,128)(2,1)S(1)}, bf16[128,512]{1,0:T(8,128)(2,1)S(1)}, u32[]{:S(2)}, u32[]{:S(2)}) collective-permute-start(bf16[128,512]{1,0:T(8,128)(2,1)S(1)} %get-tuple-element.26.w0), channel_id=1, source_target_pairs={{0,16},{8,24},{16,0},{24,8},{1,17},{9,25},{17,1},{25,9},{2,18},{10... | collective-permute-start | bytes 393224 | tf_op jit(solution)/shard_map/ppermute | solution.py:319
  29.9 3.0 %collective-permute-start.2 = (bf16[128,512]{1,0:T(8,128)(2,1)S(1)}, bf16[128,512]{1,0:T(8,128)(2,1)S(1)}, u32[]{:S(2)}, u32[]{:S(2)}) collective-permute-start(bf16[128,512]{1,0:T(8,128)(2,1)S(1)} %get-tuple-element.26.w0), channel_id=1, source_target_pairs={{0,24},{8,0},{16,8},{24,16},{1,25},{9,1},{17,9},{25,17},{2,26},{10... | collective-permute-start | bytes 393224 | tf_op jit(solution)/shard_map/ppermute | solution.py:319
  35.6 4.2 %all-to-all-start.1 = ((bf16[4,16,2,4,512]{4,3,2,1,0:T(4,128)(2,1)}), bf16[4,16,2,4,512]{4,3,2,1,0:T(4,128)(2,1)S(1)}, u32[]{:S(2)}, u32[]{:S(2)}) async-start(bf16[4,16,2,4,512]{4,3,2,1,0:T(4,128)(2,1)} %broadcast_in_dim.7), calls=%async_computation.1 | async-start | bytes 1048576 | tf_op jit(solution)/shard_map/all_to_all | solution.py:28
  41.1 5.7 %all-to-all-done.1 = bf16[4,16,2,4,512]{4,3,2,1,0:T(4,128)(2,1)S(1)} async-done(((bf16[4,16,2,4,512]{4,3,2,1,0:T(4,128)(2,1)}), bf16[4,16,2,4,512]{4,3,2,1,0:T(4,128)(2,1)S(1)}, u32[]{:S(2)}, u32[]{:S(2)}) %all-to-all-start.1) | async-done | bytes 524320 | tf_op jit(solution)/shard_map/all_to_all | solution.py:28
  48.8 10.6 %all-to-all-start.2 = ((bf16[8,24,640]{2,1,0:T(8,128)(2,1)}), bf16[8,24,640]{2,1,0:T(8,128)(2,1)S(1)}, u32[]{:S(2)}, u32[]{:S(2)}) async-start(bf16[8,24,640]{2,1,0:T(8,128)(2,1)} %shard_map.174), calls=%async_computation.2 | async-start | bytes 491520 | tf_op jit(solution)/shard_map/all_to_all | solution.py:28
  59.8 2.8 %copy.79 = bf16[72,16,4,2]{3,2,1,0:T(4,128)(2,1)} copy(bf16[72,16,4,2]{0,3,1,2:T(2,128)(2,1)S(1)} %bitcast.87) | data formatting | bytes 36864 | tf_op jit(solution)/shard_map/slice | solution.py:357
  62.6 3.0 %reshape.82 = bf16[2,6,3,256]{3,2,1,0:T(4,128)(2,1)S(1)} reshape(bf16[72,16,4,2]{3,2,1,0:T(4,128)(2,1)} %copy.79) | data formatting | bytes 36864 | tf_op jit(solution)/shard_map/reshape | solution.py:357
  68.1 5.6 %all-to-all-start.3 = ((bf16[32,8,128]{2,1,0:T(8,128)(2,1)}), bf16[32,8,128]{2,1,0:T(8,128)(2,1)S(1)}, u32[]{:S(2)}, u32[]{:S(2)}) async-start(bf16[32,8,128]{2,1,0:T(8,128)(2,1)} %get-tuple-element.25), calls=%async_computation.3 | async-start | bytes 131072 | tf_op jit(solution)/shard_map/all_to_all | solution.py:28
  73.7 7.2 %all-to-all-done.3 = bf16[32,8,128]{2,1,0:T(8,128)(2,1)S(1)} async-done(((bf16[32,8,128]{2,1,0:T(8,128)(2,1)}), bf16[32,8,128]{2,1,0:T(8,128)(2,1)S(1)}, u32[]{:S(2)}, u32[]{:S(2)}) %all-to-all-start.3) | async-done | bytes 65568 | tf_op jit(solution)/shard_map/all_to_all | solution.py:28
  82.4 6.4 %all-to-all-start.4 = ((bf16[16,4,512]{2,1,0:T(4,128)(2,1)}), bf16[16,4,512]{2,1,0:T(4,128)(2,1)S(1)}, u32[]{:S(2)}, u32[]{:S(2)}) async-start(bf16[16,4,512]{2,1,0:T(4,128)(2,1)} %shard_map.176), calls=%async_computation.4 | async-start | bytes 131072 | tf_op jit(solution)/shard_map/all_to_all | solution.py:28
  88.8 2.2 %collective-permute-start.3 = (bf16[448,512]{1,0:T(8,128)(2,1)S(1)}, bf16[448,512]{1,0:T(8,128)(2,1)S(1)}, u32[]{:S(2)}, u32[]{:S(2)}) collective-permute-start(bf16[448,512]{1,0:T(8,128)(2,1)S(1)} %pad_maximum_fusion.1.w0), channel_id=1, source_target_pairs={{0,8},{8,16},{16,24},{24,0},{1,9},{9,17},{17,25},{25,1},{2,10},{10... | collective-permute-start | bytes 1376264 | tf_op jit(solution)/shard_map/ppermute | solution.py:319
  91.0 3.6 %collective-permute-start.4 = (bf16[448,512]{1,0:T(8,128)(2,1)S(1)}, bf16[448,512]{1,0:T(8,128)(2,1)S(1)}, u32[]{:S(2)}, u32[]{:S(2)}) collective-permute-start(bf16[448,512]{1,0:T(8,128)(2,1)S(1)} %pad_maximum_fusion.1.w0), channel_id=1, source_target_pairs={{0,16},{8,24},{16,0},{24,8},{1,17},{9,25},{17,1},{25,9},{2,18},{10... | collective-permute-start | bytes 1376264 | tf_op jit(solution)/shard_map/ppermute | solution.py:319
  94.7 2.9 %collective-permute-start.5 = (bf16[448,512]{1,0:T(8,128)(2,1)S(1)}, bf16[448,512]{1,0:T(8,128)(2,1)S(1)}, u32[]{:S(2)}, u32[]{:S(2)}) collective-permute-start(bf16[448,512]{1,0:T(8,128)(2,1)S(1)} %pad_maximum_fusion.1.w0), channel_id=1, source_target_pairs={{0,24},{8,0},{16,8},{24,16},{1,25},{9,1},{17,9},{25,17},{2,26},{10... | collective-permute-start | bytes 1376264 | tf_op jit(solution)/shard_map/ppermute | solution.py:319
  97.5 2.8 %all-to-all-done.4 = bf16[16,4,512]{2,1,0:T(4,128)(2,1)S(1)} async-done(((bf16[16,4,512]{2,1,0:T(4,128)(2,1)}), bf16[16,4,512]{2,1,0:T(4,128)(2,1)S(1)}, u32[]{:S(2)}, u32[]{:S(2)}) %all-to-all-start.4) | async-done | bytes 65568 | tf_op jit(solution)/shard_map/all_to_all | solution.py:28
  100.5 20.0 %all_to_all.45 = bf16[16,4,512]{2,1,0:T(4,128)(2,1)S(1)} all-to-all(bf16[16,4,512]{2,1,0:T(4,128)(2,1)S(1)} %broadcast_in_dim.8), channel_id=1, replica_groups=mesh['z'=16,'y'=4,'dp'=8] {'z'}, dimensions={0} | all-to-all | bytes 131072 | tf_op jit(solution)/shard_map/all_to_all | solution.py:28
  120.5 1.9 %shard_map.177 = bf16[4,64,640]{2,1,0:T(8,128)(2,1)} custom-call(s32[3]{0:T(128)S(1)} %pad_add_fusion.at_ref, bf16[64,512]{1,0:T(8,128)(2,1)S(1)} %reshape.86.rows_ref, f32[2,512]{1,0:T(2,128)S(1)} %copy-done, bf16[1,512,128]{2,1,0:T(8,128)(2,1)S(1)} %get-tuple-element.66.step_ref, bf16[448,512]{1,0:T(8,128)(2,1)S(1)} %pad_maximum_fusion.1.w0, ...), custom_call_target="tpu_custom_call" | custom-call | tf_op jit(solution)/shard_map/pallas_call | solution.py:306
  122.5 7.7 %all-to-all-start.6 = ((bf16[32,8,640]{2,1,0:T(8,128)(2,1)}), bf16[32,8,640]{2,1,0:T(8,128)(2,1)S(1)}, u32[]{:S(2)}, u32[]{:S(2)}) async-start(bf16[32,8,640]{2,1,0:T(8,128)(2,1)} %bitcast.23), calls=%async_computation.6 | async-start | bytes 655360 | tf_op jit(solution)/shard_map/all_to_all | solution.py:28
  131.6 8.0 %all-to-all-done.6 = bf16[32,8,640]{2,1,0:T(8,128)(2,1)S(1)} async-done(((bf16[32,8,640]{2,1,0:T(8,128)(2,1)}), bf16[32,8,640]{2,1,0:T(8,128)(2,1)S(1)}, u32[]{:S(2)}, u32[]{:S(2)}) %all-to-all-start.6) | async-done | bytes 327712 | tf_op jit(solution)/shard_map/all_to_all | solution.py:28
  141.4 3.7 %all-to-all-start.7 = ((bf16[32,8,128]{2,1,0:T(8,128)(2,1)}), bf16[32,8,128]{2,1,0:T(8,128)(2,1)S(1)}, u32[]{:S(2)}, u32[]{:S(2)}) async-start(bf16[32,8,128]{2,1,0:T(8,128)(2,1)} %get-tuple-element.29), calls=%async_computation.7 | async-start | bytes 131072 | tf_op jit(solution)/shard_map/all_to_all | solution.py:28
  146.0 6.6 %all-to-all-done.7 = bf16[32,8,128]{2,1,0:T(8,128)(2,1)S(1)} async-done(((bf16[32,8,128]{2,1,0:T(8,128)(2,1)}), bf16[32,8,128]{2,1,0:T(8,128)(2,1)S(1)}, u32[]{:S(2)}, u32[]{:S(2)}) %all-to-all-start.7) | async-done | bytes 65568 | tf_op jit(solution)/shard_map/all_to_all | solution.py:28
  154.1 5.1 %all-to-all-start.8 = ((bf16[16,4,512]{2,1,0:T(4,128)(2,1)}), bf16[16,4,512]{2,1,0:T(4,128)(2,1)S(1)}, u32[]{:S(2)}, u32[]{:S(2)}) async-start(bf16[16,4,512]{2,1,0:T(4,128)(2,1)} %shard_map.181), calls=%async_computation.8 | async-start | bytes 131072 | tf_op jit(solution)/shard_map/all_to_all | solution.py:28
  160.8 10.0 %all-to-all-done.8 = bf16[16,4,512]{2,1,0:T(4,128)(2,1)S(1)} async-done(((bf16[16,4,512]{2,1,0:T(4,128)(2,1)}), bf16[16,4,512]{2,1,0:T(4,128)(2,1)S(1)}, u32[]{:S(2)}, u32[]{:S(2)}) %all-to-all-start.8) | async-done | bytes 65568 | tf_op jit(solution)/shard_map/all_to_all | solution.py:28
  (98 shorter events, 24.7 us)
Async XLA Ops:
  0.6 32.2 %copy-start.12 = (bf16[2,4,128]{2,1,0:T(4,128)(2,1)S(1)}, bf16[2,4,128]{2,1,0:T(4,128)(2,1)}, u32[]{:S(2)}) copy-start(bf16[2,4,128]{2,1,0:T(4,128)(2,1)} %param.24) | copy-start | bytes 6148
  0.7 32.2 %copy-start.7 = (bf16[2,512,128]{2,1,0:T(8,128)(2,1)S(1)}, bf16[2,512,128]{2,1,0:T(8,128)(2,1)}, u32[]{:S(2)}) copy-start(bf16[2,512,128]{2,1,0:T(8,128)(2,1)} %param.19) | copy-start | bytes 786436
  1.8 31.1 %copy-start.8 = (bf16[2,512,128]{2,1,0:T(8,128)(2,1)S(1)}, bf16[2,512,128]{2,1,0:T(8,128)(2,1)}, u32[]{:S(2)}) copy-start(bf16[2,512,128]{2,1,0:T(8,128)(2,1)} %param.21) | copy-start | bytes 786436
  1.8 31.1 %copy-start.9 = (bf16[2,512,128]{2,1,0:T(8,128)(2,1)S(1)}, bf16[2,512,128]{2,1,0:T(8,128)(2,1)}, u32[]{:S(2)}) copy-start(bf16[2,512,128]{2,1,0:T(8,128)(2,1)} %param.18) | copy-start | bytes 786436
  6.4 28.2 %all-to-all-start = ((bf16[16,3,4,512]{3,2,1,0:T(4,128)(2,1)}), bf16[16,3,4,512]{3,2,1,0:T(4,128)(2,1)S(1)}, u32[]{:S(2)}, u32[]{:S(2)}) async-start(bf16[16,3,4,512]{3,2,1,0:T(4,128)(2,1)} %pad_maximum_fusion.2), calls=%async_computation | async-start | bytes 393216 | tf_op jit(solution)/shard_map/all_to_all | solution.py:28
  22.1 51.6 %collective-permute-start = (bf16[128,512]{1,0:T(8,128)(2,1)S(1)}, bf16[128,512]{1,0:T(8,128)(2,1)S(1)}, u32[]{:S(2)}, u32[]{:S(2)}) collective-permute-start(bf16[128,512]{1,0:T(8,128)(2,1)S(1)} %get-tuple-element.26.w0), channel_id=1, source_target_pairs={{0,8},{8,16},{16,24},{24,0},{1,9},{9,17},{17,25},{25,1},{2,10},{10... | collective-permute-start | bytes 393224 | tf_op jit(solution)/shard_map/ppermute | solution.py:319
  25.3 48.4 %collective-permute-start.1 = (bf16[128,512]{1,0:T(8,128)(2,1)S(1)}, bf16[128,512]{1,0:T(8,128)(2,1)S(1)}, u32[]{:S(2)}, u32[]{:S(2)}) collective-permute-start(bf16[128,512]{1,0:T(8,128)(2,1)S(1)} %get-tuple-element.26.w0), channel_id=1, source_target_pairs={{0,16},{8,24},{16,0},{24,8},{1,17},{9,25},{17,1},{25,9},{2,18},{10... | collective-permute-start | bytes 393224 | tf_op jit(solution)/shard_map/ppermute | solution.py:319
  29.9 43.9 %collective-permute-start.2 = (bf16[128,512]{1,0:T(8,128)(2,1)S(1)}, bf16[128,512]{1,0:T(8,128)(2,1)S(1)}, u32[]{:S(2)}, u32[]{:S(2)}) collective-permute-start(bf16[128,512]{1,0:T(8,128)(2,1)S(1)} %get-tuple-element.26.w0), channel_id=1, source_target_pairs={{0,24},{8,0},{16,8},{24,16},{1,25},{9,1},{17,9},{25,17},{2,26},{10... | collective-permute-start | bytes 393224 | tf_op jit(solution)/shard_map/ppermute | solution.py:319
  33.0 6.9 %copy-start.11 = (bf16[2,6,3,128]{3,0,2,1:T(2,128)(2,1)S(1)}, bf16[2,6,3,128]{3,0,2,1:T(2,128)(2,1)}, u32[]{:S(2)}) copy-start(bf16[2,6,3,128]{3,0,2,1:T(2,128)(2,1)} %param.28) | copy-start | bytes 27652
  35.6 11.1 %all-to-all-start.1 = ((bf16[4,16,2,4,512]{4,3,2,1,0:T(4,128)(2,1)}), bf16[4,16,2,4,512]{4,3,2,1,0:T(4,128)(2,1)S(1)}, u32[]{:S(2)}, u32[]{:S(2)}) async-start(bf16[4,16,2,4,512]{4,3,2,1,0:T(4,128)(2,1)} %broadcast_in_dim.7), calls=%async_computation.1 | async-start | bytes 1048576 | tf_op jit(solution)/shard_map/all_to_all | solution.py:28
  48.8 17.5 %all-to-all-start.2 = ((bf16[8,24,640]{2,1,0:T(8,128)(2,1)}), bf16[8,24,640]{2,1,0:T(8,128)(2,1)S(1)}, u32[]{:S(2)}, u32[]{:S(2)}) async-start(bf16[8,24,640]{2,1,0:T(8,128)(2,1)} %shard_map.174), calls=%async_computation.2 | async-start | bytes 491520 | tf_op jit(solution)/shard_map/all_to_all | solution.py:28
  59.7 6.6 %copy-start.1 = (s32[6]{0:T(128)S(1)}, s32[6]{0:T(128)}, u32[]{:S(2)}) copy-start(s32[6]{0:T(128)} %len_ref.7) | copy-start | bytes 76
  59.7 6.6 %copy-start.2 = (f32[2,2]{1,0:T(2,128)S(1)}, f32[2,2]{1,0:T(2,128)}, u32[]{:S(2)}) copy-start(f32[2,2]{1,0:T(2,128)} %bias_ref.3) | copy-start | bytes 52
  59.8 6.6 %copy-start.3 = (f32[2,2]{1,0:T(2,128)S(1)}, f32[2,2]{1,0:T(2,128)}, u32[]{:S(2)}) copy-start(f32[2,2]{1,0:T(2,128)} %rate_ref.3) | copy-start | bytes 52
  62.6 11.1 %copy-start.5 = (bf16[16,8,4,128]{3,1,2,0:T(8,128)(2,1)S(1)}, bf16[16,8,4,128]{3,1,2,0:T(8,128)(2,1)}, u32[]{:S(2)}) copy-start(bf16[16,8,4,128]{3,1,2,0:T(8,128)(2,1)} %copy.97) | copy-start | bytes 393220
  62.6 11.1 %copy-start.6 = (bf16[128,512]{1,0:T(8,128)(2,1)S(1)}, bf16[128,512]{1,0:T(8,128)(2,1)}, u32[]{:S(2)}) copy-start(bf16[128,512]{1,0:T(8,128)(2,1)} %get-tuple-element.72) | copy-start | bytes 393220
  68.1 12.9 %all-to-all-start.3 = ((bf16[32,8,128]{2,1,0:T(8,128)(2,1)}), bf16[32,8,128]{2,1,0:T(8,128)(2,1)S(1)}, u32[]{:S(2)}, u32[]{:S(2)}) async-start(bf16[32,8,128]{2,1,0:T(8,128)(2,1)} %get-tuple-element.25), calls=%async_computation.3 | async-start | bytes 131072 | tf_op jit(solution)/shard_map/all_to_all | solution.py:28
  82.4 18.0 %all-to-all-start.4 = ((bf16[16,4,512]{2,1,0:T(4,128)(2,1)}), bf16[16,4,512]{2,1,0:T(4,128)(2,1)S(1)}, u32[]{:S(2)}, u32[]{:S(2)}) async-start(bf16[16,4,512]{2,1,0:T(4,128)(2,1)} %shard_map.176), calls=%async_computation.4 | async-start | bytes 131072 | tf_op jit(solution)/shard_map/all_to_all | solution.py:28
  88.8 31.7 %collective-permute-start.3 = (bf16[448,512]{1,0:T(8,128)(2,1)S(1)}, bf16[448,512]{1,0:T(8,128)(2,1)S(1)}, u32[]{:S(2)}, u32[]{:S(2)}) collective-permute-start(bf16[448,512]{1,0:T(8,128)(2,1)S(1)} %pad_maximum_fusion.1.w0), channel_id=1, source_target_pairs={{0,8},{8,16},{16,24},{24,0},{1,9},{9,17},{17,25},{25,1},{2,10},{10... | collective-permute-start | bytes 1376264 | tf_op jit(solution)/shard_map/ppermute | solution.py:319
  91.0 29.5 %collective-permute-start.4 = (bf16[448,512]{1,0:T(8,128)(2,1)S(1)}, bf16[448,512]{1,0:T(8,128)(2,1)S(1)}, u32[]{:S(2)}, u32[]{:S(2)}) collective-permute-start(bf16[448,512]{1,0:T(8,128)(2,1)S(1)} %pad_maximum_fusion.1.w0), channel_id=1, source_target_pairs={{0,16},{8,24},{16,0},{24,8},{1,17},{9,25},{17,1},{25,9},{2,18},{10... | collective-permute-start | bytes 1376264 | tf_op jit(solution)/shard_map/ppermute | solution.py:319
  94.7 25.9 %collective-permute-start.5 = (bf16[448,512]{1,0:T(8,128)(2,1)S(1)}, bf16[448,512]{1,0:T(8,128)(2,1)S(1)}, u32[]{:S(2)}, u32[]{:S(2)}) collective-permute-start(bf16[448,512]{1,0:T(8,128)(2,1)S(1)} %pad_maximum_fusion.1.w0), channel_id=1, source_target_pairs={{0,24},{8,0},{16,8},{24,16},{1,25},{9,1},{17,9},{25,17},{2,26},{10... | collective-permute-start | bytes 1376264 | tf_op jit(solution)/shard_map/ppermute | solution.py:319
  122.5 17.2 %all-to-all-start.6 = ((bf16[32,8,640]{2,1,0:T(8,128)(2,1)}), bf16[32,8,640]{2,1,0:T(8,128)(2,1)S(1)}, u32[]{:S(2)}, u32[]{:S(2)}) async-start(bf16[32,8,640]{2,1,0:T(8,128)(2,1)} %bitcast.23), calls=%async_computation.6 | async-start | bytes 655360 | tf_op jit(solution)/shard_map/all_to_all | solution.py:28
  141.4 11.2 %all-to-all-start.7 = ((bf16[32,8,128]{2,1,0:T(8,128)(2,1)}), bf16[32,8,128]{2,1,0:T(8,128)(2,1)S(1)}, u32[]{:S(2)}, u32[]{:S(2)}) async-start(bf16[32,8,128]{2,1,0:T(8,128)(2,1)} %get-tuple-element.29), calls=%async_computation.7 | async-start | bytes 131072 | tf_op jit(solution)/shard_map/all_to_all | solution.py:28
  154.1 16.7 %all-to-all-start.8 = ((bf16[16,4,512]{2,1,0:T(4,128)(2,1)}), bf16[16,4,512]{2,1,0:T(4,128)(2,1)S(1)}, u32[]{:S(2)}, u32[]{:S(2)}) async-start(bf16[16,4,512]{2,1,0:T(4,128)(2,1)} %shard_map.181), calls=%async_computation.8 | async-start | bytes 131072 | tf_op jit(solution)/shard_map/all_to_all | solution.py:28
  (3 other events, 11.9 us)

commit v4 on v3

--- a/solution.py
+++ b/solution.py
@@ -10,7 +10,6 @@
 D = 4096
 HEADS = 128
 HEAD_DIM = 64
-STATE = 128
 GROUPS = 16
 CONV = 4
 NEW = 4
@@ -99,7 +98,7 @@
     stacked = jnp.concatenate([w[384:448] for w in pieces], axis=0)
     vector_w = mm(one_hot(256, 256, source), stacked).astype(bf16)
     vector = mm_t(normed, vector_w).astype(bf16)
-    extra = step_lanes(at_ref, normed, squares, step_ref[0]).astype(bf16)
+    extra = step_lanes(at_ref, normed, squares, step_ref[1]).astype(bf16)
     for k, w in enumerate(pieces):
         to = (y - k) % YN
         for n in range(2):
@@ -150,11 +149,11 @@
     return x * jax.nn.sigmoid(x)
 
 
-def lengths_column(len_ref):
+def lengths_column(at_ref):
     row = lax.broadcasted_iota(jnp.int32, (8, 1), 0)
     lens = jnp.zeros((8, 1), jnp.int32)
     for s in range(SEQ):
-        lens = jnp.where(row == s, len_ref[s], lens)
+        lens = jnp.where(row == s, at_ref[3 + s], lens)
     return lens
 
 
@@ -168,21 +167,104 @@
     return jnp.where(i < 3, 8 * (n % NEW) + n // NEW, -1)
 
 
-def conv(history_ref, fresh, taps_ref):
-    rows = [history_ref[k].astype(f32) for k in range(CONV - 1)]
+def conv(history_ref, fresh, taps_ref, layer):
+    rows = [history_ref[layer, k].astype(f32) for k in range(CONV - 1)]
     rows += [fresh[8 * t : 8 * t + 8] for t in range(NEW)]
-    taps = [taps_ref[k : k + 1].astype(f32) for k in range(CONV)]
+    taps = [taps_ref[layer, k : k + 1].astype(f32) for k in range(CONV)]
     return [silu(sum(rows[t + k] * taps[k] for k in range(CONV))) for t in range(NEW)]
+
+
+def prepare(
+    token_hbm,
+    weight_hbm,
+    history_hbm,
+    taps_hbm,
+    out_ref,
+    token_ref,
+    weight_ref,
+    history_ref,
+    taps_ref,
+    stack_ref,
+    sems,
+):
+    moves = [
+        pltpu.make_async_copy(source, target, sems.at[n])
+        for n, (source, target) in enumerate(
+            (
+                (history_hbm, history_ref),
+                (taps_hbm, taps_ref),
+                (token_hbm, token_ref),
+                (weight_hbm, weight_ref),
+            )
+        )
+    ]
+    for move in moves:
+        move.start()
+    for move in moves[:3]:
+        move.wait()
+    stack_ref[...] = jnp.zeros((128, 32), f32)
+    at = 0
+    for layer in range(LAYERS):
+        for s in range(SEQ):
+            for k in range(CONV - 1):
+                stack_ref[at : at + 2] = history_ref[layer, s, k].astype(f32)
+                at += 2
+    for layer in range(LAYERS):
+        for k in range(CONV):
+            stack_ref[at : at + 2] = taps_ref[layer, k].astype(f32)
+            at += 2
+    turned = jnp.transpose(stack_ref[...])
+    tokens = jnp.concatenate([token_ref[...].astype(f32), jnp.zeros((1, 512), f32)], axis=0)
+    row, _ = row_col((4, 512))
+    for g in range(GROUPS):
+        both = [turned[g : g + 1], turned[GROUPS + g : GROUPS + g + 1], jnp.zeros((1, 256), f32)]
+        tail = jnp.broadcast_to(jnp.concatenate(both, axis=1), (4, 512))
+        out_ref[g, 0] = jnp.where(row == 3, tail, tokens).astype(bf16)
+
+    def source(col):
+        c = col % 32
+        return 4 * (c % GROUPS) + 2 * (col // 32) + c // GROUPS
+
+    order = one_hot(64, 64, source)
+    moves[3].wait()
+    for layer in range(LAYERS):
+        cols = weight_ref[layer].reshape(64, 512)
+        out_ref[:, 1 + layer] = mm(order, cols).astype(bf16).reshape(GROUPS, 4, 512)
+
+
+def unpack(plane_ref, vhist_ref, vtaps_ref):
+    def source(col):
+        return jnp.where(col % 8 == 3, 4 * ((col // 8) % ZN) + col // 128, -1)
+
+    small = mm(one_hot(64, 512, source), plane_ref[:, 0:256])
+    spread = jnp.zeros((128, 128), f32)
+    row, col = row_col((64, 128))
+    for nl in range(2):
+        turned = jnp.transpose(small[:, 128 * nl : 128 * nl + 128]).astype(bf16)
+        spread += mm(turned, jnp.where(col == 2 * row + nl, 1.0, 0.0).astype(bf16))
+
+    def order(m):
+        kind = m // 2
+        old = 24 * (2 * (m // 36) + m % 2) + 8 * (kind % 3) + (kind // 3) % SEQ
+        tap = 96 + 8 * (2 * ((m - 72) // 8) + m % 2) + (kind - 36) % CONV
+        return jnp.where(m < 72, old, jnp.where(m < 88, tap, -1))
+
+    rows = mm(one_hot(128, 128, order), spread.astype(bf16)).astype(bf16)
+    for layer in range(LAYERS):
+        for rw in range(2):
+            lanes = slice(128 * rw, 128 * rw + 128)
+            for k in range(CONV - 1):
+                at = 24 * (2 * layer + rw) + 8 * k
+                vhist_ref[layer, k, :, lanes] = rows[at : at + 8]
+            at = 96 + 8 * (2 * layer + rw)
+            vtaps_ref[layer, :, lanes] = rows[at : at + 8]
 
 
 def middle(
     at_ref,
-    len_ref,
-    bias_ref,
-    rate_ref,
+    scale_ref,
     part_ref,
     history_ref,
-    taps_ref,
     vhist_ref,
     vtaps_ref,
     state_ref,
@@ -215,10 +297,10 @@
     first = jnp.sum(jnp.where(lane == head, tail, 0.0), axis=1, keepdims=True)
     second = jnp.sum(jnp.where(lane == head + 1, tail, 0.0), axis=1, keepdims=True)
     left = lane < HEAD_DIM
-    raw = jnp.where(left, first + bias_ref[layer, 0], second + bias_ref[layer, 1])
-    rate = jnp.where(left[:8], rate_ref[layer, 0], rate_ref[layer, 1])
+    raw = jnp.where(left, first + scale_ref[2 * layer], second + scale_ref[2 * layer + 1])
+    rate = jnp.where(left[:8], scale_ref[4 + 2 * layer], scale_ref[5 + 2 * layer])
     soft = jnp.maximum(raw, 0.0) + jnp.log1p(jnp.exp(-jnp.abs(raw)))
-    lens = lengths_column(len_ref)
+    lens = lengths_column(at_ref)
     live = [jnp.where(lens > t, 1.0, 0.0) for t in range(NEW)]
     step = [soft[8 * t : 8 * t + 8] * live[t] for t in range(NEW)]
     cumulative = []
@@ -226,8 +308,8 @@
         grown = step[t] * rate
         cumulative.append(grown if t == 0 else cumulative[-1] + grown)
 
-    values = conv(history_ref, rows[:, 128:256], taps_ref)
-    vectors = conv(vhist_ref, rows[:, 256:512], vtaps_ref)
+    values = conv(history_ref, rows[:, 128:256], history_ref.at[:, 3], layer)
+    vectors = conv(vhist_ref, rows[:, 256:512], vtaps_ref, layer)
     write = [v[:, 0:128] for v in vectors]
     read = [v[:, 128:256] for v in vectors]
     stepped = [values[t] * step[t] for t in range(NEW)]
@@ -236,7 +318,7 @@
     row, _ = row_col((32, 128))
     carried = jnp.zeros((32, 128), f32)
     for s in range(SEQ):
-        carried = jnp.where(row % 8 == s, mm_t(reads, state_ref[s].astype(bf16)), carried)
+        carried = jnp.where(row % 8 == s, mm_t(reads, state_ref[layer, s].astype(bf16)), carried)
 
     mixed = []
     for t in range(NEW):
@@ -263,7 +345,7 @@
 
 
 def finish(
-    len_ref,
+    at_ref,
     keep_ref,
     write_ref,
     decay_ref,
@@ -274,6 +356,8 @@
     next_ref,
     value_ref,
     vector_ref,
+    *,
+    layer,
 ):
     kept = jnp.transpose(keep_ref[...])
     _, col = row_col(kept.shape)
@@ -283,13 +367,13 @@
         for h in range(2):
             at = slice(HEAD_DIM * h, HEAD_DIM * h + HEAD_DIM)
             decay = decay_ref[s : s + 1, HEAD_DIM * h : HEAD_DIM * h + 1]
-            next_ref[s, at] = state_ref[s, at] * decay + fresh[at]
-    lens = lengths_column(len_ref)
+            next_ref[s, at] = state_ref[layer, s, at] * decay + fresh[at]
+    lens = lengths_column(at_ref)
     for out_ref, old_ref, lo, hi in (
         (value_ref, history_ref, 0, 128),
         (vector_ref, vhist_ref, 128, 384),
     ):
-        rows = [old_ref[k].astype(f32) for k in range(CONV - 1)]
+        rows = [old_ref[layer, k].astype(f32) for k in range(CONV - 1)]
         rows += [fresh_ref[8 * t : 8 * t + 8, lo:hi].astype(f32) for t in range(NEW)]
         for k in range(CONV - 1):
             chosen = rows[k + 1]
@@ -313,11 +397,12 @@
     return results[0] if len(outs) == 1 else results
 
 
+def from_y(value, k):
+    return lax.ppermute(value, "y", [(i, (i + k) % YN) for i in range(YN)])
+
+
 def around_y(value):
-    pieces = [value]
-    for k in range(1, YN):
-        pieces.append(lax.ppermute(value, "y", [(i, (i + k) % YN) for i in range(YN)]))
-    return pieces
+    return [value, *(from_y(value, k) for k in range(1, YN))]
 
 
 def body(
@@ -340,28 +425,34 @@
     z = lax.axis_index("z")
     y = lax.axis_index("y")
     square_lane = (8 * z + 64) % HEADS
-    vector_cols = vector_weight.transpose(0, 2, 3, 1).reshape(2, 2, 2, GROUPS, 512)
-    vector_cols = vector_cols.transpose(3, 0, 1, 2, 4).reshape(GROUPS, 8, 512)
-    small = jnp.concatenate([vector_history.reshape(72, 32), vector_taps.reshape(16, 32)], axis=0)
-    small = small.reshape(88, 2, GROUPS).transpose(2, 1, 0).reshape(GROUPS, 1, 176)
-    small = jnp.pad(small, ((0, 0), (0, 0), (0, 512 - 176)))
-    first = jnp.concatenate([copies(tokens, ZN), small], axis=1).reshape(ZN, 1, 4, 512)
-    first = jnp.concatenate([first, vector_cols.reshape(ZN, 2, 4, 512)], axis=1)
-    at = jnp.stack([z, y, square_lane]).astype(jnp.int32)
-    first, own_out = lax.optimization_barrier((first, out_weight[0]))
+    first = pl.pallas_call(
+        prepare,
+        out_shape=jax.ShapeDtypeStruct((ZN, 3, 4, 512), bf16),
+        in_specs=[pl.BlockSpec(memory_space=pltpu.MemorySpace.HBM)] * 4,
+        out_specs=pl.BlockSpec(memory_space=pltpu.VMEM),
+        scratch_shapes=[
+            pltpu.VMEM((3, 512), bf16),
+            pltpu.VMEM((2, 2, 32, 512), bf16),
+            pltpu.VMEM((2, SEQ, 3, 2, 32), bf16),
+            pltpu.VMEM((2, CONV, 2, 32), bf16),
+            pltpu.VMEM((128, 32), f32),
+            pltpu.SemaphoreType.DMA((4,)),
+        ],
+    )(tokens, vector_weight.transpose(0, 2, 3, 1), vector_history, vector_taps)
+    first, own_out = lax.optimization_barrier((first, out_weight))
     first = exchange(first, "z")
-    own_out = around_y(own_out)
-    plane = exchange(copies(first[:, :2], YN), "y").reshape(YN, ZN, 8, 512)
-
-    small = plane[:, :, 3, :176].reshape(YN, ZN, 2, 88).transpose(3, 1, 0, 2).reshape(88, 128)
-    vhist = small[:72].reshape(2, SEQ, 3, 256).transpose(0, 2, 1, 3)
-    vhist = jnp.pad(vhist, ((0, 0), (0, 0), (0, 2), (0, 0)))
-    vtaps = small[72:].reshape(2, CONV, 256)
-    history = jnp.pad(value_history.transpose(0, 2, 1, 3), ((0, 0), (0, 0), (0, 2), (0, 0)))
-    states = [recurrent_state[layer].reshape(SEQ, 128, 128) for layer in range(LAYERS)]
+    at = jnp.concatenate([jnp.stack([z, y, square_lane]), lengths]).astype(jnp.int32)
+    scale = jnp.concatenate([step_bias.reshape(4), decay_rate.reshape(4)])
+    own_out = around_y(own_out[0])
+    plane = exchange(copies(first[:, :2], YN), "y").reshape(512, 512)
+    vhist, vtaps = call(unpack, [((2, 3, 8, 256), bf16), ((2, 8, 256), bf16)], 0, plane)
+    history = jnp.pad(value_history.transpose(0, 2, 1, 3), ((0, 0), (0, 1), (0, 2), (0, 0)))
+    history += jnp.pad(value_taps[:, None], ((0, 0), (3, 0), (0, 4), (0, 0)))
+    gain = jnp.pad(norm_gain, ((0, 6), (0, 0)))
+    states = recurrent_state.reshape(LAYERS, SEQ, 128, 128)
 
     def mid(part, layer):
-        old = (history[layer], vhist[layer])
+        old = (history, vhist)
         msg, keep, write, decay, fresh = call(
             functools.partial(middle, layer=layer),
             [
@@ -371,29 +462,26 @@
                 ((8, 128), f32),
                 ((32, 384), bf16),
             ],
-            4,
+            2,
             at,
-            lengths,
-            step_bias,
-            decay_rate,
+            scale,
             part,
-            history[layer],
-            value_taps[layer],
-            vhist[layer],
-            vtaps[layer],
-            states[layer],
+            history,
+            vhist,
+            vtaps,
+            states,
         )
         after = call(
-            finish,
+            functools.partial(finish, layer=layer),
             [((SEQ, 128, 128), f32), ((3, 8, 128), bf16), ((3, 8, 256), bf16)],
             1,
-            lengths,
+            at,
             keep,
             write,
             decay,
             fresh,
             *old,
-            states[layer],
+            states,
         )
         return exchange(msg, ("y", "dp")).reshape(YN, DN * 8, 128), after
 
@@ -402,11 +490,11 @@
         [((DN, 24, COLS), bf16)],
         1,
         at,
-        plane.reshape(512, 512),
-        norm_gain,
-        gate_weight[:1],
-        value_weight[:1],
-        step_weight[:1],
+        plane,
+        gain,
+        gate_weight,
+        value_weight,
+        step_weight,
     )
     part = exchange(part, "dp")
     mixed, (state0, value0, vector0) = mid(part, 0)
@@ -433,19 +521,23 @@
     )
     update, later = lax.optimization_barrier((update, later))
     update = exchange(update, "z")
-    later = around_y(later)
+    pieces = [later, from_y(later, 1), from_y(later, 2)]
     update = jnp.sum(update.astype(f32), axis=0)[:3]
     token_rows = (tokens.astype(f32) + update).astype(bf16)
-
-    quarter = exchange(copies(jnp.pad(token_rows, ((0, 1), (0, 0))), ZN), "z").reshape(64, 512)
+    quarter = copies(jnp.pad(token_rows, ((0, 1), (0, 0))), ZN)
+    quarter, last = lax.optimization_barrier((quarter, later))
+    quarter = exchange(quarter, "z")
+    last = from_y(last, 3)
+    quarter = quarter.reshape(64, 512)
+    later = [*pieces, last]
     part = call(
         second_projection,
         [((YN, 64, COLS), bf16)],
         1,
         at,
         quarter,
-        norm_gain,
-        step_weight[1:],
+        gain,
+        step_weight,
         *later,
     )
     part = exchange(part.reshape(YN * DN, 8, COLS), ("y", "dp")).reshape(YN, DN, 8, COLS)

time: 173 us -> 168 us (0.971)
  local copies, waits for them, and re-layouts: 16.2 us -> 8.97 us
  waiting for transfers between devices: 42 us -> 46.2 us
  blocking collectives: 20 us -> 17.3 us
  Pallas kernels: 11.9 us -> 14.2 us
    all_to_all x8, waiting for transfers between devices: 42 us -> 46.2 us  [exchange(): return lax.all_to_all(pieces, axis, 0, 0, tiled=True)]
    reshape x5, local copies, waits for them, and re-layouts: 4.17 us -> 1.03 us  [the longest x1 0.73 us: lanes(): return w.reshape(4, 128, 128).transpose(1, 0, 2).reshape(128, 512)]
    slice x8 -> x3, local copies, waits for them, and re-layouts: 4.08 us -> 0.95 us  [the longest x2 0.9 us: body(): gate_weight[1]]
    all_to_all x1, blocking collectives: 20 us -> 17.3 us  [exchange(): return lax.all_to_all(pieces, axis, 0, 0, tiled=True)]
    unnamed x30 -> x34, local copies, waits for them, and re-layouts: 1.48 us -> 3.9 us
    pallas_call x0 -> x1, Pallas kernels: none -> 1.83 us  [body(): pl.pallas_call(prepare, out_shape=jax.ShapeDtypeStruct((ZN, 3, 4, 512), b...]
    concatenate x4 -> x0, local copies, waits for them, and re-layouts: 1.79 us -> none  [body(): jnp.concatenate([vector_history.reshape(72, 32), vector_taps.reshape(16,...]
    pallas_call x8 -> x9, Pallas kernels: 11.9 us -> 12.3 us  [call(): pl.pallas_call(kernel, out_shape=outs, in_specs=space, out_specs=[vmem] *...]
  transfers between devices with their start and end apart: 14 -> 14, of which waited for: 7 -> 8; matrix products, arithmetic and copies ran while one was open for 7% -> 2% of each run, Pallas kernels for 3% -> 3%
where the time goes in v4:
time: 168 us; the launch traced here: 167 us
  starting transfers between devices  77.7 us (46%)
  waiting for transfers between devices  46.2 us (28%)
  blocking collectives  17.3 us (10%)
  Pallas kernels  14.2 us (8%)
  local copies, waits for them, and re-layouts  8.97 us (5%)
  other arithmetic  1.83 us (1%)
    all_to_all x8, starting transfers between devices, exchange(): return lax.all_to_all(pieces, axis, 0, 0, tiled=True)  58.3 us
    all_to_all x8, waiting for transfers between devices, exchange(): return lax.all_to_all(pieces, axis, 0, 0, tiled=True)  46.2 us
    ppermute x6, starting transfers between devices, from_y(): return lax.ppermute(value, 'y', [(i, (i + k) % YN) for i in range(YN)])  19.4 us
    all_to_all x1, blocking collectives, exchange(): return lax.all_to_all(pieces, axis, 0, 0, tiled=True)  17.3 us
    pallas_call x9, Pallas kernels, call(): pl.pallas_call(kernel, out_shape=outs, in_specs=space, out_specs=[vmem] *...  12.3 us
    unnamed x34, local copies, waits for them, and re-layouts  3.9 us
  transfers between devices with their start and end apart: 14, of which 8 were waited for; matrix products, arithmetic and copies ran while one was open for 2% of the time, Pallas kernels for 3%

profile of v4, /device:TPU:1, one launch (start us, length us, event | category | flops | bytes accessed | tf_op | source)
XLA Modules:
  0.0 167.2 jit_solution(3479624986449146858)
XLA Ops:
  0.6 1.8 %shard_map.174 = bf16[16,3,4,512]{3,2,1,0:T(4,128)(2,1)} custom-call(bf16[3,512]{1,0:T(4,128)(2,1)} %token_hbm.1, bf16[2,2,32,512]{3,2,1,0:T(8,128)(2,1)} %bitcast.55, bf16[2,6,3,2,32]{4,3,2,1,0:T(2,128)(2,1)} %history_hbm.1, bf16[2,4,2,32]{3,2,1,0:T(2,128)(2,1)} %taps_hbm.1), custom_call_target="tpu_custom_call" | custom-call | tf_op jit(solution)/shard_map/pallas_call | solution.py:428
  2.5 15.9 %all-to-all-start = ((bf16[16,3,4,512]{3,2,1,0:T(4,128)(2,1)}), bf16[16,3,4,512]{3,2,1,0:T(4,128)(2,1)S(1)}, u32[]{:S(2)}, u32[]{:S(2)}) async-start(bf16[16,3,4,512]{3,2,1,0:T(4,128)(2,1)} %shard_map.174), calls=%async_computation | async-start | bytes 393216 | tf_op jit(solution)/shard_map/all_to_all | solution.py:27
  18.4 3.2 %collective-permute-start = (bf16[128,512]{1,0:T(8,128)(2,1)S(1)}, bf16[128,512]{1,0:T(8,128)(2,1)S(1)}, u32[]{:S(2)}, u32[]{:S(2)}) collective-permute-start(bf16[128,512]{1,0:T(8,128)(2,1)S(1)} %slice_bitcast_fusion.1.w0), channel_id=1, source_target_pairs={{0,8},{8,16},{16,24},{24,0},{1,9},{9,17},{17,25},{25,1},{2,10},{10... | collective-permute-start | bytes 393224 | tf_op jit(solution)/shard_map/ppermute | solution.py:401
  21.6 4.5 %collective-permute-start.1 = (bf16[128,512]{1,0:T(8,128)(2,1)S(1)}, bf16[128,512]{1,0:T(8,128)(2,1)S(1)}, u32[]{:S(2)}, u32[]{:S(2)}) collective-permute-start(bf16[128,512]{1,0:T(8,128)(2,1)S(1)} %slice_bitcast_fusion.1.w0), channel_id=1, source_target_pairs={{0,16},{8,24},{16,0},{24,8},{1,17},{9,25},{17,1},{25,9},{2,18},{10... | collective-permute-start | bytes 393224 | tf_op jit(solution)/shard_map/ppermute | solution.py:401
  26.1 3.0 %collective-permute-start.2 = (bf16[128,512]{1,0:T(8,128)(2,1)S(1)}, bf16[128,512]{1,0:T(8,128)(2,1)S(1)}, u32[]{:S(2)}, u32[]{:S(2)}) collective-permute-start(bf16[128,512]{1,0:T(8,128)(2,1)S(1)} %slice_bitcast_fusion.1.w0), channel_id=1, source_target_pairs={{0,24},{8,0},{16,8},{24,16},{1,25},{9,1},{17,9},{25,17},{2,26},{10... | collective-permute-start | bytes 393224 | tf_op jit(solution)/shard_map/ppermute | solution.py:401
  31.9 4.2 %all-to-all-start.1 = ((bf16[4,16,2,4,512]{4,3,2,1,0:T(4,128)(2,1)}), bf16[4,16,2,4,512]{4,3,2,1,0:T(4,128)(2,1)S(1)}, u32[]{:S(2)}, u32[]{:S(2)}) async-start(bf16[4,16,2,4,512]{4,3,2,1,0:T(4,128)(2,1)} %broadcast_in_dim.6), calls=%async_computation.1 | async-start | bytes 1048576 | tf_op jit(solution)/shard_map/all_to_all | solution.py:27
  43.2 1.9 %shard_map.175 = bf16[8,24,640]{2,1,0:T(8,128)(2,1)} custom-call(s32[9]{0:T(128)S(1)} %pad_add_fusion.1.at_ref, bf16[512,512]{1,0:T(8,128)(2,1)S(1)} %reshape.59.plane_ref, f32[8,512]{1,0:T(8,128)S(1)} %pad.16.gain_ref, bf16[2,512,128]{2,1,0:T(8,128)(2,1)S(1)} %copy-done.2, bf16[2,512,128]{2,1,0:T(8,128)(2,1)S(1)} %copy-done.3, ...), custom_call_target="tpu_custom_call" | custom-call | tf_op jit(solution)/shard_map/pallas_call | solution.py:390
  45.1 10.7 %all-to-all-start.2 = ((bf16[8,24,640]{2,1,0:T(8,128)(2,1)}), bf16[8,24,640]{2,1,0:T(8,128)(2,1)S(1)}, u32[]{:S(2)}, u32[]{:S(2)}) async-start(bf16[8,24,640]{2,1,0:T(8,128)(2,1)} %shard_map.175), calls=%async_computation.2 | async-start | bytes 491520 | tf_op jit(solution)/shard_map/all_to_all | solution.py:27
  56.5 5.6 %all-to-all-done.2.part_ref = bf16[8,24,640]{2,1,0:T(8,128)(2,1)S(1)} async-done(((bf16[8,24,640]{2,1,0:T(8,128)(2,1)}), bf16[8,24,640]{2,1,0:T(8,128)(2,1)S(1)}, u32[]{:S(2)}, u32[]{:S(2)}) %all-to-all-start.2) | async-done | bytes 245792 | tf_op jit(solution)/shard_map/all_to_all | solution.py:27
  63.8 5.1 %all-to-all-start.3 = ((bf16[32,8,128]{2,1,0:T(8,128)(2,1)}), bf16[32,8,128]{2,1,0:T(8,128)(2,1)S(1)}, u32[]{:S(2)}, u32[]{:S(2)}) async-start(bf16[32,8,128]{2,1,0:T(8,128)(2,1)} %get-tuple-element.31), calls=%async_computation.3 | async-start | bytes 131072 | tf_op jit(solution)/shard_map/all_to_all | solution.py:27
  69.0 7.2 %all-to-all-done.3 = bf16[32,8,128]{2,1,0:T(8,128)(2,1)S(1)} async-done(((bf16[32,8,128]{2,1,0:T(8,128)(2,1)}), bf16[32,8,128]{2,1,0:T(8,128)(2,1)S(1)}, u32[]{:S(2)}, u32[]{:S(2)}) %all-to-all-start.3) | async-done | bytes 65568 | tf_op jit(solution)/shard_map/all_to_all | solution.py:27
  77.6 6.0 %all-to-all-start.4 = ((bf16[16,4,512]{2,1,0:T(4,128)(2,1)}), bf16[16,4,512]{2,1,0:T(4,128)(2,1)S(1)}, u32[]{:S(2)}, u32[]{:S(2)}) async-start(bf16[16,4,512]{2,1,0:T(4,128)(2,1)} %shard_map.178), calls=%async_computation.4 | async-start | bytes 131072 | tf_op jit(solution)/shard_map/all_to_all | solution.py:27
  83.6 2.2 %collective-permute-start.3 = (bf16[448,512]{1,0:T(8,128)(2,1)S(1)}, bf16[448,512]{1,0:T(8,128)(2,1)S(1)}, u32[]{:S(2)}, u32[]{:S(2)}) collective-permute-start(bf16[448,512]{1,0:T(8,128)(2,1)S(1)} %pad_maximum_fusion.1.w0), channel_id=1, source_target_pairs={{0,8},{8,16},{16,24},{24,0},{1,9},{9,17},{17,25},{25,1},{2,10},{10... | collective-permute-start | bytes 1376264 | tf_op jit(solution)/shard_map/ppermute | solution.py:401
  85.9 3.6 %collective-permute-start.4 = (bf16[448,512]{1,0:T(8,128)(2,1)S(1)}, bf16[448,512]{1,0:T(8,128)(2,1)S(1)}, u32[]{:S(2)}, u32[]{:S(2)}) collective-permute-start(bf16[448,512]{1,0:T(8,128)(2,1)S(1)} %pad_maximum_fusion.1.w0), channel_id=1, source_target_pairs={{0,16},{8,24},{16,0},{24,8},{1,17},{9,25},{17,1},{25,9},{2,18},{10... | collective-permute-start | bytes 1376264 | tf_op jit(solution)/shard_map/ppermute | solution.py:401
  89.5 5.7 %all-to-all-done.4 = bf16[16,4,512]{2,1,0:T(4,128)(2,1)S(1)} async-done(((bf16[16,4,512]{2,1,0:T(4,128)(2,1)}), bf16[16,4,512]{2,1,0:T(4,128)(2,1)S(1)}, u32[]{:S(2)}, u32[]{:S(2)}) %all-to-all-start.4) | async-done | bytes 65568 | tf_op jit(solution)/shard_map/all_to_all | solution.py:27
  95.3 2.8 %collective-permute-start.5 = (bf16[448,512]{1,0:T(8,128)(2,1)S(1)}, bf16[448,512]{1,0:T(8,128)(2,1)S(1)}, u32[]{:S(2)}, u32[]{:S(2)}) collective-permute-start(bf16[448,512]{1,0:T(8,128)(2,1)S(1)} %pad_maximum_fusion.1.w0), channel_id=1, source_target_pairs={{0,24},{8,0},{16,8},{24,16},{1,25},{9,1},{17,9},{25,17},{2,26},{10... | collective-permute-start | bytes 1376264 | tf_op jit(solution)/shard_map/ppermute | solution.py:401
  98.1 17.3 %all_to_all.45 = bf16[16,4,512]{2,1,0:T(4,128)(2,1)S(1)} all-to-all(bf16[16,4,512]{2,1,0:T(4,128)(2,1)S(1)} %broadcast_in_dim.8), channel_id=1, replica_groups=mesh['z'=16,'y'=4,'dp'=8] {'z'}, dimensions={0} | all-to-all | bytes 131072 | tf_op jit(solution)/shard_map/all_to_all | solution.py:27
  115.4 1.9 %shard_map.179 = bf16[4,64,640]{2,1,0:T(8,128)(2,1)} custom-call(s32[9]{0:T(128)S(1)} %pad_add_fusion.1.at_ref, bf16[64,512]{1,0:T(8,128)(2,1)S(1)} %reshape.64.rows_ref, f32[8,512]{1,0:T(8,128)S(1)} %pad.16.gain_ref, bf16[2,512,128]{2,1,0:T(8,128)(2,1)S(1)} %copy-done.1, bf16[448,512]{1,0:T(8,128)(2,1)S(1)} %pad_maximum_fusion.1.w0, ...), custom_call_target="tpu_custom_call" | custom-call | tf_op jit(solution)/shard_map/pallas_call | solution.py:390
  117.3 7.7 %all-to-all-start.6 = ((bf16[32,8,640]{2,1,0:T(8,128)(2,1)}), bf16[32,8,640]{2,1,0:T(8,128)(2,1)S(1)}, u32[]{:S(2)}, u32[]{:S(2)}) async-start(bf16[32,8,640]{2,1,0:T(8,128)(2,1)} %bitcast.14), calls=%async_computation.6 | async-start | bytes 655360 | tf_op jit(solution)/shard_map/all_to_all | solution.py:27
  125.8 8.7 %all-to-all-done.6 = bf16[32,8,640]{2,1,0:T(8,128)(2,1)S(1)} async-done(((bf16[32,8,640]{2,1,0:T(8,128)(2,1)}), bf16[32,8,640]{2,1,0:T(8,128)(2,1)S(1)}, u32[]{:S(2)}, u32[]{:S(2)}) %all-to-all-start.6) | async-done | bytes 327712 | tf_op jit(solution)/shard_map/all_to_all | solution.py:27
  136.2 3.7 %all-to-all-start.7 = ((bf16[32,8,128]{2,1,0:T(8,128)(2,1)}), bf16[32,8,128]{2,1,0:T(8,128)(2,1)S(1)}, u32[]{:S(2)}, u32[]{:S(2)}) async-start(bf16[32,8,128]{2,1,0:T(8,128)(2,1)} %get-tuple-element.37), calls=%async_computation.7 | async-start | bytes 131072 | tf_op jit(solution)/shard_map/all_to_all | solution.py:27
  141.5 5.8 %all-to-all-done.7 = bf16[32,8,128]{2,1,0:T(8,128)(2,1)S(1)} async-done(((bf16[32,8,128]{2,1,0:T(8,128)(2,1)}), bf16[32,8,128]{2,1,0:T(8,128)(2,1)S(1)}, u32[]{:S(2)}, u32[]{:S(2)}) %all-to-all-start.7) | async-done | bytes 65568 | tf_op jit(solution)/shard_map/all_to_all | solution.py:27
  148.9 5.1 %all-to-all-start.8 = ((bf16[16,4,512]{2,1,0:T(4,128)(2,1)}), bf16[16,4,512]{2,1,0:T(4,128)(2,1)S(1)}, u32[]{:S(2)}, u32[]{:S(2)}) async-start(bf16[16,4,512]{2,1,0:T(4,128)(2,1)} %shard_map.183), calls=%async_computation.8 | async-start | bytes 131072 | tf_op jit(solution)/shard_map/all_to_all | solution.py:27
  155.5 10.0 %all-to-all-done.8 = bf16[16,4,512]{2,1,0:T(4,128)(2,1)S(1)} async-done(((bf16[16,4,512]{2,1,0:T(4,128)(2,1)}), bf16[16,4,512]{2,1,0:T(4,128)(2,1)S(1)}, u32[]{:S(2)}, u32[]{:S(2)}) %all-to-all-start.8) | async-done | bytes 65568 | tf_op jit(solution)/shard_map/all_to_all | solution.py:27
  (86 shorter events, 22.4 us)
Async XLA Ops:
  2.5 15.9 %copy-start.8 = (bf16[2,128,512]{2,1,0:T(8,128)(2,1)S(1)}, bf16[2,128,512]{2,1,0:T(8,128)(2,1)}, u32[]{:S(2)}) copy-start(bf16[2,128,512]{2,1,0:T(8,128)(2,1)} %param.26) | copy-start | bytes 786436
  2.5 28.4 %all-to-all-start = ((bf16[16,3,4,512]{3,2,1,0:T(4,128)(2,1)}), bf16[16,3,4,512]{3,2,1,0:T(4,128)(2,1)S(1)}, u32[]{:S(2)}, u32[]{:S(2)}) async-start(bf16[16,3,4,512]{3,2,1,0:T(4,128)(2,1)} %shard_map.174), calls=%async_computation | async-start | bytes 393216 | tf_op jit(solution)/shard_map/all_to_all | solution.py:27
  18.4 50.6 %collective-permute-start = (bf16[128,512]{1,0:T(8,128)(2,1)S(1)}, bf16[128,512]{1,0:T(8,128)(2,1)S(1)}, u32[]{:S(2)}, u32[]{:S(2)}) collective-permute-start(bf16[128,512]{1,0:T(8,128)(2,1)S(1)} %slice_bitcast_fusion.1.w0), channel_id=1, source_target_pairs={{0,8},{8,16},{16,24},{24,0},{1,9},{9,17},{17,25},{25,1},{2,10},{10... | collective-permute-start | bytes 393224 | tf_op jit(solution)/shard_map/ppermute | solution.py:401
  21.6 47.4 %collective-permute-start.1 = (bf16[128,512]{1,0:T(8,128)(2,1)S(1)}, bf16[128,512]{1,0:T(8,128)(2,1)S(1)}, u32[]{:S(2)}, u32[]{:S(2)}) collective-permute-start(bf16[128,512]{1,0:T(8,128)(2,1)S(1)} %slice_bitcast_fusion.1.w0), channel_id=1, source_target_pairs={{0,16},{8,24},{16,0},{24,8},{1,17},{9,25},{17,1},{25,9},{2,18},{10... | collective-permute-start | bytes 393224 | tf_op jit(solution)/shard_map/ppermute | solution.py:401
  26.1 42.9 %collective-permute-start.2 = (bf16[128,512]{1,0:T(8,128)(2,1)S(1)}, bf16[128,512]{1,0:T(8,128)(2,1)S(1)}, u32[]{:S(2)}, u32[]{:S(2)}) collective-permute-start(bf16[128,512]{1,0:T(8,128)(2,1)S(1)} %slice_bitcast_fusion.1.w0), channel_id=1, source_target_pairs={{0,24},{8,0},{16,8},{24,16},{1,25},{9,1},{17,9},{25,17},{2,26},{10... | collective-permute-start | bytes 393224 | tf_op jit(solution)/shard_map/ppermute | solution.py:401
  31.9 11.1 %all-to-all-start.1 = ((bf16[4,16,2,4,512]{4,3,2,1,0:T(4,128)(2,1)}), bf16[4,16,2,4,512]{4,3,2,1,0:T(4,128)(2,1)S(1)}, u32[]{:S(2)}, u32[]{:S(2)}) async-start(bf16[4,16,2,4,512]{4,3,2,1,0:T(4,128)(2,1)} %broadcast_in_dim.6), calls=%async_computation.1 | async-start | bytes 1048576 | tf_op jit(solution)/shard_map/all_to_all | solution.py:27
  41.6 1.5 copy-start.1
  41.6 1.5 copy-start.2
  41.6 1.5 copy-start.3
  43.1 12.6 %copy-start.12 = (bf16[2,4,128]{2,1,0:T(4,128)(2,1)S(1)}, bf16[2,4,128]{2,1,0:T(4,128)(2,1)}, u32[]{:S(2)}) copy-start(bf16[2,4,128]{2,1,0:T(4,128)(2,1)} %param.24) | copy-start | bytes 6148
  45.0 17.0 %copy-start = (f32[2,6,2,64,128]{4,3,2,1,0:T(8,128)S(1)}, f32[2,6,2,64,128]{4,3,2,1,0:T(8,128)}, u32[]{:S(2)}) copy-start(f32[2,6,2,64,128]{4,3,2,1,0:T(8,128)} %param.27) | copy-start | bytes 2359300
  45.1 17.0 %all-to-all-start.2 = ((bf16[8,24,640]{2,1,0:T(8,128)(2,1)}), bf16[8,24,640]{2,1,0:T(8,128)(2,1)S(1)}, u32[]{:S(2)}, u32[]{:S(2)}) async-start(bf16[8,24,640]{2,1,0:T(8,128)(2,1)} %shard_map.175), calls=%async_computation.2 | async-start | bytes 491520 | tf_op jit(solution)/shard_map/all_to_all | solution.py:27
  62.1 6.9 %copy-start.7 = (bf16[128,512]{1,0:T(8,128)(2,1)S(1)}, bf16[128,512]{1,0:T(8,128)(2,1)}, u32[]{:S(2)}) copy-start(bf16[128,512]{1,0:T(8,128)(2,1)} %get-tuple-element.65) | copy-start | bytes 393220
  63.8 5.2 %copy-start.6 = (bf16[128,512]{1,0:T(8,128)(2,1)S(1)}, bf16[128,512]{1,0:T(8,128)(2,1)}, u32[]{:S(2)}) copy-start(bf16[128,512]{1,0:T(8,128)(2,1)} %get-tuple-element.64) | copy-start | bytes 393220
  63.8 12.5 %all-to-all-start.3 = ((bf16[32,8,128]{2,1,0:T(8,128)(2,1)}), bf16[32,8,128]{2,1,0:T(8,128)(2,1)S(1)}, u32[]{:S(2)}, u32[]{:S(2)}) async-start(bf16[32,8,128]{2,1,0:T(8,128)(2,1)} %get-tuple-element.31), calls=%async_computation.3 | async-start | bytes 131072 | tf_op jit(solution)/shard_map/all_to_all | solution.py:27
  77.6 17.6 %all-to-all-start.4 = ((bf16[16,4,512]{2,1,0:T(4,128)(2,1)}), bf16[16,4,512]{2,1,0:T(4,128)(2,1)S(1)}, u32[]{:S(2)}, u32[]{:S(2)}) async-start(bf16[16,4,512]{2,1,0:T(4,128)(2,1)} %shard_map.178), calls=%async_computation.4 | async-start | bytes 131072 | tf_op jit(solution)/shard_map/all_to_all | solution.py:27
  83.6 11.6 %copy-start.9 = (bf16[3,512]{1,0:T(4,128)(2,1)S(1)}, bf16[3,512]{1,0:T(4,128)(2,1)}, u32[]{:S(2)}) copy-start(bf16[3,512]{1,0:T(4,128)(2,1)} %token_hbm.1) | copy-start | bytes 9220
  83.6 31.8 %collective-permute-start.3 = (bf16[448,512]{1,0:T(8,128)(2,1)S(1)}, bf16[448,512]{1,0:T(8,128)(2,1)S(1)}, u32[]{:S(2)}, u32[]{:S(2)}) collective-permute-start(bf16[448,512]{1,0:T(8,128)(2,1)S(1)} %pad_maximum_fusion.1.w0), channel_id=1, source_target_pairs={{0,8},{8,16},{16,24},{24,0},{1,9},{9,17},{17,25},{25,1},{2,10},{10... | collective-permute-start | bytes 1376264 | tf_op jit(solution)/shard_map/ppermute | solution.py:401
  85.9 29.5 %collective-permute-start.4 = (bf16[448,512]{1,0:T(8,128)(2,1)S(1)}, bf16[448,512]{1,0:T(8,128)(2,1)S(1)}, u32[]{:S(2)}, u32[]{:S(2)}) collective-permute-start(bf16[448,512]{1,0:T(8,128)(2,1)S(1)} %pad_maximum_fusion.1.w0), channel_id=1, source_target_pairs={{0,16},{8,24},{16,0},{24,8},{1,17},{9,25},{17,1},{25,9},{2,18},{10... | collective-permute-start | bytes 1376264 | tf_op jit(solution)/shard_map/ppermute | solution.py:401
  95.3 20.1 %collective-permute-start.5 = (bf16[448,512]{1,0:T(8,128)(2,1)S(1)}, bf16[448,512]{1,0:T(8,128)(2,1)S(1)}, u32[]{:S(2)}, u32[]{:S(2)}) collective-permute-start(bf16[448,512]{1,0:T(8,128)(2,1)S(1)} %pad_maximum_fusion.1.w0), channel_id=1, source_target_pairs={{0,24},{8,0},{16,8},{24,16},{1,25},{9,1},{17,9},{25,17},{2,26},{10... | collective-permute-start | bytes 1376264 | tf_op jit(solution)/shard_map/ppermute | solution.py:401
  117.3 17.2 %all-to-all-start.6 = ((bf16[32,8,640]{2,1,0:T(8,128)(2,1)}), bf16[32,8,640]{2,1,0:T(8,128)(2,1)S(1)}, u32[]{:S(2)}, u32[]{:S(2)}) async-start(bf16[32,8,640]{2,1,0:T(8,128)(2,1)} %bitcast.14), calls=%async_computation.6 | async-start | bytes 655360 | tf_op jit(solution)/shard_map/all_to_all | solution.py:27
  136.2 11.1 %all-to-all-start.7 = ((bf16[32,8,128]{2,1,0:T(8,128)(2,1)}), bf16[32,8,128]{2,1,0:T(8,128)(2,1)S(1)}, u32[]{:S(2)}, u32[]{:S(2)}) async-start(bf16[32,8,128]{2,1,0:T(8,128)(2,1)} %get-tuple-element.37), calls=%async_computation.7 | async-start | bytes 131072 | tf_op jit(solution)/shard_map/all_to_all | solution.py:27
  147.3 7.3 %copy-start.5 = (f32[6,128,128]{2,1,0:T(8,128)S(1)}, f32[6,128,128]{2,1,0:T(8,128)}, u32[]{:S(2)}) copy-start(f32[6,128,128]{2,1,0:T(8,128)} %copy-done.4) | copy-start | bytes 1179652
  148.9 16.7 %all-to-all-start.8 = ((bf16[16,4,512]{2,1,0:T(4,128)(2,1)}), bf16[16,4,512]{2,1,0:T(4,128)(2,1)S(1)}, u32[]{:S(2)}, u32[]{:S(2)}) async-start(bf16[16,4,512]{2,1,0:T(4,128)(2,1)} %shard_map.183), calls=%async_computation.8 | async-start | bytes 131072 | tf_op jit(solution)/shard_map/all_to_all | solution.py:27
  (8 other events, 6.7 us)

commit v5 on v4

--- a/solution.py
+++ b/solution.py
@@ -57,7 +57,7 @@
     return jnp.where(lane == at_ref[2], squares, step)
 
 
-def first_projection(at_ref, plane_ref, gain_ref, gate_ref, value_ref, step_ref, out_ref):
+def first_projection(at_ref, plane_ref, misc_ref, gate_ref, value_ref, step_ref, out_ref):
     plane = plane_ref[...]
 
     def token_source(col):
@@ -71,7 +71,7 @@
 
     rows = mm(one_hot(192, 512, token_source), plane).astype(bf16)
     vector_w = mm(one_hot(256, 512, vector_source), plane).astype(bf16)
-    normed, squares = normed_rows(rows, gain_ref[0:1])
+    normed, squares = normed_rows(rows, gain_row(misc_ref, 0))
     parts = [
         mm(normed, gate_ref[0]),
         mm(normed, value_ref[0]),
@@ -85,9 +85,9 @@
         at += width
 
 
-def second_projection(at_ref, rows_ref, gain_ref, step_ref, w0, w1, w2, w3, out_ref):
+def second_projection(at_ref, rows_ref, misc_ref, step_ref, w0, w1, w2, w3, out_ref):
     y = at_ref[1]
-    normed, squares = normed_rows(rows_ref[...], gain_ref[1:2])
+    normed, squares = normed_rows(rows_ref[...], gain_row(misc_ref, 1))
     pieces = [w0, w1, w2, w3]
 
     def source(col):
@@ -95,19 +95,20 @@
         n = 8 * ((col // 4) % ZN) + 2 * ((y - col // 64) % YN) + j % 2
         return 128 * (j // 2) + n
 
-    stacked = jnp.concatenate([w[384:448] for w in pieces], axis=0)
+    stacked = jnp.concatenate(
+        [
+            jnp.concatenate([w[1024 + 64 * b : 1088 + 64 * b] for b in range(4)], axis=1)
+            for w in pieces
+        ],
+        axis=0,
+    )
     vector_w = mm(one_hot(256, 256, source), stacked).astype(bf16)
     vector = mm_t(normed, vector_w).astype(bf16)
-    extra = step_lanes(at_ref, normed, squares, step_ref[1]).astype(bf16)
+    extra = step_lanes(at_ref, normed, squares, step_ref[0]).astype(bf16)
     for k, w in enumerate(pieces):
         to = (y - k) % YN
         for n in range(2):
-            total = jnp.zeros((64, 128), f32)
-            for b in range(4):
-                total += mm(
-                    normed[:, 128 * b : 128 * b + 128],
-                    w[128 * n : 128 * n + 128, 128 * b : 128 * b + 128],
-                )
+            total = mm(normed, w[512 * n : 512 * n + 512])
             out_ref[to, :, 128 * n : 128 * n + 128] = total.astype(bf16)
         out_ref[to, :, 256:512] = vector
         out_ref[to, :, 512:640] = extra
@@ -149,14 +150,6 @@
     return x * jax.nn.sigmoid(x)
 
 
-def lengths_column(at_ref):
-    row = lax.broadcasted_iota(jnp.int32, (8, 1), 0)
-    lens = jnp.zeros((8, 1), jnp.int32)
-    for s in range(SEQ):
-        lens = jnp.where(row == s, at_ref[3 + s], lens)
-    return lens
-
-
 def place_first(col):
     return 8 * (col % NEW) + col // NEW
 
@@ -167,11 +160,77 @@
     return jnp.where(i < 3, 8 * (n % NEW) + n // NEW, -1)
 
 
-def conv(history_ref, fresh, taps_ref, layer):
-    rows = [history_ref[layer, k].astype(f32) for k in range(CONV - 1)]
-    rows += [fresh[8 * t : 8 * t + 8] for t in range(NEW)]
-    taps = [taps_ref[layer, k : k + 1].astype(f32) for k in range(CONV)]
+def conv(old, taps, fresh):
+    rows = old + [fresh[8 * t : 8 * t + 8] for t in range(NEW)]
     return [silu(sum(rows[t + k] * taps[k] for k in range(CONV))) for t in range(NEW)]
+
+
+def old_values(misc_ref, layer):
+    return [misc_ref[32 * layer + 8 * k : 32 * layer + 8 * k + 8] for k in range(CONV - 1)]
+
+
+def old_vectors(vhist_ref, layer):
+    return [vhist_ref[layer, k].astype(f32) for k in range(CONV - 1)]
+
+
+def setup(
+    len_ref,
+    gain_hbm,
+    bias_hbm,
+    rate_hbm,
+    taps_hbm,
+    history_hbm,
+    gate_hbm,
+    value_hbm,
+    misc_ref,
+    base_ref,
+    gain_ref,
+    bias_ref,
+    rate_ref,
+    taps_ref,
+    history_ref,
+    sems,
+):
+    pairs = (
+        (gain_hbm, gain_ref),
+        (bias_hbm, bias_ref),
+        (rate_hbm, rate_ref),
+        (taps_hbm, taps_ref),
+        (history_hbm, history_ref),
+        (gate_hbm.at[1], base_ref.at[0:512]),
+        (value_hbm.at[1], base_ref.at[512:1024]),
+    )
+    moves = [pltpu.make_async_copy(a, b, sems.at[n]) for n, (a, b) in enumerate(pairs)]
+    for move in moves:
+        move.start()
+    row, lane = row_col((8, 128))
+    lens = jnp.zeros((8, 128), f32)
+    for s in range(SEQ):
+        lens = jnp.where(row == s, len_ref[s].astype(f32), lens)
+    misc_ref[0:64] = jnp.zeros((64, 128), f32)
+    misc_ref[64:72] = lens
+    misc_ref[72:80] = jnp.zeros((8, 128), f32)
+    for move in moves:
+        move.wait()
+    left = lane[0:1] < HEAD_DIM
+    for layer in range(LAYERS):
+        for n, ref in enumerate((bias_ref, rate_ref)):
+            both = jnp.where(left, ref[layer : layer + 1, 0:1], ref[layer : layer + 1, 1:2])
+            misc_ref[72 + 2 * layer + n : 73 + 2 * layer + n] = both
+        for b in range(4):
+            part = gain_ref[layer : layer + 1, 128 * b : 128 * b + 128]
+            misc_ref[80 + 4 * layer + b : 81 + 4 * layer + b] = part
+        for k in range(CONV - 1):
+            at = 32 * layer + 8 * k
+            for s in range(SEQ):
+                misc_ref[at + s : at + s + 1] = history_ref[s, k, layer : layer + 1].astype(f32)
+        at = 32 * layer + 24
+        misc_ref[at : at + CONV] = taps_ref[layer].astype(f32)
+
+
+def gain_row(misc_ref, layer):
+    parts = [misc_ref[80 + 4 * layer + b : 81 + 4 * layer + b] for b in range(4)]
+    return jnp.concatenate(parts, axis=1)
 
 
 def prepare(
@@ -262,9 +321,8 @@
 
 def middle(
     at_ref,
-    scale_ref,
     part_ref,
-    history_ref,
+    misc_ref,
     vhist_ref,
     vtaps_ref,
     state_ref,
@@ -297,10 +355,11 @@
     first = jnp.sum(jnp.where(lane == head, tail, 0.0), axis=1, keepdims=True)
     second = jnp.sum(jnp.where(lane == head + 1, tail, 0.0), axis=1, keepdims=True)
     left = lane < HEAD_DIM
-    raw = jnp.where(left, first + scale_ref[2 * layer], second + scale_ref[2 * layer + 1])
-    rate = jnp.where(left[:8], scale_ref[4 + 2 * layer], scale_ref[5 + 2 * layer])
+    at = 72 + 2 * layer
+    raw = jnp.where(left, first, second) + misc_ref[at : at + 1]
+    rate = misc_ref[at + 1 : at + 2]
     soft = jnp.maximum(raw, 0.0) + jnp.log1p(jnp.exp(-jnp.abs(raw)))
-    lens = lengths_column(at_ref)
+    lens = misc_ref[64:72, 0:1]
     live = [jnp.where(lens > t, 1.0, 0.0) for t in range(NEW)]
     step = [soft[8 * t : 8 * t + 8] * live[t] for t in range(NEW)]
     cumulative = []
@@ -308,8 +367,11 @@
         grown = step[t] * rate
         cumulative.append(grown if t == 0 else cumulative[-1] + grown)
 
-    values = conv(history_ref, rows[:, 128:256], history_ref.at[:, 3], layer)
-    vectors = conv(vhist_ref, rows[:, 256:512], vtaps_ref, layer)
+    at = 32 * layer + 24
+    taps = [misc_ref[at + k : at + k + 1] for k in range(CONV)]
+    values = conv(old_values(misc_ref, layer), taps, rows[:, 128:256])
+    taps = [vtaps_ref[layer, k : k + 1].astype(f32) for k in range(CONV)]
+    vectors = conv(old_vectors(vhist_ref, layer), taps, rows[:, 256:512])
     write = [v[:, 0:128] for v in vectors]
     read = [v[:, 128:256] for v in vectors]
     stepped = [values[t] * step[t] for t in range(NEW)]
@@ -318,7 +380,7 @@
     row, _ = row_col((32, 128))
     carried = jnp.zeros((32, 128), f32)
     for s in range(SEQ):
-        carried = jnp.where(row % 8 == s, mm_t(reads, state_ref[layer, s].astype(bf16)), carried)
+        carried = jnp.where(row % 8 == s, mm_t(reads, state_ref[0, s].astype(bf16)), carried)
 
     mixed = []
     for t in range(NEW):
@@ -345,20 +407,17 @@
 
 
 def finish(
-    at_ref,
+    misc_ref,
     keep_ref,
     write_ref,
     decay_ref,
     fresh_ref,
-    history_ref,
     vhist_ref,
     state_ref,
-    next_ref,
-    value_ref,
-    vector_ref,
-    *,
+    *rest,
     layer,
 ):
+    next_ref, value_ref, vector_ref = rest[-3:]
     kept = jnp.transpose(keep_ref[...])
     _, col = row_col(kept.shape)
     write = write_ref[...].astype(bf16)
@@ -367,14 +426,13 @@
         for h in range(2):
             at = slice(HEAD_DIM * h, HEAD_DIM * h + HEAD_DIM)
             decay = decay_ref[s : s + 1, HEAD_DIM * h : HEAD_DIM * h + 1]
-            next_ref[s, at] = state_ref[layer, s, at] * decay + fresh[at]
-    lens = lengths_column(at_ref)
-    for out_ref, old_ref, lo, hi in (
-        (value_ref, history_ref, 0, 128),
-        (vector_ref, vhist_ref, 128, 384),
+            next_ref[0, s, at] = state_ref[0, s, at] * decay + fresh[at]
+    lens = misc_ref[64:72, 0:1]
+    for out_ref, old, lo, hi in (
+        (value_ref, old_values(misc_ref, layer), 0, 128),
+        (vector_ref, old_vectors(vhist_ref, layer), 128, 384),
     ):
-        rows = [old_ref[layer, k].astype(f32) for k in range(CONV - 1)]
-        rows += [fresh_ref[8 * t : 8 * t + 8, lo:hi].astype(f32) for t in range(NEW)]
+        rows = old + [fresh_ref[8 * t : 8 * t + 8, lo:hi].astype(f32) for t in range(NEW)]
         for k in range(CONV - 1):
             chosen = rows[k + 1]
             for r in range(k + 2, k + NEW + 1):
@@ -397,12 +455,27 @@
     return results[0] if len(outs) == 1 else results
 
 
+def close(layer, *args):
+    vmem = pl.BlockSpec(memory_space=pltpu.VMEM)
+    block = pl.BlockSpec((1, SEQ, 128, 128), lambda i: (layer, 0, 0, 0))
+    space = [vmem] * 7 + [pl.BlockSpec(memory_space=pl.ANY)] * (len(args) - 7)
+    return pl.pallas_call(
+        functools.partial(finish, layer=layer),
+        grid=(1,),
+        out_shape=[
+            jax.ShapeDtypeStruct((LAYERS, SEQ, 128, 128), f32),
+            jax.ShapeDtypeStruct((3, 8, 128), bf16),
+            jax.ShapeDtypeStruct((3, 8, 256), bf16),
+        ],
+        in_specs=space,
+        out_specs=[block, vmem, vmem],
+        input_output_aliases={7: 0} if layer else {},
+        compiler_params=pltpu.CompilerParams(vmem_limit_bytes=12 << 20),
+    )(*args)
+
+
 def from_y(value, k):
     return lax.ppermute(value, "y", [(i, (i + k) % YN) for i in range(YN)])
-
-
-def around_y(value):
-    return [value, *(from_y(value, k) for k in range(1, YN))]
 
 
 def body(
@@ -439,20 +512,46 @@
             pltpu.SemaphoreType.DMA((4,)),
         ],
     )(tokens, vector_weight.transpose(0, 2, 3, 1), vector_history, vector_taps)
-    first, own_out = lax.optimization_barrier((first, out_weight))
+    first, outs, lens = lax.optimization_barrier(
+        (first, out_weight.reshape(256, 512), lengths)
+    )
     first = exchange(first, "z")
-    at = jnp.concatenate([jnp.stack([z, y, square_lane]), lengths]).astype(jnp.int32)
-    scale = jnp.concatenate([step_bias.reshape(4), decay_rate.reshape(4)])
-    own_out = around_y(own_out[0])
+    out_2 = from_y(outs, 2)
+    at = jnp.stack([z, y, square_lane]).astype(jnp.int32)
+    misc, base = pl.pallas_call(
+        setup,
+        out_shape=[jax.ShapeDtypeStruct((88, 128), f32), jax.ShapeDtypeStruct((1280, 128), bf16)],
+        in_specs=[pl.BlockSpec(memory_space=pltpu.SMEM)]
+        + [pl.BlockSpec(memory_space=pltpu.MemorySpace.HBM)] * 7,
+        out_specs=[pl.BlockSpec(memory_space=pltpu.VMEM)] * 2,
+        scratch_shapes=[
+            pltpu.VMEM((2, 512), f32),
+            pltpu.VMEM((2, 2), f32),
+            pltpu.VMEM((2, 2), f32),
+            pltpu.VMEM((2, CONV, 128), bf16),
+            pltpu.VMEM((SEQ, 3, 2, 128), bf16),
+            pltpu.SemaphoreType.DMA((7,)),
+        ],
+    )(
+        lens,
+        norm_gain,
+        step_bias,
+        decay_rate,
+        value_taps,
+        value_history.transpose(1, 2, 0, 3),
+        gate_weight,
+        value_weight,
+    )
     plane = exchange(copies(first[:, :2], YN), "y").reshape(512, 512)
+    out_1 = from_y(outs, 1)
+    out_3 = from_y(outs, 3)
+    outs = [outs, out_1, out_2, out_3]
+    blocks = first[:, 2].reshape(64, 4, 128).transpose(1, 0, 2).reshape(256, 128)
+    later = lax.dynamic_update_slice(base, blocks, (1024, 0))
     vhist, vtaps = call(unpack, [((2, 3, 8, 256), bf16), ((2, 8, 256), bf16)], 0, plane)
-    history = jnp.pad(value_history.transpose(0, 2, 1, 3), ((0, 0), (0, 1), (0, 2), (0, 0)))
-    history += jnp.pad(value_taps[:, None], ((0, 0), (3, 0), (0, 4), (0, 0)))
-    gain = jnp.pad(norm_gain, ((0, 6), (0, 0)))
-    states = recurrent_state.reshape(LAYERS, SEQ, 128, 128)
-
-    def mid(part, layer):
-        old = (history, vhist)
+    states = [recurrent_state[n : n + 1].reshape(1, SEQ, 128, 128) for n in range(LAYERS)]
+
+    def mid(part, layer, *done):
         msg, keep, write, decay, fresh = call(
             functools.partial(middle, layer=layer),
             [
@@ -462,28 +561,17 @@
                 ((8, 128), f32),
                 ((32, 384), bf16),
             ],
-            2,
+            1,
             at,
-            scale,
             part,
-            history,
+            misc,
             vhist,
             vtaps,
-            states,
+            states[layer],
         )
-        after = call(
-            functools.partial(finish, layer=layer),
-            [((SEQ, 128, 128), f32), ((3, 8, 128), bf16), ((3, 8, 256), bf16)],
-            1,
-            at,
-            keep,
-            write,
-            decay,
-            fresh,
-            *old,
-            states,
-        )
-        return exchange(msg, ("y", "dp")).reshape(YN, DN * 8, 128), after
+        after = close(layer, misc, keep, write, decay, fresh, vhist, states[layer], *done)
+        msg = exchange(msg, ("y", "dp"))
+        return msg.reshape(YN, DN * 8, 128), after
 
     part = call(
         first_projection,
@@ -491,64 +579,49 @@
         1,
         at,
         plane,
-        gain,
+        misc,
         gate_weight,
         value_weight,
         step_weight,
     )
     part = exchange(part, "dp")
-    mixed, (state0, value0, vector0) = mid(part, 0)
+    later_2 = from_y(later, 2)
+    mixed, (state, value0, vector0) = mid(part, 0)
+    later_3 = from_y(later, 3)
     update = call(
         functools.partial(out_projection, first_row=0),
         [((ZN, 4, 512), bf16)],
         1,
         at,
         mixed,
-        *own_out,
-    )
-
-    def lanes(w):
-        return w.reshape(4, 128, 128).transpose(1, 0, 2).reshape(128, 512)
-
-    later = jnp.concatenate(
-        [
-            lanes(gate_weight[1]),
-            lanes(value_weight[1]),
-            out_weight[1],
-            first[:, 2].reshape(64, 512),
-        ],
-        axis=0,
-    )
-    update, later = lax.optimization_barrier((update, later))
+        *outs,
+    )
     update = exchange(update, "z")
-    pieces = [later, from_y(later, 1), from_y(later, 2)]
+    later_1 = from_y(later, 1)
     update = jnp.sum(update.astype(f32), axis=0)[:3]
     token_rows = (tokens.astype(f32) + update).astype(bf16)
     quarter = copies(jnp.pad(token_rows, ((0, 1), (0, 0))), ZN)
-    quarter, last = lax.optimization_barrier((quarter, later))
-    quarter = exchange(quarter, "z")
-    last = from_y(last, 3)
-    quarter = quarter.reshape(64, 512)
-    later = [*pieces, last]
+    quarter = exchange(quarter, "z").reshape(64, 512)
+    later = [later, later_1, later_2, later_3]
     part = call(
         second_projection,
         [((YN, 64, COLS), bf16)],
         1,
         at,
         quarter,
-        gain,
-        step_weight,
+        misc,
+        step_weight[1:],
         *later,
     )
     part = exchange(part.reshape(YN * DN, 8, COLS), ("y", "dp")).reshape(YN, DN, 8, COLS)
-    mixed, (state1, value1, vector1) = mid(part, 1)
+    mixed, (state, value1, vector1) = mid(part, 1, state)
     update = call(
-        functools.partial(out_projection, first_row=256),
+        functools.partial(out_projection, first_row=128),
         [((ZN, 4, 512), bf16)],
         1,
         at,
         mixed,
-        *later,
+        *outs,
         jnp.concatenate([vector0, vector1], axis=0).reshape(48, 256),
     )
     update = exchange(update, "z")
@@ -560,7 +633,7 @@
     next_vector = returned.reshape(2, SEQ, 3, 2, 32)
     return (
         token_rows,
-        jnp.stack([state0, state1]).reshape(recurrent_state.shape),
+        state.reshape(recurrent_state.shape),
         jnp.stack([value0, value1])[:, :, :SEQ].transpose(0, 2, 1, 3),
         next_vector,
     )
@@ -569,6 +642,7 @@
 def solution(mesh):
     grid = Mesh(mesh.devices.reshape(ZN, YN, DN), ("z", "y", "dp"))
     tp = ("z", "y")
+
     return jax.shard_map(
         body,
         mesh=grid,

time: 168 us -> 174 us (1.036)
  starting transfers between devices: 77.7 us -> 66.2 us
  blocking collectives: 17.3 us -> 28.2 us
  waiting for transfers between devices: 46.2 us -> 52.9 us
  Pallas kernels: 14.2 us -> 17.6 us
  local copies, waits for them, and re-layouts: 8.97 us -> 5.76 us
    all_to_all x1, blocking collectives: 17.3 us -> 28.2 us  [exchange(): return lax.all_to_all(pieces, axis, 0, 0, tiled=True)]
    all_to_all x8, starting transfers between devices: 58.3 us -> 48.8 us  [exchange(): return lax.all_to_all(pieces, axis, 0, 0, tiled=True)]
    all_to_all x8, waiting for transfers between devices: 46.2 us -> 52.9 us  [exchange(): return lax.all_to_all(pieces, axis, 0, 0, tiled=True)]
    pallas_call x0 -> x3, Pallas kernels: none -> 4.6 us  [the longest x1 2.54 us: body(): pl.pallas_call(setup, out_shape=[jax.ShapeDtypeStruct((88, 128), f32), ja...]
    unnamed x34 -> x15, local copies, waits for them, and re-layouts: 3.9 us -> 0.63 us
    ppermute x6, starting transfers between devices: 19.4 us -> 17.4 us  [from_y(): return lax.ppermute(value, 'y', [(i, (i + k) % YN) for i in range(YN)])]
    pallas_call x9 -> x7, Pallas kernels: 12.3 us -> 11.2 us  [call(): pl.pallas_call(kernel, out_shape=outs, in_specs=space, out_specs=[vmem] *...]
  transfers between devices with their start and end apart: 14 -> 14, of which waited for: 8 -> 7; matrix products, arithmetic and copies ran while one was open for 2% -> 2% of each run, Pallas kernels for 3% -> 5%
where the time goes in v5:
time: 174 us; the launch traced here: 172 us
  starting transfers between devices  66.2 us (38%)
  waiting for transfers between devices  52.9 us (30%)
  blocking collectives  28.2 us (16%)
  Pallas kernels  17.6 us (10%)
  local copies, waits for them, and re-layouts  5.76 us (3%)
    all_to_all x8, waiting for transfers between devices, exchange(): return lax.all_to_all(pieces, axis, 0, 0, tiled=True)  52.9 us
    all_to_all x8, starting transfers between devices, exchange(): return lax.all_to_all(pieces, axis, 0, 0, tiled=True)  48.8 us
    all_to_all x1, blocking collectives, exchange(): return lax.all_to_all(pieces, axis, 0, 0, tiled=True)  28.2 us
    ppermute x6, starting transfers between devices, from_y(): return lax.ppermute(value, 'y', [(i, (i + k) % YN) for i in range(YN)])  17.4 us
    pallas_call x7, Pallas kernels, call(): pl.pallas_call(kernel, out_shape=outs, in_specs=space, out_specs=[vmem] *...  11.2 us
  transfers between devices with their start and end apart: 14, of which 7 were waited for; matrix products, arithmetic and copies ran while one was open for 2% of the time, Pallas kernels for 5%

profile of v5, /device:TPU:1, one launch (start us, length us, event | category | flops | bytes accessed | tf_op | source)
XLA Modules:
  0.0 172.4 jit_solution(1267746350708423792)
XLA Ops:
  2.5 28.2 %all_to_all.45 = bf16[16,3,4,512]{3,2,1,0:T(4,128)(2,1)S(1)} all-to-all(bf16[16,3,4,512]{3,2,1,0:T(4,128)(2,1)} %shard_map.174), channel_id=1, replica_groups=mesh['z'=16,'y'=4,'dp'=8] {'z'}, dimensions={0} | all-to-all | bytes 393216 | tf_op jit(solution)/shard_map/all_to_all | solution.py:27
  31.7 4.3 %all-to-all-start.1 = ((bf16[4,16,2,4,512]{4,3,2,1,0:T(4,128)(2,1)}), bf16[4,16,2,4,512]{4,3,2,1,0:T(4,128)(2,1)}, u32[]{:S(2)}, u32[]{:S(2)}) async-start(bf16[4,16,2,4,512]{4,3,2,1,0:T(4,128)(2,1)} %broadcast_in_dim.4), calls=%async_computation.1 | async-start | bytes 1048576 | tf_op jit(solution)/shard_map/all_to_all | solution.py:27
  36.0 4.6 %collective-permute-start.2 = (bf16[256,512]{1,0:T(8,128)(2,1)S(1)}, bf16[256,512]{1,0:T(8,128)(2,1)S(1)}, u32[]{:S(2)}, u32[]{:S(2)}) collective-permute-start(bf16[256,512]{1,0:T(8,128)(2,1)S(1)} %bitcast.31), channel_id=1, source_target_pairs={{0,24},{8,0},{16,8},{24,16},{1,25},{9,1},{17,9},{25,17},{2,26},{10... | collective-permute-start | bytes 786440 | tf_op jit(solution)/shard_map/ppermute | solution.py:478
  40.6 2.5 %collective-permute-start.1 = (bf16[256,512]{1,0:T(8,128)(2,1)S(1)}, bf16[256,512]{1,0:T(8,128)(2,1)S(1)}, u32[]{:S(2)}, u32[]{:S(2)}) collective-permute-start(bf16[256,512]{1,0:T(8,128)(2,1)S(1)} %bitcast.32), channel_id=1, source_target_pairs={{0,16},{8,24},{16,0},{24,8},{1,17},{9,25},{17,1},{25,9},{2,18},{10... | collective-permute-start | bytes 786440 | tf_op jit(solution)/shard_map/ppermute | solution.py:478
  43.1 2.5 %collective-permute-start = (bf16[256,512]{1,0:T(8,128)(2,1)S(1)}, bf16[256,512]{1,0:T(8,128)(2,1)S(1)}, u32[]{:S(2)}, u32[]{:S(2)}) collective-permute-start(bf16[256,512]{1,0:T(8,128)(2,1)S(1)} %bitcast.33), channel_id=1, source_target_pairs={{0,8},{8,16},{16,24},{24,0},{1,9},{9,17},{17,25},{25,1},{2,10},{10... | collective-permute-start | bytes 786440 | tf_op jit(solution)/shard_map/ppermute | solution.py:478
  45.6 2.5 %shard_map.175 = (f32[88,128]{1,0:T(8,128)}, bf16[1280,128]{1,0:T(8,128)(2,1)}) custom-call(s32[6]{0:T(128)} %len_ref, f32[2,512]{1,0:T(2,128)} %gain_hbm.1, f32[2,2]{1,0:T(2,128)} %bias_hbm.1, f32[2,2]{1,0:T(2,128)} %rate_hbm.1, bf16[2,4,128]{2,1,0:T(4,128)(2,1)} %taps_hbm.3, bf16[6,3,2,128]{3,2,1,0:T(2,128)(2,1)} %bitcast.45, ...), custom_call_target="tpu_custom_call" | custom-call | tf_op jit(solution)/shard_map/pallas_call | solution.py:521
  51.5 10.5 %all-to-all-start.2 = ((bf16[8,24,640]{2,1,0:T(8,128)(2,1)}), bf16[8,24,640]{2,1,0:T(8,128)(2,1)S(1)}, u32[]{:S(2)}, u32[]{:S(2)}) async-start(bf16[8,24,640]{2,1,0:T(8,128)(2,1)} %shard_map.176), calls=%async_computation.2 | async-start | bytes 491520 | tf_op jit(solution)/shard_map/all_to_all | solution.py:27
  63.7 4.6 %all-to-all-done.2.part_ref = bf16[8,24,640]{2,1,0:T(8,128)(2,1)S(1)} async-done(((bf16[8,24,640]{2,1,0:T(8,128)(2,1)}), bf16[8,24,640]{2,1,0:T(8,128)(2,1)S(1)}, u32[]{:S(2)}, u32[]{:S(2)}) %all-to-all-start.2) | async-done | bytes 245792 | tf_op jit(solution)/shard_map/all_to_all | solution.py:27
  70.0 5.4 %all-to-all-start.3 = ((bf16[32,8,128]{2,1,0:T(8,128)(2,1)}), bf16[32,8,128]{2,1,0:T(8,128)(2,1)S(1)}, u32[]{:S(2)}, u32[]{:S(2)}) async-start(bf16[32,8,128]{2,1,0:T(8,128)(2,1)} %get-tuple-element.32), calls=%async_computation.3 | async-start | bytes 131072 | tf_op jit(solution)/shard_map/all_to_all | solution.py:27
  75.5 7.3 %all-to-all-done.3 = bf16[32,8,128]{2,1,0:T(8,128)(2,1)S(1)} async-done(((bf16[32,8,128]{2,1,0:T(8,128)(2,1)}), bf16[32,8,128]{2,1,0:T(8,128)(2,1)S(1)}, u32[]{:S(2)}, u32[]{:S(2)}) %all-to-all-start.3) | async-done | bytes 65568 | tf_op jit(solution)/shard_map/all_to_all | solution.py:27
  84.2 4.8 %all-to-all-start.4 = ((bf16[16,4,512]{2,1,0:T(4,128)(2,1)}), bf16[16,4,512]{2,1,0:T(4,128)(2,1)S(1)}, u32[]{:S(2)}, u32[]{:S(2)}) async-start(bf16[16,4,512]{2,1,0:T(4,128)(2,1)} %shard_map.179), calls=%async_computation.4 | async-start | bytes 131072 | tf_op jit(solution)/shard_map/all_to_all | solution.py:27
  89.1 2.8 %collective-permute-start.5 = (bf16[1280,128]{1,0:T(8,128)(2,1)S(1)}, bf16[1280,128]{1,0:T(8,128)(2,1)S(1)}, u32[]{:S(2)}, u32[]{:S(2)}) collective-permute-start(bf16[1280,128]{1,0:T(8,128)(2,1)S(1)} %constant_dynamic-update-slice_fusion.w0), channel_id=1, source_target_pairs={{0,24},{8,0},{16,8},{24,16},{1,25},{9,1},{17,9},{25,17},{2,26},{10... | collective-permute-start | bytes 983048 | tf_op jit(solution)/shard_map/ppermute | solution.py:478
  91.9 3.2 %collective-permute-start.4 = (bf16[1280,128]{1,0:T(8,128)(2,1)S(1)}, bf16[1280,128]{1,0:T(8,128)(2,1)}, u32[]{:S(2)}, u32[]{:S(2)}) collective-permute-start(bf16[1280,128]{1,0:T(8,128)(2,1)S(1)} %constant_dynamic-update-slice_fusion.w0), channel_id=1, source_target_pairs={{0,16},{8,24},{16,0},{24,8},{1,17},{9,25},{17,1},{25,9},{2,18},{10... | collective-permute-start | bytes 983048 | tf_op jit(solution)/shard_map/ppermute | solution.py:478
  95.1 1.9 %collective-permute-start.3 = (bf16[1280,128]{1,0:T(8,128)(2,1)S(1)}, bf16[1280,128]{1,0:T(8,128)(2,1)}, u32[]{:S(2)}, u32[]{:S(2)}) collective-permute-start(bf16[1280,128]{1,0:T(8,128)(2,1)S(1)} %constant_dynamic-update-slice_fusion.w0), channel_id=1, source_target_pairs={{0,8},{8,16},{16,24},{24,0},{1,9},{9,17},{17,25},{25,1},{2,10},{10... | collective-permute-start | bytes 983048 | tf_op jit(solution)/shard_map/ppermute | solution.py:478
  97.0 3.6 %all-to-all-done.4 = bf16[16,4,512]{2,1,0:T(4,128)(2,1)S(1)} async-done(((bf16[16,4,512]{2,1,0:T(4,128)(2,1)}), bf16[16,4,512]{2,1,0:T(4,128)(2,1)S(1)}, u32[]{:S(2)}, u32[]{:S(2)}) %all-to-all-start.4) | async-done | bytes 65568 | tf_op jit(solution)/shard_map/all_to_all | solution.py:27
  101.3 7.9 %all-to-all-start.5 = ((bf16[16,4,512]{2,1,0:T(4,128)(2,1)}), bf16[16,4,512]{2,1,0:T(4,128)(2,1)S(1)}, u32[]{:S(2)}, u32[]{:S(2)}) async-start(bf16[16,4,512]{2,1,0:T(4,128)(2,1)} %broadcast_in_dim.5), calls=%async_computation.5 | async-start | bytes 131072 | tf_op jit(solution)/shard_map/all_to_all | solution.py:27
  109.3 11.5 %all-to-all-done.5 = bf16[16,4,512]{2,1,0:T(4,128)(2,1)S(1)} async-done(((bf16[16,4,512]{2,1,0:T(4,128)(2,1)}), bf16[16,4,512]{2,1,0:T(4,128)(2,1)S(1)}, u32[]{:S(2)}, u32[]{:S(2)}) %all-to-all-start.5) | async-done | bytes 65568 | tf_op jit(solution)/shard_map/all_to_all | solution.py:27
  120.9 2.4 %shard_map.180 = bf16[4,64,640]{2,1,0:T(8,128)(2,1)} custom-call(s32[3]{0:T(128)S(1)} %pad_add_fusion.at_ref, bf16[64,512]{1,0:T(8,128)(2,1)S(1)} %reshape.56.rows_ref, f32[88,128]{1,0:T(8,128)S(1)} %copy-done, bf16[1,512,128]{2,1,0:T(8,128)(2,1)S(1)} %slice.36.step_ref, bf16[1280,128]{1,0:T(8,128)(2,1)S(1)} %constant_dynamic-update-slice_fusion.w0, ...), custom_call_target="tpu_custom_call" | custom-call | tf_op jit(solution)/shard_map/pallas_call | solution.py:448
  123.2 8.6 %all-to-all-start.6 = ((bf16[32,8,640]{2,1,0:T(8,128)(2,1)}), bf16[32,8,640]{2,1,0:T(8,128)(2,1)S(1)}, u32[]{:S(2)}, u32[]{:S(2)}) async-start(bf16[32,8,640]{2,1,0:T(8,128)(2,1)} %bitcast.10), calls=%async_computation.6 | async-start | bytes 655360 | tf_op jit(solution)/shard_map/all_to_all | solution.py:27
  132.8 8.5 %all-to-all-done.6 = bf16[32,8,640]{2,1,0:T(8,128)(2,1)S(1)} async-done(((bf16[32,8,640]{2,1,0:T(8,128)(2,1)}), bf16[32,8,640]{2,1,0:T(8,128)(2,1)S(1)}, u32[]{:S(2)}, u32[]{:S(2)}) %all-to-all-start.6) | async-done | bytes 327712 | tf_op jit(solution)/shard_map/all_to_all | solution.py:27
  143.0 3.7 %all-to-all-start.7 = ((bf16[32,8,128]{2,1,0:T(8,128)(2,1)}), bf16[32,8,128]{2,1,0:T(8,128)(2,1)S(1)}, u32[]{:S(2)}, u32[]{:S(2)}) async-start(bf16[32,8,128]{2,1,0:T(8,128)(2,1)} %get-tuple-element.35), calls=%async_computation.7 | async-start | bytes 131072 | tf_op jit(solution)/shard_map/all_to_all | solution.py:27
  147.8 6.4 %all-to-all-done.7 = bf16[32,8,128]{2,1,0:T(8,128)(2,1)S(1)} async-done(((bf16[32,8,128]{2,1,0:T(8,128)(2,1)}), bf16[32,8,128]{2,1,0:T(8,128)(2,1)S(1)}, u32[]{:S(2)}, u32[]{:S(2)}) %all-to-all-start.7) | async-done | bytes 65568 | tf_op jit(solution)/shard_map/all_to_all | solution.py:27
  155.7 3.5 %all-to-all-start.8 = ((bf16[16,4,512]{2,1,0:T(4,128)(2,1)}), bf16[16,4,512]{2,1,0:T(4,128)(2,1)S(1)}, u32[]{:S(2)}, u32[]{:S(2)}) async-start(bf16[16,4,512]{2,1,0:T(4,128)(2,1)} %shard_map.184), calls=%async_computation.8 | async-start | bytes 131072 | tf_op jit(solution)/shard_map/all_to_all | solution.py:27
  159.8 11.1 %all-to-all-done.8 = bf16[16,4,512]{2,1,0:T(4,128)(2,1)S(1)} async-done(((bf16[16,4,512]{2,1,0:T(4,128)(2,1)}), bf16[16,4,512]{2,1,0:T(4,128)(2,1)S(1)}, u32[]{:S(2)}, u32[]{:S(2)}) %all-to-all-start.8) | async-done | bytes 65568 | tf_op jit(solution)/shard_map/all_to_all | solution.py:27
  (56 shorter events, 19.2 us)
Async XLA Ops:
  31.7 4.3 %copy-start.3 = (bf16[2,128,512]{2,1,0:T(8,128)(2,1)S(1)}, bf16[2,128,512]{2,1,0:T(8,128)(2,1)}, u32[]{:S(2)}) copy-start(bf16[2,128,512]{2,1,0:T(8,128)(2,1)} %param.26) | copy-start | bytes 786436
  31.7 16.5 %all-to-all-start.1 = ((bf16[4,16,2,4,512]{4,3,2,1,0:T(4,128)(2,1)}), bf16[4,16,2,4,512]{4,3,2,1,0:T(4,128)(2,1)}, u32[]{:S(2)}, u32[]{:S(2)}) async-start(bf16[4,16,2,4,512]{4,3,2,1,0:T(4,128)(2,1)} %broadcast_in_dim.4), calls=%async_computation.1 | async-start | bytes 1048576 | tf_op jit(solution)/shard_map/all_to_all | solution.py:27
  36.0 39.4 %collective-permute-start.2 = (bf16[256,512]{1,0:T(8,128)(2,1)S(1)}, bf16[256,512]{1,0:T(8,128)(2,1)S(1)}, u32[]{:S(2)}, u32[]{:S(2)}) collective-permute-start(bf16[256,512]{1,0:T(8,128)(2,1)S(1)} %bitcast.31), channel_id=1, source_target_pairs={{0,24},{8,0},{16,8},{24,16},{1,25},{9,1},{17,9},{25,17},{2,26},{10... | collective-permute-start | bytes 786440 | tf_op jit(solution)/shard_map/ppermute | solution.py:478
  40.6 34.8 %collective-permute-start.1 = (bf16[256,512]{1,0:T(8,128)(2,1)S(1)}, bf16[256,512]{1,0:T(8,128)(2,1)S(1)}, u32[]{:S(2)}, u32[]{:S(2)}) collective-permute-start(bf16[256,512]{1,0:T(8,128)(2,1)S(1)} %bitcast.32), channel_id=1, source_target_pairs={{0,16},{8,24},{16,0},{24,8},{1,17},{9,25},{17,1},{25,9},{2,18},{10... | collective-permute-start | bytes 786440 | tf_op jit(solution)/shard_map/ppermute | solution.py:478
  43.1 32.4 %collective-permute-start = (bf16[256,512]{1,0:T(8,128)(2,1)S(1)}, bf16[256,512]{1,0:T(8,128)(2,1)S(1)}, u32[]{:S(2)}, u32[]{:S(2)}) collective-permute-start(bf16[256,512]{1,0:T(8,128)(2,1)S(1)} %bitcast.33), channel_id=1, source_target_pairs={{0,8},{8,16},{16,24},{24,0},{1,9},{9,17},{17,25},{25,1},{2,10},{10... | collective-permute-start | bytes 786440 | tf_op jit(solution)/shard_map/ppermute | solution.py:478
  48.3 1.3 copy-start
  48.3 1.3 copy-start.1
  48.3 1.3 copy-start.2
  48.3 1.3 copy-start.4
  51.5 16.9 %all-to-all-start.2 = ((bf16[8,24,640]{2,1,0:T(8,128)(2,1)}), bf16[8,24,640]{2,1,0:T(8,128)(2,1)S(1)}, u32[]{:S(2)}, u32[]{:S(2)}) async-start(bf16[8,24,640]{2,1,0:T(8,128)(2,1)} %shard_map.176), calls=%async_computation.2 | async-start | bytes 491520 | tf_op jit(solution)/shard_map/all_to_all | solution.py:27
  70.0 12.8 %all-to-all-start.3 = ((bf16[32,8,128]{2,1,0:T(8,128)(2,1)}), bf16[32,8,128]{2,1,0:T(8,128)(2,1)S(1)}, u32[]{:S(2)}, u32[]{:S(2)}) async-start(bf16[32,8,128]{2,1,0:T(8,128)(2,1)} %get-tuple-element.32), calls=%async_computation.3 | async-start | bytes 131072 | tf_op jit(solution)/shard_map/all_to_all | solution.py:27
  84.2 4.9 %copy-start.5 = (bf16[1280,128]{1,0:T(8,128)(2,1)S(1)}, bf16[1280,128]{1,0:T(8,128)(2,1)}, u32[]{:S(2)}) copy-start(bf16[1280,128]{1,0:T(8,128)(2,1)} %get-tuple-element.34) | copy-start | bytes 983044
  84.2 16.4 %all-to-all-start.4 = ((bf16[16,4,512]{2,1,0:T(4,128)(2,1)}), bf16[16,4,512]{2,1,0:T(4,128)(2,1)S(1)}, u32[]{:S(2)}, u32[]{:S(2)}) async-start(bf16[16,4,512]{2,1,0:T(4,128)(2,1)} %shard_map.179), calls=%async_computation.4 | async-start | bytes 131072 | tf_op jit(solution)/shard_map/all_to_all | solution.py:27
  89.1 11.5 %copy-start.6 = (bf16[3,512]{1,0:T(4,128)(2,1)S(1)}, bf16[3,512]{1,0:T(4,128)(2,1)}, u32[]{:S(2)}) copy-start(bf16[3,512]{1,0:T(4,128)(2,1)} %token_hbm.1) | copy-start | bytes 9220
  89.1 31.7 %collective-permute-start.5 = (bf16[1280,128]{1,0:T(8,128)(2,1)S(1)}, bf16[1280,128]{1,0:T(8,128)(2,1)S(1)}, u32[]{:S(2)}, u32[]{:S(2)}) collective-permute-start(bf16[1280,128]{1,0:T(8,128)(2,1)S(1)} %constant_dynamic-update-slice_fusion.w0), channel_id=1, source_target_pairs={{0,24},{8,0},{16,8},{24,16},{1,25},{9,1},{17,9},{25,17},{2,26},{10... | collective-permute-start | bytes 983048 | tf_op jit(solution)/shard_map/ppermute | solution.py:478
  91.9 28.9 %collective-permute-start.4 = (bf16[1280,128]{1,0:T(8,128)(2,1)S(1)}, bf16[1280,128]{1,0:T(8,128)(2,1)}, u32[]{:S(2)}, u32[]{:S(2)}) collective-permute-start(bf16[1280,128]{1,0:T(8,128)(2,1)S(1)} %constant_dynamic-update-slice_fusion.w0), channel_id=1, source_target_pairs={{0,16},{8,24},{16,0},{24,8},{1,17},{9,25},{17,1},{25,9},{2,18},{10... | collective-permute-start | bytes 983048 | tf_op jit(solution)/shard_map/ppermute | solution.py:478
  95.1 25.8 %collective-permute-start.3 = (bf16[1280,128]{1,0:T(8,128)(2,1)S(1)}, bf16[1280,128]{1,0:T(8,128)(2,1)}, u32[]{:S(2)}, u32[]{:S(2)}) collective-permute-start(bf16[1280,128]{1,0:T(8,128)(2,1)S(1)} %constant_dynamic-update-slice_fusion.w0), channel_id=1, source_target_pairs={{0,8},{8,16},{16,24},{24,0},{1,9},{9,17},{17,25},{25,1},{2,10},{10... | collective-permute-start | bytes 983048 | tf_op jit(solution)/shard_map/ppermute | solution.py:478
  101.3 19.5 %all-to-all-start.5 = ((bf16[16,4,512]{2,1,0:T(4,128)(2,1)}), bf16[16,4,512]{2,1,0:T(4,128)(2,1)S(1)}, u32[]{:S(2)}, u32[]{:S(2)}) async-start(bf16[16,4,512]{2,1,0:T(4,128)(2,1)} %broadcast_in_dim.5), calls=%async_computation.5 | async-start | bytes 131072 | tf_op jit(solution)/shard_map/all_to_all | solution.py:27
  123.2 18.1 %all-to-all-start.6 = ((bf16[32,8,640]{2,1,0:T(8,128)(2,1)}), bf16[32,8,640]{2,1,0:T(8,128)(2,1)S(1)}, u32[]{:S(2)}, u32[]{:S(2)}) async-start(bf16[32,8,640]{2,1,0:T(8,128)(2,1)} %bitcast.10), calls=%async_computation.6 | async-start | bytes 655360 | tf_op jit(solution)/shard_map/all_to_all | solution.py:27
  143.0 11.1 %all-to-all-start.7 = ((bf16[32,8,128]{2,1,0:T(8,128)(2,1)}), bf16[32,8,128]{2,1,0:T(8,128)(2,1)S(1)}, u32[]{:S(2)}, u32[]{:S(2)}) async-start(bf16[32,8,128]{2,1,0:T(8,128)(2,1)} %get-tuple-element.35), calls=%async_computation.7 | async-start | bytes 131072 | tf_op jit(solution)/shard_map/all_to_all | solution.py:27
  155.7 15.2 %all-to-all-start.8 = ((bf16[16,4,512]{2,1,0:T(4,128)(2,1)}), bf16[16,4,512]{2,1,0:T(4,128)(2,1)S(1)}, u32[]{:S(2)}, u32[]{:S(2)}) async-start(bf16[16,4,512]{2,1,0:T(4,128)(2,1)} %shard_map.184), calls=%async_computation.8 | async-start | bytes 131072 | tf_op jit(solution)/shard_map/all_to_all | solution.py:27
